TPU v7x, 128 devices: a whole 4x4x4 slice. The times are simulated.
128 devices in a mesh: sp: 16 (over z, y), dp: 8 (over x, core).
Axes of the slice: x: 4, y: 4, z: 4, core: 2. Of those that a mesh axis runs over, the one named last changes fastest.
Arguments:
- query: bfloat16 [8, 3072, 3072], P('dp', 'sp'), may hold values from -18 to 18
- latent: bfloat16 [8, 3072, 1024], P('dp', 'sp'), may hold values from -6 to 6
- rope_key: bfloat16 [8, 3072, 32], P('dp', 'sp'), may hold values from -5 to 5
- latent_norm_gain: float32 [1024], replicated, may hold values from 0.1 to 1.9
- key_up_matrix: bfloat16 [2048, 1024], P('dp'), may hold values from -0.1875 to 0.1875
- value_up_matrix: bfloat16 [2048, 1024], P('dp'), may hold values from -0.1875 to 0.1875
- out_grad: bfloat16 [8, 3072, 2048], P('dp', 'sp'), may hold values from -6 to 6
Outputs:
- query_grad: bfloat16 [8, 3072, 3072], P('dp', 'sp')
- latent_grad: float32 [8, 3072, 1024], P('dp', 'sp')
- rope_key_grad: float32 [8, 3072, 32], P('dp', 'sp')
- key_weight_grad: float32 [2048, 1024], P('dp')
- value_weight_grad: float32 [2048, 1024], P('dp')
- gain_grad: float32 [1024], replicated
All inputs are finite; a program needn't handle non-finite values.
Results may differ from a plain program's by a relative error of at most 0.011.
Values may be sent and summed in bfloat16 or wider, within the bound.
A program may use at most 256 MiB of HBM per device.

v0:
```python
import functools

import jax
import jax.numpy as jnp
from jax import lax
from jax.sharding import Mesh
from jax.sharding import PartitionSpec as P

ATTENTION_HEADS = 32
PLAIN_HEAD_WIDTH = 64
ROPE = 32
VALUE_HEAD_WIDTH = 64
SPAN = 64
DP = ("dp_0", "dp_1")
SP = ("sp_0", "sp_1")
SP_DP = ("sp_0", "sp_1", "dp_0", "dp_1")


eps = 1e-06
rope_base = 10000.0


def from_everyone(value, axis):
    size = lax.axis_size(axis)
    return lax.all_to_all(
        jnp.broadcast_to(value[None], (size, *value.shape)), axis, 0, 0, tiled=True
    )


def in_order(blocks, dim):
    blocks = jnp.moveaxis(blocks, 0, dim)
    shape = blocks.shape
    return blocks.reshape(*shape[:dim], shape[dim] * shape[dim + 1], *shape[dim + 2 :])


def gather_directly(value, axis, dim):
    blocks = from_everyone(value, axis)
    return in_order(blocks, dim)


def split_up(value, dim, size):
    shape = value.shape
    blocks = value.reshape(*shape[:dim], size, shape[dim] // size, *shape[dim + 1 :])
    return jnp.moveaxis(blocks, dim, 0)


def sent_and_summed(value, axis, dim):
    blocks = split_up(value, dim, lax.axis_size(axis))
    arrived = lax.all_to_all(blocks, axis, split_axis=0, concat_axis=0, tiled=True)
    return arrived.sum(axis=0)


def edges_of(length, count):
    unit = 8 if length >= 8 * count else 1
    return [length // unit * k // count * unit for k in range(1, count)]


def all_blocks(value, axes, turns):
    blocks = value[None]
    for k in turns:
        blocks = lax.all_gather(blocks, axes[k], axis=0, tiled=True)
    carried = [lax.axis_size(axes[k]) for k in reversed(turns)]
    blocks = blocks.reshape(*carried, *value.shape)
    turned = sorted(range(len(turns)), key=lambda place: turns[len(turns) - 1 - place])
    return blocks.transpose(*turned, *range(len(turns), blocks.ndim)).reshape(-1, *value.shape)


def gather_all_axes(value, axes, dim):
    numbers = list(range(len(axes)))[::-1]
    widest = value.shape.index(max(value.shape[:-1] or value.shape))
    edges = [0, *edges_of(value.shape[widest], len(axes)), value.shape[widest]]
    finished = []
    for k, (start, end) in enumerate(zip(edges, edges[1:])):
        if end > start:
            section = lax.slice_in_dim(value, start, end, axis=widest)
            finished.append(all_blocks(section, axes, numbers[k:] + numbers[:k]))
    return in_order(jnp.concatenate(finished, axis=widest + 1), dim)


def by_axis(value, axes):
    return functools.reduce(lax.psum, axes, value)


def rotate(values, cosine, sine):
    half = values.shape[-1] // 2
    first = values[..., :half]
    second = values[..., half:]
    return jnp.concatenate(
        [first * cosine - second * sine, second * cosine + first * sine], axis=-1
    )


def angles(length, width):
    inverse = 1.0 / rope_base ** (jnp.arange(0, width, 2, dtype=jnp.float32) / width)
    turned = jnp.arange(length, dtype=jnp.float32)[:, None] * inverse[None, :]
    return (jnp.cos(turned), jnp.sin(turned))


def attend_backward(arrived, rope_full):
    f32 = jnp.float32
    bf16 = jnp.bfloat16
    length = arrived.shape[0]
    local_heads = arrived.shape[1]
    width = PLAIN_HEAD_WIDTH + ROPE
    scale = width ** (-0.5)
    block = 512
    cosine, sine = angles(length, ROPE)
    neg = jnp.finfo(f32).min
    q_nope = arrived[:, :, :PLAIN_HEAD_WIDTH]
    q_rope = rotate(
        arrived[:, :, PLAIN_HEAD_WIDTH:width].astype(f32), cosine[:, None, :], sine[:, None, :]
    ).astype(bf16)
    key_nope = arrived[:, :, width : width + PLAIN_HEAD_WIDTH]
    values = arrived[:, :, width + PLAIN_HEAD_WIDTH : width + PLAIN_HEAD_WIDTH + VALUE_HEAD_WIDTH]
    d_out = arrived[:, :, width + PLAIN_HEAD_WIDTH + VALUE_HEAD_WIDTH :]
    k_rope = rotate(rope_full.astype(f32), cosine, sine).astype(bf16)
    dk_nope = jnp.zeros((length, local_heads, PLAIN_HEAD_WIDTH), f32)
    dk_rope = jnp.zeros((length, ROPE), f32)
    d_vals = jnp.zeros((length, local_heads, VALUE_HEAD_WIDTH), f32)
    dq_parts = []
    for begin in range(0, length, block):
        end = begin + block
        qn = q_nope[begin:end]
        qr = q_rope[begin:end]
        go = d_out[begin:end]
        scores = jnp.einsum("qhd,khd->hqk", qn, key_nope[:end], preferred_element_type=f32)
        scores = (
            scores + jnp.einsum("qhd,kd->hqk", qr, k_rope[:end], preferred_element_type=f32)
        ) * scale
        q_seg = jnp.arange(begin, end) // SPAN
        k_seg = jnp.arange(end) // SPAN
        allowed = k_seg[None, :] <= q_seg[:, None]
        scores = jnp.where(allowed[None], scores, neg)
        probs = jax.nn.softmax(scores, axis=-1)
        d_probs = jnp.einsum("qhd,khd->hqk", go, values[:end], preferred_element_type=f32)
        d_scores = probs * (d_probs - jnp.sum(probs * d_probs, axis=-1, keepdims=True))
        ds_b = d_scores.astype(bf16)
        p_b = probs.astype(bf16)
        dq_n = jnp.einsum("hqk,khd->qhd", ds_b, key_nope[:end], preferred_element_type=f32) * scale
        dq_r = jnp.einsum("hqk,kd->qhd", ds_b, k_rope[:end], preferred_element_type=f32) * scale
        dq_r = rotate(dq_r, cosine[begin:end, None, :], -sine[begin:end, None, :])
        dq_parts.append(jnp.concatenate([dq_n, dq_r], axis=-1).astype(bf16))
        dk_nope = dk_nope.at[:end].add(
            jnp.einsum("hqk,qhd->khd", ds_b, qn, preferred_element_type=f32) * scale
        )
        dk_rope = dk_rope.at[:end].add(
            jnp.einsum("hqk,qhd->kd", ds_b, qr, preferred_element_type=f32) * scale
        )
        d_vals = d_vals.at[:end].add(
            jnp.einsum("hqk,qhd->khd", p_b, go, preferred_element_type=f32)
        )
    query_part = jnp.concatenate(dq_parts, axis=0)
    grads = jnp.concatenate([query_part, dk_nope.astype(bf16), d_vals.astype(bf16)], axis=-1)
    return (grads, rotate(dk_rope, cosine, -sine))


def local(query, latent, rope_key, latent_norm_gain, key_up_matrix, value_up_matrix, out_grad):
    f32 = jnp.float32
    bf16 = jnp.bfloat16
    tokens = latent.shape[1]
    width = PLAIN_HEAD_WIDTH + ROPE
    head_cols = ATTENTION_HEADS * PLAIN_HEAD_WIDTH
    lat = latent[0].astype(f32)
    inv_rms = lax.rsqrt(jnp.mean(lat * lat, axis=-1, keepdims=True) + eps)
    normed = lat * inv_rms
    nlat = (normed * latent_norm_gain).astype(bf16)
    stacked = jnp.stack([key_up_matrix, value_up_matrix])
    whole = lax.all_gather(stacked, DP, axis=1, tiled=True)
    kv_tok = jnp.einsum("tc,gnc->tgn", nlat, whole, preferred_element_type=f32).astype(bf16)
    heads_query = query[0].reshape(tokens, ATTENTION_HEADS, width)
    key_nope = kv_tok[:, 0].reshape(tokens, ATTENTION_HEADS, PLAIN_HEAD_WIDTH)
    values = kv_tok[:, 1].reshape(tokens, ATTENTION_HEADS, VALUE_HEAD_WIDTH)
    d_out = out_grad[0].reshape(tokens, ATTENTION_HEADS, VALUE_HEAD_WIDTH)
    packed = jnp.concatenate([heads_query, key_nope, values, d_out], axis=2)
    arrived = lax.all_to_all(packed, SP, split_axis=1, concat_axis=0, tiled=True)
    rope_full = gather_directly(rope_key[0], SP, 0)
    grads_heads, rope_full_grad = attend_backward(arrived, rope_full)
    returned = lax.all_to_all(grads_heads, SP, split_axis=0, concat_axis=1, tiled=True)
    rope_grad = sent_and_summed(rope_full_grad, SP, 0)
    query_grad = returned[:, :, :width].reshape(tokens, ATTENTION_HEADS * width)
    key_cols = returned[:, :, width : width + PLAIN_HEAD_WIDTH].reshape(tokens, head_cols)
    value_cols = returned[:, :, width + PLAIN_HEAD_WIDTH :].reshape(tokens, head_cols)
    dkv = jnp.stack([key_cols, value_cols], axis=1)
    d_nlat = jnp.einsum("tgn,gnc->tc", dkv, whole, preferred_element_type=f32)
    latents_all = gather_all_axes(nlat[None], DP, 0)
    columns = lax.all_to_all(dkv[None], DP, split_axis=3, concat_axis=0, tiled=True)
    partial_value = jnp.einsum("stgr,stc->grc", columns, latents_all, preferred_element_type=f32)
    weight_grads = lax.psum(partial_value, SP)
    gain_grad = by_axis(jnp.sum(d_nlat * normed, axis=0), SP_DP)
    scaled = d_nlat * latent_norm_gain
    latent_grad = inv_rms * (scaled - normed * jnp.mean(scaled * normed, axis=-1, keepdims=True))
    return (
        query_grad[None],
        latent_grad[None],
        rope_grad[None],
        weight_grads[0],
        weight_grads[1],
        gain_grad,
    )


def solution(mesh):
    split = Mesh(mesh.devices.reshape(4, 4, 4, 2), ("sp_0", "sp_1", "dp_0", "dp_1"))
    in_specs = (
        P(DP, SP, None),
        P(DP, SP, None),
        P(DP, SP, None),
        P(),
        P(DP, None),
        P(DP, None),
        P(DP, SP, None),
    )
    out_specs = (P(DP, SP, None), P(DP, SP, None), P(DP, SP, None), P(DP, None), P(DP, None), P())
    return jax.shard_map(local, mesh=split, in_specs=in_specs, out_specs=out_specs, check_vma=False)
```

profile of v0, /device:TPU:0, one launch (start us, length us, event | category | flops | bytes accessed | tf_op | source)
XLA Modules:
  0.0 623.8 jit_solution(4799579515403184759)
XLA Ops:
  11.1 14.5 %all-gather.2 = bf16[4,96,1024]{2,1,0:T(8,128)(2,1)} all-gather(bf16[1,96,1024]{2,1,0:T(8,128)(2,1)S(1)} %get-tuple-element.261), channel_id=4, replica_groups=mesh['sp_0'=4,'sp_1'=4,'dp_0'=4,'dp_1'=2] {'dp_0'}, dimensions={0}, use_global_device_ids=true | all-gather | bytes 983040 | tf_op jit(solution)/shard_map/all_gather | solution.py:61
  26.4 8.6 %all-to-all-start.1 = ((bf16[16,192,32]{1,2,0:T(8,128)(2,1)}), bf16[16,192,32]{1,2,0:T(8,128)(2,1)S(1)}, u32[]{:S(2)}, u32[]{:S(2)}) async-start(bf16[16,192,32]{1,2,0:T(8,128)(2,1)} %broadcast_in_dim.80), calls=%async_computation.1 | async-start | bytes 524288 | tf_op jit(solution)/shard_map/all_to_all | solution.py:25
  45.3 17.1 %all-gather.8.cloned.1.call-done = bf16[2,2048,1024]{2,1,0:T(8,128)(2,1)} async-done(((bf16[2,256,1024]{2,1,0:T(8,128)(2,1)}), bf16[2,2048,1024]{2,1,0:T(8,128)(2,1)}) %all-gather.8.cloned.1.call-update) | async-done | bytes 8388624 | tf_op jit(solution)/shard_map/all_gather | solution.py:168
  88.3 7.2 %all-to-all-start = ((bf16[192,32,288]{2,0,1:T(8,128)(2,1)}), bf16[192,32,288]{2,0,1:T(8,128)(2,1)}, u32[]{:S(2)}, u32[]{:S(2)}) async-start(bf16[192,32,288]{2,0,1:T(8,128)(2,1)} %copy.83), calls=%async_computation | async-start | bytes 9437184 | tf_op jit(solution)/shard_map/all_to_all | solution.py:175
  105.9 61.1 %all-to-all-done = bf16[192,32,288]{2,0,1:T(8,128)(2,1)} async-done(((bf16[192,32,288]{2,0,1:T(8,128)(2,1)}), bf16[192,32,288]{2,0,1:T(8,128)(2,1)}, u32[]{:S(2)}, u32[]{:S(2)}) %all-to-all-start) | async-done | bytes 3538976 | tf_op jit(solution)/shard_map/all_to_all | solution.py:175
  167.0 8.3 %copy.84 = bf16[16,192,2,288]{1,0,3,2:T(8,128)(2,1)} copy(bf16[16,192,2,288]{3,1,2,0:T(8,128)(2,1)} %bitcast.8) | data formatting | bytes 7077888 | tf_op jit(solution)/shard_map/all_to_all | solution.py:175
  175.3 7.2 %all_to_all.48 = bf16[3072,2,288]{0,2,1:T(8,128)(2,1)S(1)} reshape(bf16[16,192,2,288]{1,0,3,2:T(8,128)(2,1)} %copy.84) | data formatting | bytes 7077888 | tf_op jit(solution)/shard_map/all_to_all | solution.py:175
  225.4 7.3 %fusion.297 = (f32[2,512]{1,0:T(2,128)S(1)}, f32[2,512,2048]{2,1,0:T(8,128)S(1)}) fusion(f32[2,512,2048]{2,1,0:T(8,128)} %fusion.11), kind=kOutput, calls=%fused_computation.433 | output fusion | flops 4196351 | bytes 16781312 | tf_op jit(solution)/shard_map/sub | solution.py:134
  282.7 14.9 %fusion.299 = (f32[2,512]{1,0:T(2,128)S(1)}, f32[2,512,3072]{2,1,0:T(8,128)}) fusion(f32[2,512,3072]{2,1,0:T(8,128)} %fusion.7), kind=kOutput, calls=%fused_computation.435 | output fusion | flops 6294527 | bytes 25169920 | tf_op jit(solution)/shard_map/sub | solution.py:134
  297.6 11.8 %multiply_reduce_fusion = (f32[2,512]{1,0:T(2,128)S(1)}, f32[2,512,3072]{2,1,0:T(8,128)}) fusion(f32[2,512,3072]{2,1,0:T(8,128)} %get-tuple-element.301, f32[2,512]{1,0:T(2,128)S(1)} %get-tuple-element.300, bf16[3072,2,288]{0,2,1:T(8,128)(2,1)} %copy-done.6), kind=kOutput, calls=%fused_computation.10 | convolution fusion | flops 412089344 | bytes 26091520 | tf_op jit(solution)/shard_map/qhd,khd->hqk/dot_general | solution.py:135
  309.5 7.4 %multiply_convert_fusion = bf16[2,512,3072]{2,1,0:T(8,128)(2,1)S(1)} fusion(f32[2,512,3072]{2,1,0:T(8,128)} %get-tuple-element.313, f32[2,512]{1,0:T(2,128)S(1)} %get-tuple-element.312, f32[2,512,3072]{2,1,0:T(8,128)S(1)} %bitcast.325, f32[2,512]{1,0:T(2,128)S(1)} %get-tuple-element.300), kind=kLoop, calls=%fused_computation.9 | loop fusion | flops 12582912 | bytes 31465472 | tf_op jit(solution)/shard_map/convert_element_type | solution.py:137
  325.9 6.4 %fusion.99 = f32[3072,2,64]{0,2,1:T(8,128)} fusion(f32[3072,2,64]{0,2,1:T(8,128)} %scatter-add.59, f32[512,2,64]{0,2,1:T(8,128)} %convolution_bitcast_fusion.5, bf16[3072,2,288]{0,2,1:T(8,128)(2,1)} %copy-done.6, f32[2,512]{1,0:T(2,128)S(1)} %get-tuple-element.292, f32[2,512,1024]{2,1,0:T(8,128)} %copy-done.19), kind=kOutput, calls=%fused_computation.121 | convolution fusion | flops 137496576 | bytes 9310208 | tf_op jit(solution)/shard_map/hqk,qhd->khd/dot_general | solution.py:150
  335.3 8.0 %fusion.77 = f32[3072,2,64]{0,2,1:T(8,128)} fusion(f32[3072,2,64]{0,2,1:T(8,128)} %fusion.99, bf16[3072,2,288]{0,2,1:T(8,128)(2,1)} %copy-done.6, f32[2,512]{1,0:T(2,128)S(1)} %get-tuple-element.294, f32[2,512,1536]{2,1,0:T(8,128)} %copy-done.16), kind=kOutput, calls=%fused_computation.91 | convolution fusion | flops 206244352 | bytes 14290944 | tf_op jit(solution)/shard_map/hqk,qhd->khd/dot_general | solution.py:150
  346.1 9.4 %fusion.65 = f32[3072,2,64]{0,2,1:T(8,128)} fusion(f32[3072,2,64]{0,2,1:T(8,128)} %fusion.77, bf16[3072,2,288]{0,2,1:T(8,128)(2,1)} %copy-done.6, f32[2,512]{1,0:T(2,128)S(1)} %get-tuple-element.296, f32[2,512,2048]{2,1,0:T(8,128)} %fusion.11), kind=kOutput, calls=%fused_computation.84 | convolution fusion | flops 274992128 | bytes 19009536 | tf_op jit(solution)/shard_map/hqk,qhd->khd/dot_general | solution.py:150
  359.9 11.3 %fusion.31 = f32[3072,2,64]{0,2,1:T(8,128)} fusion(f32[3072,2,64]{0,2,1:T(8,128)} %fusion.65, bf16[3072,2,288]{0,2,1:T(8,128)(2,1)} %copy-done.6, f32[2,512]{1,0:T(2,128)S(1)} %get-tuple-element.298, f32[2,512,2560]{2,1,0:T(8,128)} %copy-done.3), kind=kOutput, calls=%fused_computation.52 | convolution fusion | flops 343739904 | bytes 23728128 | tf_op jit(solution)/shard_map/hqk,qhd->khd/dot_general | solution.py:150
  376.3 12.7 %fusion.42 = bf16[3072,2,64]{0,2,1:T(8,128)(2,1)} fusion(f32[3072,2,64]{0,2,1:T(8,128)} %fusion.31, bf16[3072,2,288]{0,2,1:T(8,128)(2,1)} %copy-done.6, f32[2,512]{1,0:T(2,128)S(1)} %copy-done.72, f32[2,512,3072]{2,1,0:T(8,128)} %fusion.7), kind=kOutput, calls=%fused_computation.58 | convolution fusion | flops 412880896 | bytes 27660288 | tf_op jit(solution)/shard_map/hqk,qhd->khd/dot_general | solution.py:150
  396.7 8.6 %copy.95 = bf16[3072,2,224]{2,1,0:T(2,128)(2,1)} copy(bf16[3072,2,224]{0,2,1:T(8,128)(2,1)} %pad_maximum_fusion.1) | data formatting | bytes 5505024 | tf_op jit(solution)/shard_map/concatenate | solution.py:153
  424.4 31.9 %all-to-all-done.2 = bf16[3072,2,224]{2,1,0:T(2,128)(2,1)} async-done(((bf16[3072,2,224]{2,1,0:T(2,128)(2,1)}), bf16[3072,2,224]{2,1,0:T(2,128)(2,1)}, u32[]{:S(2)}, u32[]{:S(2)}) %all-to-all-start.2) | async-done | bytes 2752544 | tf_op jit(solution)/shard_map/all_to_all | solution.py:178
  498.8 14.3 %all-to-all-done.4 = bf16[1,192,2,2048]{1,2,0,3:T(2,128)(2,1)} async-done(((bf16[1,192,2,2048]{1,2,0,3:T(2,128)(2,1)}), bf16[1,192,2,2048]{1,2,0,3:T(2,128)(2,1)}, u32[]{:S(2)}, u32[]{:S(2)}) %all-to-all-start.4) | async-done | bytes 1572896 | tf_op jit(solution)/shard_map/all_to_all | solution.py:186
  524.9 19.4 %all_to_all.64 = f32[16,192,32]{1,2,0:T(8,128)} all-to-all(f32[16,192,32]{1,2,0:T(8,128)S(1)} %copy.104), channel_id=1, replica_groups=mesh['sp_0'=4,'sp_1'=4,'dp_0'=4,'dp_1'=2] {'sp_0','sp_1'}, dimensions={0} | all-to-all | bytes 786432 | tf_op jit(solution)/shard_map/all_to_all | solution.py:49
  555.6 8.8 %psum.36 = f32[1024]{0:T(1024)S(1)} all-reduce(f32[1024]{0:T(1024)S(1)} %get-tuple-element.246), channel_id=1, replica_groups=mesh['sp_0'=4,'sp_1'=4,'dp_0'=4,'dp_1'=2] {'sp_0'}, use_global_device_ids=true, to_apply=%region_23.24 | all-reduce | flops 1024 | bytes 8192 | tf_op jit(solution)/shard_map/psum | solution.py:81
  564.4 8.7 %psum.37 = f32[1024]{0:T(1024)S(1)} all-reduce(f32[1024]{0:T(1024)S(1)} %psum.36), channel_id=1, replica_groups=mesh['sp_0'=4,'sp_1'=4,'dp_0'=4,'dp_1'=2] {'sp_1'}, use_global_device_ids=true, to_apply=%region_24.25 | all-reduce | flops 1024 | bytes 8192 | tf_op jit(solution)/shard_map/psum | solution.py:81
  573.2 9.4 %psum.38 = f32[1024]{0:T(1024)S(1)} all-reduce(f32[1024]{0:T(1024)S(1)} %psum.37), channel_id=1, replica_groups=mesh['sp_0'=4,'sp_1'=4,'dp_0'=4,'dp_1'=2] {'dp_0'}, use_global_device_ids=true, to_apply=%region_25.26 | all-reduce | flops 1024 | bytes 8192 | tf_op jit(solution)/shard_map/psum | solution.py:81
  586.8 27.2 %all-reduce.5.cloned.1.call-done = f32[2,256,1024]{2,1,0:T(8,128)} async-done(((f32[2,256,1024]{2,1,0:T(8,128)}), f32[2,256,1024]{2,1,0:T(8,128)}) %all-reduce.5.cloned.1.call-update) | async-done | bytes 2097168 | tf_op jit(solution)/shard_map/psum | solution.py:188
  (322 shorter events, 266.9 us)
Async XLA Ops:
  7.2 18.4 %copy-start.73 = (bf16[1,192,32]{1,2,0:T(8,128)(2,1)S(1)}, bf16[1,192,32]{1,2,0:T(8,128)(2,1)}, u32[]{:S(2)}) copy-start(bf16[1,192,32]{1,2,0:T(8,128)(2,1)} %param.51) | copy-start | bytes 36868
  7.2 55.2 %all-gather.8.cloned.1.call-start = ((), (), s32[]{:S(2)}) async-start(), calls=%async_computation.5 | async-start | bytes 9437184 | tf_op jit(solution)/shard_map/all_gather | solution.py:168
  9.6 28.7 %copy-start.41 = (bf16[1,192,2048]{2,1,0:T(8,128)(2,1)S(1)}, bf16[1,192,2048]{2,1,0:T(8,128)(2,1)}, u32[]{:S(2)}) copy-start(bf16[1,192,2048]{2,1,0:T(8,128)(2,1)} %param.55) | copy-start | bytes 2359300
  9.6 400.9 %all-gather.12.cloned.1.call-start = ((), (), s32[]{:S(2)}) async-start(), calls=%async_computation.8 | async-start | bytes 2359296 | tf_op jit(solution)/shard_map/all_gather | solution.py:61
  10.9 51.5 %copy-start.74 = (f32[192]{0:T(256)}, f32[192]{0:T(256)S(1)}, u32[]{:S(2)}) copy-start(f32[192]{0:T(256)S(1)} %add_rsqrt_fusion) | copy-start | bytes 2308
  26.4 62.0 %all-to-all-start.1 = ((bf16[16,192,32]{1,2,0:T(8,128)(2,1)}), bf16[16,192,32]{1,2,0:T(8,128)(2,1)S(1)}, u32[]{:S(2)}, u32[]{:S(2)}) async-start(bf16[16,192,32]{1,2,0:T(8,128)(2,1)} %broadcast_in_dim.80), calls=%async_computation.1 | async-start | bytes 524288 | tf_op jit(solution)/shard_map/all_to_all | solution.py:25
  35.0 383.5 %all-gather.10.cloned.1.call-start = ((), (), s32[]{:S(2)}) async-start(), calls=%async_computation.7 | async-start | bytes 1966080 | tf_op jit(solution)/shard_map/all_gather | solution.py:61
  88.3 78.7 %all-to-all-start = ((bf16[192,32,288]{2,0,1:T(8,128)(2,1)}), bf16[192,32,288]{2,0,1:T(8,128)(2,1)}, u32[]{:S(2)}, u32[]{:S(2)}) async-start(bf16[192,32,288]{2,0,1:T(8,128)(2,1)} %copy.83), calls=%async_computation | async-start | bytes 9437184 | tf_op jit(solution)/shard_map/all_to_all | solution.py:175
  95.6 8.9 %copy-start.76 = (f32[16]{0:T(128)}, f32[16]{0:T(128)S(1)}, u32[]{:S(2)}) copy-start(f32[16]{0:T(128)S(1)} %negate_power_fusion) | copy-start | bytes 196
  182.5 30.2 %copy-start.6 = (bf16[3072,2,288]{0,2,1:T(8,128)(2,1)}, bf16[3072,2,288]{0,2,1:T(8,128)(2,1)S(1)}, u32[]{:S(2)}) copy-start(bf16[3072,2,288]{0,2,1:T(8,128)(2,1)S(1)} %all_to_all.48) | copy-start | bytes 10616836
  258.5 7.3 %slice-start.7 = ((s8[10485760]{0:T(1024)(128)(4,1)}), s8[2097152]{0:T(1024)(128)(4,1)S(1)}, s32[]{:S(2)}) async-start(s8[10485760]{0:T(1024)(128)(4,1)} %bitcast.326), calls=%async_computation.16 | async-start | bytes 4194304
  297.6 11.8 %copy-start.71 = (f32[2,512]{1,0:T(2,128)}, f32[2,512]{1,0:T(2,128)S(1)}, u32[]{:S(2)}) copy-start(f32[2,512]{1,0:T(2,128)S(1)} %get-tuple-element.300) | copy-start | bytes 12292
  297.6 11.8 %slice-start.2 = ((s8[12582912]{0:T(1024)(128)(4,1)}), s8[4194304]{0:T(1024)(128)(4,1)S(1)}, s32[]{:S(2)}) async-start(s8[12582912]{0:T(1024)(128)(4,1)} %bitcast.324), calls=%async_computation.11 | async-start | bytes 8388608
  297.6 11.8 %slice-start.3 = ((s8[12582912]{0:T(1024)(128)(4,1)}), s8[4194304]{0:T(1024)(128)(4,1)S(1)}, s32[]{:S(2)}) async-start(s8[12582912]{0:T(1024)(128)(4,1)} %bitcast.324), calls=%async_computation.12 | async-start | bytes 8388608
  297.6 11.8 %slice-start.4 = ((s8[12582912]{0:T(1024)(128)(4,1)}), s8[4194304]{0:T(1024)(128)(4,1)S(1)}, s32[]{:S(2)}) async-start(s8[12582912]{0:T(1024)(128)(4,1)} %bitcast.324), calls=%async_computation.13 | async-start | bytes 8388608
  405.3 50.9 %all-to-all-start.2 = ((bf16[3072,2,224]{2,1,0:T(2,128)(2,1)}), bf16[3072,2,224]{2,1,0:T(2,128)(2,1)}, u32[]{:S(2)}, u32[]{:S(2)}) async-start(bf16[3072,2,224]{2,1,0:T(2,128)(2,1)} %copy.95), calls=%async_computation.2 | async-start | bytes 6291456 | tf_op jit(solution)/shard_map/all_to_all | solution.py:178
  414.7 7.3 %copy-start.10 = (bf16[3072,2,16]{0,2,1:T(8,128)(2,1)S(1)}, bf16[3072,2,16]{0,2,1:T(8,128)(2,1)}, u32[]{:S(2)}) copy-start(bf16[3072,2,16]{0,2,1:T(8,128)(2,1)} %copy-done.8) | copy-start | bytes 589828
  414.7 7.3 %copy-start.13 = (bf16[3072,2,16]{0,2,1:T(8,128)(2,1)S(1)}, bf16[3072,2,16]{0,2,1:T(8,128)(2,1)}, u32[]{:S(2)}) copy-start(bf16[3072,2,16]{0,2,1:T(8,128)(2,1)} %copy-done.11) | copy-start | bytes 589828
  481.6 31.5 %all-to-all-start.4 = ((bf16[1,192,2,2048]{1,2,0,3:T(2,128)(2,1)}), bf16[1,192,2,2048]{1,2,0,3:T(2,128)(2,1)}, u32[]{:S(2)}, u32[]{:S(2)}) async-start(bf16[1,192,2,2048]{1,2,0,3:T(2,128)(2,1)} %copy.105), calls=%async_computation.4 | async-start | bytes 4194304 | tf_op jit(solution)/shard_map/all_to_all | solution.py:186
  485.9 128.1 %all-reduce.5.cloned.1.call-start = ((), (), s32[]{:S(2)}) async-start(), calls=%async_computation.6 | async-start | bytes 4194304 | tf_op jit(solution)/shard_map/psum | solution.py:188
  486.0 10.6 %slice-start = ((s8[6291456]{0:T(1024)(128)(4,1)}), s8[4194304]{0:T(1024)(128)(4,1)S(1)}, s32[]{:S(2)}) async-start(s8[6291456]{0:T(1024)(128)(4,1)} %bitcast.322), calls=%async_computation.9 | async-start | bytes 8388608
  488.4 8.2 %slice-start.1 = ((s8[6291456]{0:T(1024)(128)(4,1)}), s8[2097152]{0:T(1024)(128)(4,1)S(1)}, s32[]{:S(2)}) async-start(s8[6291456]{0:T(1024)(128)(4,1)} %bitcast.322), calls=%async_computation.10 | async-start | bytes 4194304
  498.8 18.2 %copy-start.39 = (bf16[8,1,96,1024]{3,0,2,1:T(8,128)(2,1)S(1)}, bf16[8,1,96,1024]{3,0,2,1:T(8,128)(2,1)}, u32[]{:S(2)}) copy-start(bf16[8,1,96,1024]{3,0,2,1:T(8,128)(2,1)} %reshape.969) | copy-start | bytes 4718596
  521.6 24.4 %copy-start.18 = (bf16[192,16,2,224]{3,0,2,1:T(8,128)(2,1)S(1)}, bf16[192,16,2,224]{3,0,2,1:T(8,128)(2,1)}, u32[]{:S(2)}) copy-start(bf16[192,16,2,224]{3,0,2,1:T(8,128)(2,1)} %copy-done.17) | copy-start | bytes 8257540
  (70 other events, 259.9 us)
Sparse Core Ops, SparseCore 0:
  10.3 52.0 all-gather.7
  64.1 12.6 all-gather.11
  78.4 27.7 all-gather.9
  521.7 92.2 all-reduce.4
where the time goes:
time: 634 us; the launch traced here: 624 us
  matrix products  182 us (29%)
  waiting for transfers between devices  152 us (24%)
  local copies, waits for them, and re-layouts  105 us (17%)
  other arithmetic  78.7 us (12%)
  blocking collectives  66.1 us (10%)
  starting transfers between devices  25.5 us (4%)
  between operations  15.3 us (2%)
    all_to_all x1, waiting for transfers between devices, local(): lax.all_to_all(packed, SP, split_axis=1, concat_axis=0, tiled=True)  61.1 us
    dot_general x6, matrix products, attend_backward(): jnp.einsum('hqk,qhd->khd', p_b, go, preferred_element_type=f32)  51.5 us
    sub x6, other arithmetic, attend_backward(): probs = jax.nn.softmax(scores, axis=-1)  32.6 us
    all_to_all x1, waiting for transfers between devices, local(): lax.all_to_all(grads_heads, SP, split_axis=0, concat_axis=1, tiled=True)  31.9 us
    psum x4, blocking collectives, by_axis(): return functools.reduce(lax.psum, axes, value)  30 us
    psum x1, waiting for transfers between devices, local(): weight_grads = lax.psum(partial_value, SP)  27.2 us
    dot_general x6, matrix products, attend_backward(): jnp.einsum('qhd,khd->hqk', go, values[:end], preferred_element_type=f32)  27.1 us
    dot_general x6, matrix products, attend_backward(): jnp.einsum('hqk,qhd->khd', ds_b, qn, preferred_element_type=f32) * scale  21.1 us
  transfers between devices with their start and end apart: 8, of which 5 were waited for; matrix products, arithmetic and copies ran while one was open for 50% of the time, Pallas kernels for 0%

commit v1 on v0

v1 whole, which is shorter than its diff:
```python
import functools

import jax
import jax.numpy as jnp
import numpy as np
from jax import lax
from jax.experimental import pallas as pl
from jax.experimental.pallas import tpu as pltpu
from jax.sharding import Mesh
from jax.sharding import PartitionSpec as P

ATTENTION_HEADS = 32
PLAIN_HEAD_WIDTH = 64
ROPE = 32
VALUE_HEAD_WIDTH = 64
SPAN = 64
LATENT = 1024
LENGTH = 3072
TOKENS = 192
DP = ("dp_0", "dp_1")
SP = ("sp_0", "sp_1")
SP_DP = ("sp_0", "sp_1", "dp_0", "dp_1")
SP_SIZE = 16
DP_SIZE = 8
BLOCK = 512
SCALE = (PLAIN_HEAD_WIDTH + ROPE) ** (-0.5)
LOG2E = 1.4426950408889634

eps = 1e-06
rope_base = 10000.0
f32 = jnp.float32
bf16 = jnp.bfloat16


def pack_tables():
    first = np.zeros((384 + 256 + 128, 512), np.float32)
    second = np.zeros((384 + 256 + 128, 256), np.float32)
    for t in range(2):
        q, d, r = 192 * t, 384 + 128 * t, 640
        for c in range(64):
            first[q + c, 256 * t + c] = 1
            first[d + c, 256 * t + 64 + c] = 1
            second[q + 96 + c, 128 * t + c] = 1
            second[d + 64 + c, 128 * t + 64 + c] = 1
        for c in range(32):
            first[q + 64 + c, 256 * t + 128 + c] = 1
            first[q + 160 + c, 256 * t + 160 + c] = 1
            first[r + c, 256 * t + 192 + c] = 1
    return first, second


def unpack_table():
    place = np.zeros((512, 384), np.float32)
    for t in range(2):
        for h in range(2):
            for c in range(96):
                place[256 * t + 128 * h + c, 192 * t + 96 * h + c] = 1
    return place


def rope_tables():
    swap = np.zeros((128, 128), np.float32)
    for g in range(3):
        for c in range(16):
            swap[32 * g + 16 + c, 32 * g + c] = -1
            swap[32 * g + c, 32 * g + 16 + c] = 1
    spread = np.zeros((128, 384), np.float32)
    for c in range(32):
        spread[c, c] = 1
        spread[32 + c, 128 + c] = 1
        spread[64 + c, 256 + c] = 1
    for c in range(16):
        spread[64 + 16 + c, 256 + 32 + c] = 1
        spread[64 + c, 256 + 32 + 16 + c] = -1
    return swap, spread


def pack_kernel(query, d_out, rope, first, second, out0, out1):
    both = jnp.concatenate([query[...], d_out[...], rope[...]], axis=1)
    one = jnp.dot(both, first[...], preferred_element_type=f32).astype(bf16)
    two = jnp.dot(both, second[...], preferred_element_type=f32).astype(bf16)
    for t in range(2):
        out0[t] = one[:, 256 * t : 256 * t + 256]
        out1[t] = two[:, 128 * t : 128 * t + 128]


def pack(query, d_out, rope):
    first, second = pack_tables()
    whole = lambda shape: pl.BlockSpec(shape, lambda j: (0, 0))
    return pl.pallas_call(
        pack_kernel,
        grid=(8,),
        in_specs=[
            pl.BlockSpec((TOKENS, 384), lambda j: (0, j)),
            pl.BlockSpec((TOKENS, 256), lambda j: (0, j)),
            whole((TOKENS, 128)),
            whole((768, 512)),
            whole((768, 256)),
        ],
        out_specs=[
            pl.BlockSpec((2, TOKENS, 256), lambda j: (j, 0, 0)),
            pl.BlockSpec((2, TOKENS, 128), lambda j: (j, 0, 0)),
        ],
        out_shape=[
            jax.ShapeDtypeStruct((SP_SIZE, TOKENS, 256), bf16),
            jax.ShapeDtypeStruct((SP_SIZE, TOKENS, 128), bf16),
        ],
        cost_estimate=pl.CostEstimate(
            flops=16 * 192 * 768 * 768, bytes_accessed=5_000_000, transcendentals=0
        ),
        name="pack",
    )(query, d_out, rope, jnp.asarray(first, bf16), jnp.asarray(second, bf16))


def dot_t(a, b):
    return lax.dot_general(a, b, (((1,), (1,)), ((), ())), preferred_element_type=f32)


def lanes(x, combine):
    parts = [x[:, k : k + 128] for k in range(0, x.shape[1], 128)]
    return functools.reduce(combine, parts)


def attention_kernel(a_ref, q2_ref, kv_ref, k2_ref, tab_ref, out_ref, s_ref, dp_ref, m_ref, l_ref, d_ref, dq_ref, acc_ref):
    step = pl.program_id(0)
    count = LENGTH // BLOCK
    i = count - 1 - step

    @pl.when(step == 0)
    def _():
        acc_ref[...] = jnp.zeros_like(acc_ref)

    rows = pl.ds(pl.multiple_of(i * BLOCK, BLOCK), BLOCK)
    a = a_ref[rows, :]
    q2 = q2_ref[rows, :]
    lane = lax.broadcasted_iota(jnp.int32, (BLOCK, 128), 1)
    nope = jnp.where(lane < 64, a, jnp.zeros_like(a))
    cot = jnp.where(lane < 64, jnp.zeros_like(a), a)
    query = jnp.concatenate([nope, q2], axis=1)
    a_t = a.T
    q2_t = q2.T
    left_k = jnp.concatenate([q2_t[0:32], a_t[0:64]], axis=0)
    left_v = a_t[64:128]

    def tile(j):
        return pl.ds(pl.multiple_of(j * BLOCK, BLOCK), BLOCK)

    def key(j):
        return jnp.concatenate([kv_ref[tile(j), :], k2_ref[tile(j), :]], axis=1)

    m_ref[...] = jnp.full_like(m_ref, -1e30)
    l_ref[...] = jnp.zeros_like(l_ref)
    d_ref[...] = jnp.zeros_like(d_ref)
    dq_ref[...] = jnp.zeros_like(dq_ref)

    def scores(j, masked):
        s = dot_t(query, key(j))
        if masked:
            r = lax.broadcasted_iota(jnp.int32, (BLOCK, BLOCK), 0) // SPAN
            c = lax.broadcasted_iota(jnp.int32, (BLOCK, BLOCK), 1) // SPAN
            s = jnp.where(c <= r, s, -1e30)
        s_ref[:, tile(j)] = s
        m_ref[...] = jnp.maximum(m_ref[...], lanes(s, jnp.maximum))

    @pl.loop(0, i)
    def _(j):
        scores(j, False)

    scores(i, True)
    m = jnp.max(m_ref[...], axis=1, keepdims=True)

    def weights(j):
        dp = dot_t(cot, kv_ref[tile(j), :])
        e = jnp.exp2((s_ref[:, tile(j)] - m) * (SCALE * LOG2E))
        l_ref[...] += lanes(e, jnp.add)
        d_ref[...] += lanes(e * dp, jnp.add)
        s_ref[:, tile(j)] = e
        dp_ref[:, tile(j)] = dp

    @pl.loop(0, i + 1)
    def _(j):
        weights(j)

    inverse = 1.0 / jnp.sum(l_ref[...], axis=1, keepdims=True)
    delta = jnp.sum(d_ref[...], axis=1, keepdims=True) * inverse

    @pl.loop(0, i + 1)
    def _(j):
        p = s_ref[:, tile(j)] * inverse
        ds = (p * (dp_ref[:, tile(j)] - delta)).astype(bf16)
        dq_ref[...] += jnp.dot(ds, key(j), preferred_element_type=f32)
        acc_ref[0:96, tile(j)] += jnp.dot(left_k, ds, preferred_element_type=f32)
        acc_ref[96:160, tile(j)] += jnp.dot(left_v, p.astype(bf16), preferred_element_type=f32)

    turned = dq_ref[:, 128:256] * tab_ref[...]
    turned = turned + pltpu.roll(turned, 96, 1)
    dq = jnp.where(lane < 64, dq_ref[:, 0:128], pltpu.roll(turned, 64, 1)) * SCALE
    done = acc_ref[:, rows]
    k_rope = done[0:32] * SCALE
    k_nope = done[32:96] * SCALE
    low = jnp.concatenate([jnp.zeros((96, BLOCK), f32), k_rope], axis=0).T
    out_ref[:, 0:128] = jnp.where(lane < 96, dq, low).astype(bf16)
    out_ref[:, 128:256] = jnp.concatenate([k_nope, done[96:160]], axis=0).T.astype(bf16)


def attention(a, q2, kv, k2, table):
    count = LENGTH // BLOCK
    whole = pl.BlockSpec((LENGTH, 128), lambda i: (0, 0))
    return pl.pallas_call(
        attention_kernel,
        grid=(count,),
        in_specs=[whole] * 4 + [pl.BlockSpec((BLOCK, 128), lambda i: (count - 1 - i, 0))],
        out_specs=pl.BlockSpec((BLOCK, 256), lambda i: (count - 1 - i, 0)),
        out_shape=jax.ShapeDtypeStruct((LENGTH, 256), bf16),
        scratch_shapes=[
            pltpu.VMEM((BLOCK, LENGTH), f32),
            pltpu.VMEM((BLOCK, LENGTH), f32),
            pltpu.VMEM((BLOCK, 128), f32),
            pltpu.VMEM((BLOCK, 128), f32),
            pltpu.VMEM((BLOCK, 128), f32),
            pltpu.VMEM((BLOCK, 256), f32),
            pltpu.VMEM((160, LENGTH), f32),
        ],
        compiler_params=pltpu.CompilerParams(
            dimension_semantics=("arbitrary",), vmem_limit_bytes=48 * 1024 * 1024
        ),
        cost_estimate=pl.CostEstimate(
            flops=12_000_000_000, bytes_accessed=8_000_000, transcendentals=5_000_000
        ),
        name="attention",
    )(a, q2, kv, k2, table)


def finish_kernel(ret0, ret1, w, place, latent, gain, query_grad, latent_grad, rope_sum, acc):
    step = pl.program_id(0)

    @pl.when(step == 0)
    def _():
        acc[...] = jnp.zeros_like(acc)
        rope_sum[...] = jnp.zeros_like(rope_sum)

    left = [ret[t, :, 0:128] for t in range(2) for ret in (ret0, ret1)]
    query_grad[...] = jnp.dot(
        jnp.concatenate(left, axis=1), place[...], preferred_element_type=f32
    ).astype(bf16)
    rope_sum[...] += sum(x.astype(f32) for x in left)
    total = acc[...]
    for t in range(2):
        right = jnp.concatenate([ret0[t, :, 128:256], ret1[t, :, 128:256]], axis=1)
        total += jnp.dot(right, w[t], preferred_element_type=f32)
    acc[...] = total

    @pl.when(step == pl.num_programs(0) - 1)
    def _():
        lat = latent[...].astype(f32)
        inverse = lax.rsqrt(jnp.mean(lat * lat, axis=1, keepdims=True) + eps)
        normed = lat * inverse
        scaled = acc[...] * gain[...]
        latent_grad[...] = inverse * (
            scaled - normed * jnp.mean(scaled * normed, axis=1, keepdims=True)
        )


def finish(ret0, ret1, w, latent, gain):
    fixed = lambda shape: pl.BlockSpec(shape, lambda j: (0,) * len(shape))
    return pl.pallas_call(
        finish_kernel,
        grid=(8,),
        in_specs=[
            pl.BlockSpec((2, TOKENS, 256), lambda j: (j, 0, 0)),
            pl.BlockSpec((2, TOKENS, 256), lambda j: (j, 0, 0)),
            pl.BlockSpec((2, 256, LATENT), lambda j: (j, 0, 0)),
            fixed((512, 384)),
            fixed((TOKENS, LATENT)),
            fixed((1, LATENT)),
        ],
        out_specs=[
            pl.BlockSpec((TOKENS, 384), lambda j: (0, j)),
            fixed((TOKENS, LATENT)),
            fixed((TOKENS, 128)),
        ],
        out_shape=[
            jax.ShapeDtypeStruct((TOKENS, 3072), bf16),
            jax.ShapeDtypeStruct((TOKENS, LATENT), f32),
            jax.ShapeDtypeStruct((TOKENS, 128), f32),
        ],
        scratch_shapes=[pltpu.VMEM((TOKENS, LATENT), f32)],
        compiler_params=pltpu.CompilerParams(dimension_semantics=("arbitrary",)),
        cost_estimate=pl.CostEstimate(
            flops=4_000_000_000, bytes_accessed=14_000_000, transcendentals=0
        ),
        name="finish",
    )(ret0, ret1, w, jnp.asarray(unpack_table(), bf16), latent, gain)


def rotate(values, cosine, sine):
    half = values.shape[-1] // 2
    first = values[..., :half]
    second = values[..., half:]
    return jnp.concatenate(
        [first * cosine - second * sine, second * cosine + first * sine], axis=-1
    )


def inverse_frequency(index):
    return 1.0 / rope_base ** (2.0 * index.astype(f32) / ROPE)


def to_heads():
    pairs = []
    for i in range(DP_SIZE):
        for n in range(DP_SIZE):
            for b in range(2):
                pairs.append(((8 * b + n) * DP_SIZE + i, (2 * i + b) * DP_SIZE + n))
    return pairs


def exchange(value):
    return lax.all_to_all(value, SP, split_axis=0, concat_axis=0, tiled=True)


def local(query, latent, rope_key, latent_norm_gain, key_up_matrix, value_up_matrix, out_grad):
    lat = latent[0].astype(f32)
    inv_rms = lax.rsqrt(jnp.mean(lat * lat, axis=-1, keepdims=True) + eps)
    nlat = (lat * inv_rms * latent_norm_gain).astype(bf16)
    nlat_full = lax.all_gather(nlat, SP, axis=0, tiled=True)

    shard = jnp.stack(
        [key_up_matrix.reshape(2, 2, 64, LATENT), value_up_matrix.reshape(2, 2, 64, LATENT)],
        axis=2,
    ).reshape(2, 256, LATENT)
    spot = lax.axis_index(SP)
    half = lax.dynamic_index_in_dim(shard, spot // 8, 0, keepdims=False)
    w_own = lax.ppermute(half, SP_DP, to_heads())

    rope_wide = jnp.pad(rope_key[0], ((0, 0), (0, 96)))
    sent0, sent1 = pack(query[0], out_grad[0], rope_wide)
    got0 = exchange(sent0).reshape(LENGTH, 256)

    column = jnp.arange(128)
    turned = jnp.arange(LENGTH, dtype=f32)[:, None] * inverse_frequency(column % 16)[None, :]
    cosine = jnp.cos(turned)
    sine = jnp.sin(turned)
    table = jnp.where(column < 32, cosine, jnp.where(column < 64, sine, 0.0))
    swap, spread = rope_tables()

    raw = got0[:, 128:256]
    swapped = jnp.dot(raw, jnp.asarray(swap, bf16), preferred_element_type=f32)
    rotated = (raw.astype(f32) * cosine + swapped * sine).astype(bf16)
    apart = jnp.dot(rotated, jnp.asarray(spread, bf16), preferred_element_type=f32).astype(bf16)
    q2_0, q2_1, k2 = apart[:, 0:128], apart[:, 128:256], apart[:, 256:384]

    kv = lax.dot_general(
        nlat_full, w_own, (((1,), (1,)), ((), ())), preferred_element_type=f32
    ).astype(bf16)

    shard_later, _ = lax.optimization_barrier((shard, nlat_full))
    w_whole = lax.all_gather(shard_later, DP, axis=0, tiled=True)

    grads0 = attention(got0[:, 0:128], q2_0, kv[:, 0:128], k2, table)
    ret0 = exchange(grads0.reshape(SP_SIZE, TOKENS, 256))
    got1 = exchange(sent1).reshape(LENGTH, 128)
    grads1 = attention(got1, q2_1, kv[:, 128:256], k2, table)
    ret1 = exchange(grads1.reshape(SP_SIZE, TOKENS, 256))

    parts = [
        lax.dot_general(
            g[:, 128:256], nlat_full, (((0,), (0,)), ((), ())), preferred_element_type=f32
        )
        for g in (grads0, grads1)
    ]
    d_w = jnp.concatenate(parts, axis=0)
    gain_part = jnp.sum(d_w * w_own.astype(f32), axis=0) / latent_norm_gain
    gain_grad = lax.psum(gain_part, SP_DP)

    pieces = d_w.reshape(2, 2, 4, 16, LATENT).transpose(0, 2, 1, 3, 4).reshape(DP_SIZE, 32, LATENT)
    piece = lax.all_to_all(pieces, DP, split_axis=0, concat_axis=0, tiled=True).sum(axis=0)
    moved = lax.ppermute(piece, SP_DP, [(b, a) for a, b in to_heads()])
    blocks = lax.all_gather(moved, SP, axis=0, tiled=False)

    query_grad, latent_grad, rope_sum = finish(
        ret0, ret1, w_whole, latent[0], latent_norm_gain[None]
    )
    position = (spot * TOKENS + jnp.arange(TOKENS)).astype(f32)
    angle = position[:, None] * inverse_frequency(jnp.arange(16))[None, :]
    rope_grad = rotate(rope_sum[:, 96:128], jnp.cos(angle), -jnp.sin(angle))
    return (
        query_grad[None],
        latent_grad[None],
        rope_grad[None],
        blocks[:, 0:16].reshape(256, LATENT),
        blocks[:, 16:32].reshape(256, LATENT),
        gain_grad,
    )


def solution(mesh):
    split = Mesh(mesh.devices.reshape(4, 4, 4, 2), ("sp_0", "sp_1", "dp_0", "dp_1"))
    in_specs = (
        P(DP, SP, None),
        P(DP, SP, None),
        P(DP, SP, None),
        P(),
        P(DP, None),
        P(DP, None),
        P(DP, SP, None),
    )
    out_specs = (P(DP, SP, None), P(DP, SP, None), P(DP, SP, None), P(DP, None), P(DP, None), P())
    return jax.shard_map(local, mesh=split, in_specs=in_specs, out_specs=out_specs, check_vma=False)
```

time: 634 us -> 382 us (0.60); the launches traced: 624 us -> 380 us
  matrix products: 182 us -> 15.9 us
  waiting for transfers between devices: 152 us -> 60.8 us
  local copies, waits for them, and re-layouts: 105 us -> 15.9 us
  blocking collectives: 66.1 us -> 147 us
  Pallas kernels: 0 us -> 78.2 us
  other arithmetic: 78.7 us -> 14.4 us
  starting transfers between devices: 25.5 us -> 34.1 us
    dot_general x51 -> x4, matrix products: 182 us -> 15.9 us  [the longest x1 8.05 us: local(): jnp.dot(rotated, jnp.asarray(spread, bf16), preferred_element_type=f32)]
    pallas_call x0 -> x4, Pallas kernels: none -> 78.2 us  [the longest x2 60.7 us: attention(): pl.pallas_call(attention_kernel, grid=(count,), in_specs=[whole] * 4 + [p...]
    all_to_all x4 -> x3, waiting for transfers between devices: 107 us -> 38.9 us  [exchange(): return lax.all_to_all(value, SP, split_axis=0, concat_axis=0, tiled=True)]
    psum x4 -> x1, blocking collectives: 30 us -> 83.8 us  [local(): gain_grad = lax.psum(gain_part, SP_DP)]
    all_to_all x1 -> x2, blocking collectives: 19.4 us -> 63.4 us  [the longest x1 41.2 us: exchange(): return lax.all_to_all(value, SP, split_axis=0, concat_axis=0, tiled=True)]
    sub x6 -> x0, other arithmetic: 32.6 us -> none  [attend_backward(): probs = jax.nn.softmax(scores, axis=-1)]
    psum x1 -> x0, waiting for transfers between devices: 27.2 us -> none  [local(): weight_grads = lax.psum(partial_value, SP)]
    all_to_all x5 -> x0, local copies, waits for them, and re-layouts: 22 us -> none  [the longest x2 15.5 us: local(): lax.all_to_all(packed, SP, split_axis=1, concat_axis=0, tiled=True)]
  transfers between devices with their start and end apart: 8 -> 8, of which waited for: 5 -> 2; matrix products, arithmetic and copies ran while one was open for 50% -> 8% of each run, Pallas kernels for 0% -> 2%
where the time goes in v1:
time: 382 us; the launch traced here: 380 us
  blocking collectives  147 us (38%)
  Pallas kernels  78.2 us (20%)
  waiting for transfers between devices  60.8 us (16%)
  starting transfers between devices  34.1 us (9%)
  local copies, waits for them, and re-layouts  15.9 us (4%)
  matrix products  15.9 us (4%)
  other arithmetic  14.4 us (4%)
  between operations  14 us (4%)
    psum x1, blocking collectives, local(): gain_grad = lax.psum(gain_part, SP_DP)  83.8 us
    pallas_call x2, Pallas kernels, attention(): pl.pallas_call(attention_kernel, grid=(count,), in_specs=[whole] * 4 + [p...  60.7 us
    all_to_all x1, blocking collectives, exchange(): return lax.all_to_all(value, SP, split_axis=0, concat_axis=0, tiled=True)  41.2 us
    all_to_all x3, waiting for transfers between devices, exchange(): return lax.all_to_all(value, SP, split_axis=0, concat_axis=0, tiled=True)  38.9 us
    all_to_all x3, starting transfers between devices, exchange(): return lax.all_to_all(value, SP, split_axis=0, concat_axis=0, tiled=True)  27.5 us
    all_to_all x1, blocking collectives, local(): lax.all_to_all(pieces, DP, split_axis=0, concat_axis=0, tiled=True)  22.2 us
    all_gather x1, waiting for transfers between devices, local(): nlat_full = lax.all_gather(nlat, SP, axis=0, tiled=True)  21.1 us
    pallas_call x1, Pallas kernels, finish(): pl.pallas_call(finish_kernel, grid=(8,), in_specs=[pl.BlockSpec((2, TOKEN...  10 us
  transfers between devices with their start and end apart: 8, of which 2 were waited for; matrix products, arithmetic and copies ran while one was open for 8% of the time, Pallas kernels for 2%

profile of v1, /device:TPU:0, one launch (start us, length us, event | category | flops | bytes accessed | tf_op | source)
XLA Modules:
  0.0 380.4 jit_solution(10982995614421437774)
XLA Ops:
  8.4 1.9 fusion.6
  11.1 7.5 %pack.1 = (bf16[16,192,256]{2,1,0:T(8,128)(2,1)}, bf16[16,192,128]{2,1,0:T(8,128)(2,1)}) custom-call(bf16[192,3072]{1,0:T(8,128)(2,1)} %bitcast.55, bf16[192,2048]{1,0:T(8,128)(2,1)} %bitcast.56, bf16[192,128]{1,0:T(8,128)(2,1)} %pad.4.rope, bf16[768,512]{1,0:T(8,128)(2,1)} %constant.87.clone.first, bf16[768,256]{1,0:T(8,128)(2,1)} %constant.88.clone.second), custom_call_target="tpu_custom_call" | custom-call | flops 1811939328 | bytes 5000000 | tf_op jit(solution)/shard_map/pack/pallas_call | solution.py:90
  18.6 8.3 %all-to-all-start = ((bf16[16,192,256]{2,1,0:T(8,128)(2,1)}), bf16[16,192,256]{2,1,0:T(8,128)(2,1)S(1)}, u32[]{:S(2)}, u32[]{:S(2)}) async-start(bf16[16,192,256]{2,1,0:T(8,128)(2,1)} %get-tuple-element.12), calls=%async_computation | async-start | bytes 3145728 | tf_op jit(solution)/shard_map/all_to_all | solution.py:319
  29.0 5.4 %collective-permute-start = (bf16[256,1024]{1,0:T(8,128)(2,1)}, bf16[256,1024]{1,0:T(8,128)(2,1)}, u32[]{:S(2)}, u32[]{:S(2)}) collective-permute-start(bf16[256,1024]{1,0:T(8,128)(2,1)} %dynamic-slice_bitcast_fusion), channel_id=1, source_target_pairs={{0,0},{64,8},{8,1},{72,9},{16,2},{80,10},{24,3},{88,11},{32,4},{96... | collective-permute-start | bytes 1572872 | tf_op jit(solution)/shard_map/ppermute | solution.py:334
  34.4 6.8 %select_select_fusion.tab_ref = f32[3072,128]{1,0:T(8,128)} fusion(f32[128]{0:T(128)S(1)} %fusion.24, pred[128]{0:T(512)(128)(4,1)S(1)} %get-tuple-element.41, pred[128]{0:T(512)(128)(4,1)S(1)} %get-tuple-element.42), kind=kLoop, calls=%fused_computation.5 | loop fusion | flops 1179648 | bytes 1573632 | tf_op jit(solution)/shard_map/jit(_where)/select_n | solution.py:344
  41.2 38.9 %all-to-all-done = bf16[16,192,256]{2,1,0:T(8,128)(2,1)S(1)} async-done(((bf16[16,192,256]{2,1,0:T(8,128)(2,1)}), bf16[16,192,256]{2,1,0:T(8,128)(2,1)S(1)}, u32[]{:S(2)}, u32[]{:S(2)}) %all-to-all-start) | async-done | bytes 1572896 | tf_op jit(solution)/shard_map/all_to_all | solution.py:319
  80.1 15.4 %all-to-all-start.2 = ((bf16[16,192,128]{2,1,0:T(8,128)(2,1)}), bf16[16,192,128]{2,1,0:T(8,128)(2,1)S(1)}, u32[]{:S(2)}, u32[]{:S(2)}) async-start(bf16[16,192,128]{2,1,0:T(8,128)(2,1)} %get-tuple-element.13), calls=%async_computation.2 | async-start | bytes 1572864 | tf_op jit(solution)/shard_map/all_to_all | solution.py:319
  96.6 8.0 %convolution_convert_fusion = bf16[3072,384]{1,0:T(8,128)(2,1)} fusion(bf16[128,384]{1,0:T(8,128)(2,1)S(1)} %copy-done.12, bf16[128,128]{1,0:T(8,128)(2,1)S(1)} %copy-done.13, bf16[3072,256]{1,0:T(8,128)(2,1)S(1)} %bitcast.46, f32[128]{0:T(128)S(1)} %fusion.24), kind=kOutput, calls=%fused_computation | convolution fusion | flops 406192128 | bytes 4063744 | tf_op jit(solution)/shard_map/dot_general | solution.py:350
  104.7 2.6 fusion.25
  107.3 21.1 %all-gather.5.cloned.1.call-done = bf16[3072,1024]{1,0:T(8,128)(2,1)} async-done(((bf16[192,1024]{1,0:T(8,128)(2,1)}), bf16[3072,1024]{1,0:T(8,128)(2,1)}) %all-gather.5.cloned.1.call-update) | async-done | bytes 6291472 | tf_op jit(solution)/shard_map/all_gather | solution.py:326
  128.5 4.7 %convolution_convert_fusion.1 = bf16[3072,256]{1,0:T(8,128)(2,1)S(1)} fusion(bf16[3072,1024]{1,0:T(8,128)(2,1)} %all-gather.5.cloned.1.call-done, bf16[256,1024]{1,0:T(8,128)(2,1)} %collective-permute-done), kind=kOutput, calls=%fused_computation.1 | convolution fusion | flops 1611399168 | bytes 8388608 | tf_op jit(solution)/shard_map/dot_general | solution.py:353
  133.2 1.2 fusion.27
  138.7 30.0 %attention.3 = bf16[3072,256]{1,0:T(8,128)(2,1)S(1)} custom-call(bf16[3072,128]{1,0:T(8,128)(2,1)S(1)} %bitcast.38, bf16[3072,128]{1,0:T(8,128)(2,1)S(1)} %copy-done, bf16[3072,128]{1,0:T(8,128)(2,1)S(1)} %copy-done.5, bf16[3072,128]{1,0:T(8,128)(2,1)S(1)} %get-tuple-element.31.k2_ref, f32[3072,128]{1,0:T(8,128)} %select_select_fusion.tab_ref), custom_call_target="tpu_custom_call" | custom-call | flops 12000000000 | bytes 8000000 | tf_op jit(solution)/shard_map/attention/pallas_call | solution.py:209
  168.7 30.7 %attention.2 = bf16[3072,256]{1,0:T(8,128)(2,1)} custom-call(bf16[3072,128]{1,0:T(8,128)(2,1)S(1)} %copy-done.3, bf16[3072,128]{1,0:T(8,128)(2,1)S(1)} %get-tuple-element.32.q2_ref, bf16[3072,128]{1,0:T(8,128)(2,1)S(1)} %copy-done.4, bf16[3072,128]{1,0:T(8,128)(2,1)S(1)} %get-tuple-element.31.k2_ref, f32[3072,128]{1,0:T(8,128)} %select_select_fusion.tab_ref), custom_call_target="tpu_custom_call" | custom-call | flops 12000000000 | bytes 8000000 | tf_op jit(solution)/shard_map/attention/pallas_call | solution.py:209
  200.4 2.1 fusion.9
  202.6 1.3 multiply_reduce_fusion
  203.9 22.2 %all_to_all.25 = f32[8,32,1024]{2,1,0:T(8,128)S(1)} all-to-all(f32[8,32,1024]{2,1,0:T(8,128)S(1)} %bitcast.44), channel_id=1, replica_groups=mesh['sp_0'=4,'sp_1'=4,'dp_0'=4,'dp_1'=2] {'dp_0','dp_1'}, dimensions={0} | all-to-all | bytes 2097152 | tf_op jit(solution)/shard_map/all_to_all | solution.py:377
  228.5 41.2 %all_to_all.26.ret1 = bf16[16,192,256]{2,1,0:T(8,128)(2,1)} all-to-all(bf16[16,192,256]{2,1,0:T(8,128)(2,1)S(1)} %bitcast.37), channel_id=1, replica_groups=mesh['sp_0'=4,'sp_1'=4,'dp_0'=4,'dp_1'=2] {'sp_0','sp_1'}, dimensions={0} | all-to-all | bytes 3145728 | tf_op jit(solution)/shard_map/all_to_all | solution.py:319
  269.7 3.8 %all-to-all-start.1 = ((bf16[16,192,256]{2,1,0:T(8,128)(2,1)}), bf16[16,192,256]{2,1,0:T(8,128)(2,1)S(1)}, u32[]{:S(2)}, u32[]{:S(2)}) async-start(bf16[16,192,256]{2,1,0:T(8,128)(2,1)} %bitcast.11), calls=%async_computation.1 | async-start | bytes 3145728 | tf_op jit(solution)/shard_map/all_to_all | solution.py:319
  273.6 83.8 %psum.7 = f32[1024]{0:T(1024)} all-reduce(f32[1024]{0:T(1024)S(1)} %div.46), channel_id=1, replica_groups=mesh['sp_0'=4,'sp_1'=4,'dp_0'=4,'dp_1'=2] {'sp_0','sp_1','dp_0','dp_1'}, use_global_device_ids=true, to_apply=%region_3.4 | all-reduce | flops 1024 | bytes 8192 | tf_op jit(solution)/shard_map/psum | solution.py:374
  357.4 3.1 fusion.26
  360.5 1.2 copy-done.7
  361.7 10.0 %finish.1 = (bf16[192,3072]{1,0:T(8,128)(2,1)}, f32[192,1024]{1,0:T(8,128)}, f32[192,128]{1,0:T(8,128)}) custom-call(bf16[16,192,256]{2,1,0:T(8,128)(2,1)} %copy-done.7, bf16[16,192,256]{2,1,0:T(8,128)(2,1)} %all_to_all.26.ret1, bf16[16,256,1024]{2,1,0:T(8,128)(2,1)} %all-gather.7.cloned.1.call-done.w, bf16[512,384]{1,0:T(8,128)(2,1)} %constant.91.clone.place, ...), custom_call_target="tpu_custom_call" | custom-call | flops 4000000000 | bytes 14000000 | tf_op jit(solution)/shard_map/finish/pallas_call | solution.py:266
  371.7 1.4 fusion.16
  (63 shorter events, 13.7 us)
Async XLA Ops:
  7.2 3.2 copy-start.11
  7.2 121.3 %all-gather.5.cloned.1.call-start = ((), (), s32[]{:S(2)}) async-start(), calls=%async_computation.5 | async-start | bytes 6684672 | tf_op jit(solution)/shard_map/all_gather | solution.py:326
  18.6 8.3 %copy-start.8 = (bf16[256,1024]{1,0:T(8,128)(2,1)S(1)}, bf16[256,1024]{1,0:T(8,128)(2,1)}, u32[]{:S(2)}) copy-start(bf16[256,1024]{1,0:T(8,128)(2,1)} %param.17) | copy-start | bytes 1572868
  18.6 61.4 %all-to-all-start = ((bf16[16,192,256]{2,1,0:T(8,128)(2,1)}), bf16[16,192,256]{2,1,0:T(8,128)(2,1)S(1)}, u32[]{:S(2)}, u32[]{:S(2)}) async-start(bf16[16,192,256]{2,1,0:T(8,128)(2,1)} %get-tuple-element.12), calls=%async_computation | async-start | bytes 3145728 | tf_op jit(solution)/shard_map/all_to_all | solution.py:319
  28.1 52.0 %copy-start.6 = (bf16[2,2,2,64,1024]{4,3,2,1,0:T(8,128)(2,1)}, bf16[2,2,2,64,1024]{4,3,2,1,0:T(8,128)(2,1)S(1)}, u32[]{:S(2)}) copy-start(bf16[2,2,2,64,1024]{4,3,2,1,0:T(8,128)(2,1)S(1)} %pad_maximum_fusion) | copy-start | bytes 3145732
  29.0 78.3 %collective-permute-start = (bf16[256,1024]{1,0:T(8,128)(2,1)}, bf16[256,1024]{1,0:T(8,128)(2,1)}, u32[]{:S(2)}, u32[]{:S(2)}) collective-permute-start(bf16[256,1024]{1,0:T(8,128)(2,1)} %dynamic-slice_bitcast_fusion), channel_id=1, source_target_pairs={{0,0},{64,8},{8,1},{72,9},{16,2},{80,10},{24,3},{88,11},{32,4},{96... | collective-permute-start | bytes 1572872 | tf_op jit(solution)/shard_map/ppermute | solution.py:334
  80.1 16.6 %copy-start.12 = (bf16[128,384]{1,0:T(8,128)(2,1)S(1)}, bf16[128,384]{1,0:T(8,128)(2,1)}, u32[]{:S(2)}) copy-start(bf16[128,384]{1,0:T(8,128)(2,1)} %constant.90.clone) | copy-start | bytes 294916
  80.1 16.6 %copy-start.13 = (bf16[128,128]{1,0:T(8,128)(2,1)S(1)}, bf16[128,128]{1,0:T(8,128)(2,1)}, u32[]{:S(2)}) copy-start(bf16[128,128]{1,0:T(8,128)(2,1)} %constant.89.clone) | copy-start | bytes 98308
  80.1 54.3 %all-to-all-start.2 = ((bf16[16,192,128]{2,1,0:T(8,128)(2,1)}), bf16[16,192,128]{2,1,0:T(8,128)(2,1)S(1)}, u32[]{:S(2)}, u32[]{:S(2)}) async-start(bf16[16,192,128]{2,1,0:T(8,128)(2,1)} %get-tuple-element.13), calls=%async_computation.2 | async-start | bytes 1572864 | tf_op jit(solution)/shard_map/all_to_all | solution.py:319
  95.5 261.9 %all-gather.9.cloned.1.call-start = ((), (), s32[]{:S(2)}) async-start(), calls=%async_computation.7 | async-start | bytes 2228224 | tf_op jit(solution)/shard_map/all_gather | solution.py:379
  134.4 0.9 copy-start.1
  135.3 1.1 copy-start
  136.4 1.1 copy-start.2
  137.6 1.1 copy-start.5
  138.7 30.0 %copy-start.3 = (bf16[3072,128]{1,0:T(8,128)(2,1)S(1)}, bf16[3072,128]{1,0:T(8,128)(2,1)}, u32[]{:S(2)}) copy-start(bf16[3072,128]{1,0:T(8,128)(2,1)} %slice.55.a_ref) | copy-start | bytes 2359300
  138.7 30.0 %copy-start.4 = (bf16[3072,128]{1,0:T(8,128)(2,1)S(1)}, bf16[3072,128]{1,0:T(8,128)(2,1)}, u32[]{:S(2)}) copy-start(bf16[3072,128]{1,0:T(8,128)(2,1)} %get-tuple-element.36.kv_ref) | copy-start | bytes 2359300
  138.7 60.7 %slice-start = ((s8[6291456]{0:T(1024)(128)(4,1)}), s8[2097152]{0:T(1024)(128)(4,1)S(1)}, s32[]{:S(2)}) async-start(s8[6291456]{0:T(1024)(128)(4,1)} %bitcast.39), calls=%async_computation.8 | async-start | bytes 4194304
  168.7 30.7 %slice-start.1 = ((s8[6291456]{0:T(1024)(128)(4,1)}), s8[4194304]{0:T(1024)(128)(4,1)S(1)}, s32[]{:S(2)}) async-start(s8[6291456]{0:T(1024)(128)(4,1)} %bitcast.39), calls=%async_computation.9 | async-start | bytes 8388608
  226.2 0.9 collective-permute-start.1
  227.1 0.7 copy-start.9
  227.8 132.7 %all-gather.7.cloned.1.call-start = ((), (), s32[]{:S(2)}) async-start(), calls=%async_computation.6 | async-start | bytes 9437184 | tf_op jit(solution)/shard_map/all_gather | solution.py:358
  269.7 3.9 %copy-start.10 = (f32[1024]{0:T(1024)S(1)}, f32[1024]{0:T(1024)}, u32[]{:S(2)}) copy-start(f32[1024]{0:T(1024)} %param.15) | copy-start | bytes 12292
  269.7 90.8 %all-to-all-start.1 = ((bf16[16,192,256]{2,1,0:T(8,128)(2,1)}), bf16[16,192,256]{2,1,0:T(8,128)(2,1)S(1)}, u32[]{:S(2)}, u32[]{:S(2)}) async-start(bf16[16,192,256]{2,1,0:T(8,128)(2,1)} %bitcast.11), calls=%async_computation.1 | async-start | bytes 3145728 | tf_op jit(solution)/shard_map/all_to_all | solution.py:319
  360.5 1.2 copy-start.7
Sparse Core Ops, SparseCore 0:
  10.5 117.9 all-gather.4
  227.9 73.2 all-gather.8
  303.5 51.0 all-gather.6

commit v2 on v1

--- a/solution.py
+++ b/solution.py
@@ -9,10 +9,9 @@
 from jax.sharding import Mesh
 from jax.sharding import PartitionSpec as P
 
-ATTENTION_HEADS = 32
+
 PLAIN_HEAD_WIDTH = 64
 ROPE = 32
-VALUE_HEAD_WIDTH = 64
 SPAN = 64
 LATENT = 1024
 LENGTH = 3072
@@ -315,15 +314,133 @@
     return pairs
 
 
+def spread_kernel(with_messages, *refs):
+    if with_messages:
+        x, msgs, full, got, own_sem, leg_send, leg_recv, far_send, far_recv, msg_send, msg_recv = refs
+    else:
+        x, full, own_sem, leg_send, leg_recv, far_send, far_recv = refs
+    z, y = lax.axis_index("sp_0"), lax.axis_index("sp_1")
+    me = 4 * z + y
+    size = x.shape[0] // 2
+
+    def at(dz, dy):
+        return {"sp_0": lax.rem(z + dz, 4), "sp_1": lax.rem(y + dy, 4)}
+
+    barrier = pltpu.get_barrier_semaphore()
+    for k in range(1, SP_SIZE):
+        pl.semaphore_signal(
+            barrier, inc=1, device_id=at(k // 4, k % 4), device_id_type=pl.DeviceIdType.MESH
+        )
+    pl.semaphore_wait(barrier, SP_SIZE - 1)
+
+    def copy(src, dst, send, recv, where):
+        c = pltpu.make_async_remote_copy(
+            src_ref=src,
+            dst_ref=dst,
+            send_sem=send,
+            recv_sem=recv,
+            device_id=where,
+            device_id_type=pl.DeviceIdType.MESH,
+        )
+        c.start()
+        return c
+
+    steps = (1, 3, 2)
+    halves = (pl.ds(0, size), pl.ds(size, size))
+    own = [pltpu.make_async_copy(x, full.at[me], own_sem.at[0])]
+    if with_messages:
+        own.append(pltpu.make_async_copy(msgs.at[me], got.at[me], own_sem.at[1]))
+    near = {}
+    far = []
+    for d in steps:
+        for h in range(2):
+            where = at(0, d) if h == 0 else at(d, 0)
+            near[h, d] = copy(
+                x.at[halves[h]],
+                full.at[me, halves[h]],
+                leg_send.at[h, d - 1],
+                leg_recv.at[h, d - 1],
+                where,
+            )
+    for c in own:
+        c.start()
+    for e in steps:
+        for h in range(2):
+            where = at(e, 0) if h == 0 else at(0, e)
+            far.append(
+                copy(
+                    x.at[halves[h]],
+                    full.at[me, halves[h]],
+                    far_send.at[h, 0, e - 1],
+                    far_recv.at[h, 0, e - 1],
+                    where,
+                )
+            )
+    if with_messages:
+        for k in range(1, SP_SIZE):
+            there = 4 * lax.rem(z + k // 4, 4) + lax.rem(y + k % 4, 4)
+            far.append(
+                copy(
+                    msgs.at[there],
+                    got.at[me],
+                    msg_send.at[k - 1],
+                    msg_recv.at[k - 1],
+                    at(k // 4, k % 4),
+                )
+            )
+    for d in steps:
+        for h in range(2):
+            near[h, d].wait_recv()
+            if h == 0:
+                source = 4 * z + lax.rem(y + 4 - d, 4)
+            else:
+                source = 4 * lax.rem(z + 4 - d, 4) + y
+            block = full.at[source, halves[h]]
+            for e in steps:
+                where = at(e, 0) if h == 0 else at(0, e)
+                far.append(
+                    copy(block, block, far_send.at[h, d, e - 1], far_recv.at[h, d, e - 1], where)
+                )
+    for c in near.values():
+        c.wait_send()
+    for c in far:
+        c.wait()
+    for c in own:
+        c.wait()
+
+
+def spread_over_sp(x, msgs, collective_id):
+    with_messages = msgs is not None
+    vmem = pl.BlockSpec(memory_space=pltpu.VMEM)
+    anywhere = pl.BlockSpec(memory_space=pl.ANY)
+    out_shape = [jax.ShapeDtypeStruct((SP_SIZE, *x.shape), x.dtype)]
+    dma = pltpu.SemaphoreType.DMA
+    scratch = [dma((2,)), dma((2, 3)), dma((2, 3)), dma((2, 4, 3)), dma((2, 4, 3))]
+    if with_messages:
+        out_shape.append(jax.ShapeDtypeStruct(msgs.shape, msgs.dtype))
+        scratch += [dma((SP_SIZE - 1,)), dma((SP_SIZE - 1,))]
+    return pl.pallas_call(
+        functools.partial(spread_kernel, with_messages),
+        in_specs=[vmem] * (1 + with_messages),
+        out_specs=[anywhere] * (1 + with_messages),
+        out_shape=out_shape,
+        scratch_shapes=scratch,
+        compiler_params=pltpu.CompilerParams(collective_id=collective_id, has_side_effects=True),
+        cost_estimate=pl.CostEstimate(
+            flops=8_000_000_000, bytes_accessed=8_000_000, transcendentals=0
+        ),
+        name="spread",
+    )(*((x, msgs) if with_messages else (x,)))
+
+
 def exchange(value):
     return lax.all_to_all(value, SP, split_axis=0, concat_axis=0, tiled=True)
 
 
-def local(query, latent, rope_key, latent_norm_gain, key_up_matrix, value_up_matrix, out_grad):
+def layer(query, latent, rope_key, latent_norm_gain, key_up_matrix, value_up_matrix, out_grad):
     lat = latent[0].astype(f32)
     inv_rms = lax.rsqrt(jnp.mean(lat * lat, axis=-1, keepdims=True) + eps)
     nlat = (lat * inv_rms * latent_norm_gain).astype(bf16)
-    nlat_full = lax.all_gather(nlat, SP, axis=0, tiled=True)
 
     shard = jnp.stack(
         [key_up_matrix.reshape(2, 2, 64, LATENT), value_up_matrix.reshape(2, 2, 64, LATENT)],
@@ -332,10 +449,15 @@
     spot = lax.axis_index(SP)
     half = lax.dynamic_index_in_dim(shard, spot // 8, 0, keepdims=False)
     w_own = lax.ppermute(half, SP_DP, to_heads())
+    w_whole = lax.all_gather(shard, DP, axis=0, tiled=True)
 
     rope_wide = jnp.pad(rope_key[0], ((0, 0), (0, 96)))
     sent0, sent1 = pack(query[0], out_grad[0], rope_wide)
-    got0 = exchange(sent0).reshape(LENGTH, 256)
+    nlat_full, got0 = spread_over_sp(nlat, sent0, 0)
+    nlat_full = nlat_full.reshape(LENGTH, LATENT)
+    got0 = got0.reshape(LENGTH, 256)
+    sent1, got0 = lax.optimization_barrier((sent1, got0))
+    got1 = exchange(sent1).reshape(LENGTH, 128)
 
     column = jnp.arange(128)
     turned = jnp.arange(LENGTH, dtype=f32)[:, None] * inverse_frequency(column % 16)[None, :]
@@ -354,29 +476,32 @@
         nlat_full, w_own, (((1,), (1,)), ((), ())), preferred_element_type=f32
     ).astype(bf16)
 
-    shard_later, _ = lax.optimization_barrier((shard, nlat_full))
-    w_whole = lax.all_gather(shard_later, DP, axis=0, tiled=True)
+    def weight_part(grads, h):
+        d_w = lax.dot_general(
+            grads[:, 128:256], nlat_full, (((0,), (0,)), ((), ())), preferred_element_type=f32
+        )
+        own = w_own[128 * h : 128 * h + 128].astype(f32)
+        gain_part = jnp.sum(d_w * own, axis=0)
+        pieces = (
+            d_w.reshape(2, DP_SIZE, 8, LATENT)
+            .transpose(1, 0, 2, 3)
+            .reshape(DP_SIZE, 16, LATENT)
+        )
+        arrived = lax.psum_scatter(pieces, DP, scatter_dimension=0, tiled=True)[0]
+        return arrived, gain_part
 
     grads0 = attention(got0[:, 0:128], q2_0, kv[:, 0:128], k2, table)
+    grads0, got1 = lax.optimization_barrier((grads0, got1))
     ret0 = exchange(grads0.reshape(SP_SIZE, TOKENS, 256))
-    got1 = exchange(sent1).reshape(LENGTH, 128)
+    arrived0, gain0 = weight_part(grads0, 0)
     grads1 = attention(got1, q2_1, kv[:, 128:256], k2, table)
+    grads1, ret0 = lax.optimization_barrier((grads1, ret0))
     ret1 = exchange(grads1.reshape(SP_SIZE, TOKENS, 256))
-
-    parts = [
-        lax.dot_general(
-            g[:, 128:256], nlat_full, (((0,), (0,)), ((), ())), preferred_element_type=f32
-        )
-        for g in (grads0, grads1)
-    ]
-    d_w = jnp.concatenate(parts, axis=0)
-    gain_part = jnp.sum(d_w * w_own.astype(f32), axis=0) / latent_norm_gain
-    gain_grad = lax.psum(gain_part, SP_DP)
-
-    pieces = d_w.reshape(2, 2, 4, 16, LATENT).transpose(0, 2, 1, 3, 4).reshape(DP_SIZE, 32, LATENT)
-    piece = lax.all_to_all(pieces, DP, split_axis=0, concat_axis=0, tiled=True).sum(axis=0)
+    arrived1, gain1 = weight_part(grads1, 1)
+    piece = jnp.concatenate([arrived0, arrived1], axis=0)
     moved = lax.ppermute(piece, SP_DP, [(b, a) for a, b in to_heads()])
-    blocks = lax.all_gather(moved, SP, axis=0, tiled=False)
+    gain_grad = lax.psum((gain0 + gain1) / latent_norm_gain, SP_DP)
+    (blocks,) = spread_over_sp(moved, None, 1)
 
     query_grad, latent_grad, rope_sum = finish(
         ret0, ret1, w_whole, latent[0], latent_norm_gain[None]
@@ -384,12 +509,14 @@
     position = (spot * TOKENS + jnp.arange(TOKENS)).astype(f32)
     angle = position[:, None] * inverse_frequency(jnp.arange(16))[None, :]
     rope_grad = rotate(rope_sum[:, 96:128], jnp.cos(angle), -jnp.sin(angle))
+    blocks = blocks.reshape(2, DP_SIZE, 2, 2, 8, LATENT).transpose(3, 0, 2, 1, 4, 5)
+    blocks = blocks.reshape(2, 256, LATENT)
     return (
         query_grad[None],
         latent_grad[None],
         rope_grad[None],
-        blocks[:, 0:16].reshape(256, LATENT),
-        blocks[:, 16:32].reshape(256, LATENT),
+        blocks[0],
+        blocks[1],
         gain_grad,
     )
 
@@ -406,4 +533,4 @@
         P(DP, SP, None),
     )
     out_specs = (P(DP, SP, None), P(DP, SP, None), P(DP, SP, None), P(DP, None), P(DP, None), P())
-    return jax.shard_map(local, mesh=split, in_specs=in_specs, out_specs=out_specs, check_vma=False)
+    return jax.shard_map(layer, mesh=split, in_specs=in_specs, out_specs=out_specs, check_vma=False)

time: 382 us -> 381 us (level)
  Pallas kernels: 78.2 us -> 188 us
  blocking collectives: 147 us -> 71.6 us
  waiting for transfers between devices: 60.8 us -> 29.3 us
    pallas_call x0 -> x2, Pallas kernels: none -> 109 us  [spread_over_sp(): pl.pallas_call(functools.partial(spread_kernel, with_messages), in_specs=...]
    all_to_all x2 -> x0, blocking collectives: 63.4 us -> none  [the longest x1 41.2 us: exchange(): return lax.all_to_all(value, SP, split_axis=0, concat_axis=0, tiled=True)]
    all_to_all x3, waiting for transfers between devices: 38.9 us -> 0.01 us  [exchange(): return lax.all_to_all(value, SP, split_axis=0, concat_axis=0, tiled=True)]
    reduce_scatter x0 -> x2, waiting for transfers between devices: none -> 28.6 us  [weight_part(): arrived = lax.psum_scatter(pieces, DP, scatter_dimension=0, tiled=True)[0]]
    all_gather x3 -> x1, waiting for transfers between devices: 21.1 us -> 0.01 us  [layer(): w_whole = lax.all_gather(shard, DP, axis=0, tiled=True)]
    psum x1, blocking collectives: 83.8 us -> 71.6 us  [layer(): gain_grad = lax.psum((gain0 + gain1) / latent_norm_gain, SP_DP)]
    slice x4 -> x6, local copies, waits for them, and re-layouts: 7.93 us -> 6.71 us  [the longest x2 2.72 us: layer(): blocks[1]]
  transfers between devices with their start and end apart: 8 -> 8, of which waited for: 2 -> 1; matrix products, arithmetic and copies ran while one was open for 8% -> 10% of each run, Pallas kernels for 2% -> 47%
where the time goes in v2:
time: 381 us; the launch traced here: 379 us
  Pallas kernels  188 us (49%)
  blocking collectives  71.6 us (19%)
  starting transfers between devices  32.4 us (9%)
  waiting for transfers between devices  29.3 us (8%)
  matrix products  19.3 us (5%)
  between operations  14 us (4%)
  local copies, waits for them, and re-layouts  12.9 us (3%)
  other arithmetic  12.1 us (3%)
    pallas_call x2, Pallas kernels, spread_over_sp(): pl.pallas_call(functools.partial(spread_kernel, with_messages), in_specs=...  109 us
    psum x1, blocking collectives, layer(): gain_grad = lax.psum((gain0 + gain1) / latent_norm_gain, SP_DP)  71.6 us
    pallas_call x2, Pallas kernels, attention(): pl.pallas_call(attention_kernel, grid=(count,), in_specs=[whole] * 4 + [p...  61.1 us
    reduce_scatter x2, waiting for transfers between devices, weight_part(): arrived = lax.psum_scatter(pieces, DP, scatter_dimension=0, tiled=True)[0]  28.6 us
    all_to_all x3, starting transfers between devices, exchange(): return lax.all_to_all(value, SP, split_axis=0, concat_axis=0, tiled=True)  26 us
    pallas_call x1, Pallas kernels, finish(): pl.pallas_call(finish_kernel, grid=(8,), in_specs=[pl.BlockSpec((2, TOKEN...  10 us
    dot_general x2, matrix products, weight_part(): lax.dot_general(grads[:, 128:256], nlat_full, (((0,), (0,)), ((), ())), p...  8.37 us
    dot_general x1, matrix products, layer(): jnp.dot(rotated, jnp.asarray(spread, bf16), preferred_element_type=f32)  8.07 us
  transfers between devices with their start and end apart: 8, of which 1 were waited for; matrix products, arithmetic and copies ran while one was open for 10% of the time, Pallas kernels for 47%

profile of v2, /device:TPU:0, one launch (start us, length us, event | category | flops | bytes accessed | tf_op | source)
XLA Modules:
  0.0 379.4 jit_solution(15147754359663688626)
XLA Ops:
  7.2 1.3 pad_maximum_fusion
  9.5 5.4 %collective-permute-start = (bf16[256,1024]{1,0:T(8,128)(2,1)}, bf16[256,1024]{1,0:T(8,128)(2,1)}, u32[]{:S(2)}, u32[]{:S(2)}) collective-permute-start(bf16[256,1024]{1,0:T(8,128)(2,1)} %dynamic-slice_bitcast_fusion), channel_id=1, source_target_pairs={{0,0},{64,8},{8,1},{72,9},{16,2},{80,10},{24,3},{88,11},{32,4},{96... | collective-permute-start | bytes 1572872 | tf_op jit(solution)/shard_map/ppermute | solution.py:451
  16.7 7.5 %pack.1 = (bf16[16,192,256]{2,1,0:T(8,128)(2,1)}, bf16[16,192,128]{2,1,0:T(8,128)(2,1)}) custom-call(bf16[192,3072]{1,0:T(8,128)(2,1)} %bitcast.72, bf16[192,2048]{1,0:T(8,128)(2,1)} %bitcast.73, bf16[192,128]{1,0:T(8,128)(2,1)} %pad.4.rope, bf16[768,512]{1,0:T(8,128)(2,1)} %constant.87.clone.first, bf16[768,256]{1,0:T(8,128)(2,1)} %constant.88.clone.second), custom_call_target="tpu_custom_call" | custom-call | flops 1811939328 | bytes 5000000 | tf_op jit(solution)/shard_map/pack/pallas_call | solution.py:89
  24.2 87.4 %spread.2 = (bf16[16,192,1024]{2,1,0:T(8,128)(2,1)}, bf16[16,192,256]{2,1,0:T(8,128)(2,1)}) custom-call(bf16[192,1024]{1,0:T(8,128)(2,1)} %fusion.6.refs_0_, bf16[16,192,256]{2,1,0:T(8,128)(2,1)} %get-tuple-element.20.refs_1_), custom_call_target="tpu_custom_call" | custom-call | flops 8000000000 | bytes 8000000 | tf_op jit(solution)/shard_map/spread/pallas_call | solution.py:422
  111.6 11.6 %all-to-all-start = ((bf16[16,192,128]{2,1,0:T(8,128)(2,1)}), bf16[16,192,128]{2,1,0:T(8,128)(2,1)S(1)}, u32[]{:S(2)}, u32[]{:S(2)}) async-start(bf16[16,192,128]{2,1,0:T(8,128)(2,1)} %get-tuple-element.24), calls=%async_computation | async-start | bytes 1572864 | tf_op jit(solution)/shard_map/all_to_all | solution.py:437
  123.4 8.1 %convolution_convert_fusion = bf16[3072,384]{1,0:T(8,128)(2,1)} fusion(bf16[128,384]{1,0:T(8,128)(2,1)S(1)} %copy-done.10, bf16[128,128]{1,0:T(8,128)(2,1)S(1)} %copy-done.11, f32[128]{0:T(128)S(1)} %fusion.24, bf16[3072,256]{1,0:T(8,128)(2,1)S(1)} %bitcast.67), kind=kOutput, calls=%fused_computation | convolution fusion | flops 406192128 | bytes 4063744 | tf_op jit(solution)/shard_map/dot_general | solution.py:472
  131.4 1.9 fusion.25
  133.3 6.8 %select_select_fusion.tab_ref = f32[3072,128]{1,0:T(8,128)} fusion(f32[128]{0:T(128)S(1)} %fusion.24, pred[128]{0:T(512)(128)(4,1)S(1)} %get-tuple-element.50, pred[128]{0:T(512)(128)(4,1)S(1)} %get-tuple-element.51), kind=kLoop, calls=%fused_computation.5 | loop fusion | flops 1179648 | bytes 1573632 | tf_op jit(solution)/shard_map/jit(_where)/select_n | solution.py:466
  140.1 2.9 convolution_convert_fusion.1
  144.0 30.6 %attention.2 = bf16[3072,256]{1,0:T(8,128)(2,1)} custom-call(bf16[3072,128]{1,0:T(8,128)(2,1)S(1)} %slice.50.a_ref, bf16[3072,128]{1,0:T(8,128)(2,1)S(1)} %get-tuple-element.42.q2_ref, bf16[3072,128]{1,0:T(8,128)(2,1)S(1)} %get-tuple-element.46.kv_ref, bf16[3072,128]{1,0:T(8,128)(2,1)S(1)} %get-tuple-element.41.k2_ref, f32[3072,128]{1,0:T(8,128)} %select_select_fusion.tab_ref), custom_call_target="tpu_custom_call" | custom-call | flops 12000000000 | bytes 8000000 | tf_op jit(solution)/shard_map/attention/pallas_call | solution.py:208
  174.5 7.3 %all-to-all-start.1 = ((bf16[16,192,256]{2,1,0:T(8,128)(2,1)}), bf16[16,192,256]{2,1,0:T(8,128)(2,1)}, u32[]{:S(2)}, u32[]{:S(2)}) async-start(bf16[16,192,256]{2,1,0:T(8,128)(2,1)} %bitcast.13), calls=%async_computation.1 | async-start | bytes 3145728 | tf_op jit(solution)/shard_map/all_to_all | solution.py:437
  182.0 4.1 %fusion.9 = f32[128,1024]{1,0:T(8,128)S(1)} fusion(bf16[3072,1024]{1,0:T(8,128)(2,1)} %bitcast.51, bf16[3072,256]{1,0:T(8,128)(2,1)} %attention.2), kind=kOutput, calls=%fused_computation.17 | convolution fusion | flops 805306368 | bytes 7602176 | tf_op jit(solution)/shard_map/dot_general | solution.py:480
  187.8 30.5 %attention.3 = bf16[3072,256]{1,0:T(8,128)(2,1)} custom-call(bf16[3072,128]{1,0:T(8,128)(2,1)S(1)} %bitcast.50, bf16[3072,128]{1,0:T(8,128)(2,1)S(1)} %get-tuple-element.40.q2_ref, bf16[3072,128]{1,0:T(8,128)(2,1)S(1)} %copy-done, bf16[3072,128]{1,0:T(8,128)(2,1)S(1)} %get-tuple-element.41.k2_ref, f32[3072,128]{1,0:T(8,128)} %select_select_fusion.tab_ref), custom_call_target="tpu_custom_call" | custom-call | flops 12000000000 | bytes 8000000 | tf_op jit(solution)/shard_map/attention/pallas_call | solution.py:208
  218.4 4.3 %multiply_reduce_fusion = (f32[1024]{0:T(1024)S(1)}, f32[1024]{0:T(1024)S(1)}, f32[128,1024]{1,0:T(8,128)S(1)}) fusion(bf16[256,1024]{1,0:T(8,128)(2,1)} %collective-permute-done, f32[128,1024]{1,0:T(8,128)} %copy-done.3, bf16[3072,1024]{1,0:T(8,128)(2,1)} %bitcast.52, bf16[3072,256]{1,0:T(8,128)(2,1)} %attention.3), kind=kOutput, calls=%fused_computation.23 | convolution fusion | flops 806090752 | bytes 8658944 | tf_op jit(solution)/shard_map/dot_general | solution.py:480
  224.3 7.2 %all-to-all-start.2 = ((bf16[16,192,256]{2,1,0:T(8,128)(2,1)}), bf16[16,192,256]{2,1,0:T(8,128)(2,1)S(1)}, u32[]{:S(2)}, u32[]{:S(2)}) async-start(bf16[16,192,256]{2,1,0:T(8,128)(2,1)} %bitcast.14), calls=%async_computation.2 | async-start | bytes 3145728 | tf_op jit(solution)/shard_map/all_to_all | solution.py:437
  231.5 28.6 %reduce-scatter.5.cloned.1.call-done = f32[1,16,1024]{2,1,0:T(8,128)} async-done(((f32[8,16,1024]{2,1,0:T(8,128)}), f32[1,16,1024]{2,1,0:T(8,128)}) %reduce-scatter.5.cloned.1.call-update) | async-done | bytes 65552 | tf_op jit(solution)/shard_map/reduce_scatter | solution.py:490
  261.7 71.6 %psum.7 = f32[1024]{0:T(1024)} all-reduce(f32[1024]{0:T(1024)S(1)} %add_divide_fusion), channel_id=1, replica_groups=mesh['sp_0'=4,'sp_1'=4,'dp_0'=4,'dp_1'=2] {'sp_0','sp_1','dp_0','dp_1'}, use_global_device_ids=true, to_apply=%region_5.6 | all-reduce | flops 1024 | bytes 8192 | tf_op jit(solution)/shard_map/psum | solution.py:503
  333.9 21.7 %spread.3 = f32[16,32,1024]{2,1,0:T(8,128)} custom-call(f32[32,1024]{1,0:T(8,128)} %copy-done.9), custom_call_target="tpu_custom_call" | custom-call | flops 8000000000 | bytes 8000000 | tf_op jit(solution)/shard_map/spread/pallas_call | solution.py:422
  355.7 1.7 fusion.26
  357.3 1.0 copy.43
  358.4 1.0 copy.44
  359.4 1.2 copy-done.4
  360.7 10.0 %finish.1 = (bf16[192,3072]{1,0:T(8,128)(2,1)}, f32[192,1024]{1,0:T(8,128)}, f32[192,128]{1,0:T(8,128)}) custom-call(bf16[16,192,256]{2,1,0:T(8,128)(2,1)} %all-to-all-done.1.ret0, bf16[16,192,256]{2,1,0:T(8,128)(2,1)} %copy-done.4, bf16[16,256,1024]{2,1,0:T(8,128)(2,1)} %all-gather.2.cloned.1.call-done.w, bf16[512,384]{1,0:T(8,128)(2,1)} %constant.91.clone.place, ...), custom_call_target="tpu_custom_call" | custom-call | flops 4000000000 | bytes 14000000 | tf_op jit(solution)/shard_map/finish/pallas_call | solution.py:265
  370.7 1.4 fusion.16
  (56 shorter events, 10.3 us)
Async XLA Ops:
  7.2 7.7 %copy-start.8 = (bf16[1,192,32]{1,2,0:T(8,128)(2,1)S(1)}, bf16[1,192,32]{1,2,0:T(8,128)(2,1)}, u32[]{:S(2)}) copy-start(bf16[1,192,32]{1,2,0:T(8,128)(2,1)} %param.14) | copy-start | bytes 36868
  7.2 7.8 %copy-start.5 = (bf16[1,192,1024]{2,1,0:T(8,128)(2,1)S(1)}, bf16[1,192,1024]{2,1,0:T(8,128)(2,1)}, u32[]{:S(2)}) copy-start(bf16[1,192,1024]{2,1,0:T(8,128)(2,1)} %param.13) | copy-start | bytes 1179652
  7.2 8.6 %copy-start.7 = (f32[1024]{0:T(1024)S(1)}, f32[1024]{0:T(1024)}, u32[]{:S(2)}) copy-start(f32[1024]{0:T(1024)} %param.15) | copy-start | bytes 12292
  8.6 15.6 %copy-start.2 = (bf16[2,2,2,64,1024]{4,3,2,1,0:T(8,128)(2,1)}, bf16[2,2,2,64,1024]{4,3,2,1,0:T(8,128)(2,1)S(1)}, u32[]{:S(2)}) copy-start(bf16[2,2,2,64,1024]{4,3,2,1,0:T(8,128)(2,1)S(1)} %pad_maximum_fusion) | copy-start | bytes 3145732
  9.5 130.6 %collective-permute-start = (bf16[256,1024]{1,0:T(8,128)(2,1)}, bf16[256,1024]{1,0:T(8,128)(2,1)}, u32[]{:S(2)}, u32[]{:S(2)}) collective-permute-start(bf16[256,1024]{1,0:T(8,128)(2,1)} %dynamic-slice_bitcast_fusion), channel_id=1, source_target_pairs={{0,0},{64,8},{8,1},{72,9},{16,2},{80,10},{24,3},{88,11},{32,4},{96... | collective-permute-start | bytes 1572872 | tf_op jit(solution)/shard_map/ppermute | solution.py:451
  111.6 11.7 %copy-start.6 = (bf16[16,192,256]{2,1,0:T(8,128)(2,1)S(1)}, bf16[16,192,256]{2,1,0:T(8,128)(2,1)}, u32[]{:S(2)}) copy-start(bf16[16,192,256]{2,1,0:T(8,128)(2,1)} %get-tuple-element.21) | copy-start | bytes 4718596
  111.6 11.7 %copy-start.10 = (bf16[128,384]{1,0:T(8,128)(2,1)S(1)}, bf16[128,384]{1,0:T(8,128)(2,1)}, u32[]{:S(2)}) copy-start(bf16[128,384]{1,0:T(8,128)(2,1)} %constant.90.clone) | copy-start | bytes 294916
  111.6 11.7 %copy-start.11 = (bf16[128,128]{1,0:T(8,128)(2,1)S(1)}, bf16[128,128]{1,0:T(8,128)(2,1)}, u32[]{:S(2)}) copy-start(bf16[128,128]{1,0:T(8,128)(2,1)} %constant.89.clone) | copy-start | bytes 98308
  111.6 62.9 %all-to-all-start = ((bf16[16,192,128]{2,1,0:T(8,128)(2,1)}), bf16[16,192,128]{2,1,0:T(8,128)(2,1)S(1)}, u32[]{:S(2)}, u32[]{:S(2)}) async-start(bf16[16,192,128]{2,1,0:T(8,128)(2,1)} %get-tuple-element.24), calls=%async_computation | async-start | bytes 1572864 | tf_op jit(solution)/shard_map/all_to_all | solution.py:437
  131.4 8.7 %copy-start.1 = (bf16[16,192,1024]{2,1,0:T(8,128)(2,1)S(1)}, bf16[16,192,1024]{2,1,0:T(8,128)(2,1)}, u32[]{:S(2)}) copy-start(bf16[16,192,1024]{2,1,0:T(8,128)(2,1)} %get-tuple-element.23) | copy-start | bytes 18874372
  174.5 43.8 %all-to-all-start.1 = ((bf16[16,192,256]{2,1,0:T(8,128)(2,1)}), bf16[16,192,256]{2,1,0:T(8,128)(2,1)}, u32[]{:S(2)}, u32[]{:S(2)}) async-start(bf16[16,192,256]{2,1,0:T(8,128)(2,1)} %bitcast.13), calls=%async_computation.1 | async-start | bytes 3145728 | tf_op jit(solution)/shard_map/all_to_all | solution.py:437
  181.8 49.7 %reduce-scatter.3.cloned.1.call-start = ((), (), s32[]{:S(2)}) async-start(), calls=%async_computation.6 | async-start | bytes 589824 | tf_op jit(solution)/shard_map/reduce_scatter | solution.py:490
  186.1 0.8 copy-start.3
  186.1 1.7 copy-start
  187.8 72.3 %reduce-scatter.5.cloned.1.call-start = ((), (), s32[]{:S(2)}) async-start(), calls=%async_computation.7 | async-start | bytes 589824 | tf_op jit(solution)/shard_map/reduce_scatter | solution.py:490
  223.5 135.9 %all-gather.2.cloned.1.call-start = ((), (), s32[]{:S(2)}) async-start(), calls=%async_computation.5 | async-start | bytes 9437184 | tf_op jit(solution)/shard_map/all_gather | solution.py:452
  224.3 135.1 %all-to-all-start.2 = ((bf16[16,192,256]{2,1,0:T(8,128)(2,1)}), bf16[16,192,256]{2,1,0:T(8,128)(2,1)S(1)}, u32[]{:S(2)}, u32[]{:S(2)}) async-start(bf16[16,192,256]{2,1,0:T(8,128)(2,1)} %bitcast.14), calls=%async_computation.2 | async-start | bytes 3145728 | tf_op jit(solution)/shard_map/all_to_all | solution.py:437
  261.0 72.3 %collective-permute-start.1 = (f32[32,1024]{1,0:T(8,128)S(1)}, f32[32,1024]{1,0:T(8,128)S(1)}, u32[]{:S(2)}, u32[]{:S(2)}) collective-permute-start(f32[32,1024]{1,0:T(8,128)S(1)} %pad_maximum_fusion.1), channel_id=1, source_target_pairs={{0,0},{8,64},{1,8},{9,72},{2,16},{10,80},{3,24},{11,88},{4,32},{12... | collective-permute-start | bytes 393224 | tf_op jit(solution)/shard_map/ppermute | solution.py:502
  333.3 0.7 copy-start.9
  359.4 1.2 copy-start.4
Sparse Core Ops, SparseCore 0:
  187.9 36.2 reduce-scatter.2
  227.1 32.9 reduce-scatter.4
  262.4 49.6 all-gather.1

commit v3 on v2

--- a/solution.py
+++ b/solution.py
@@ -48,42 +48,46 @@
     return first, second
 
 
-def unpack_table():
+def unpack_tables():
     place = np.zeros((512, 384), np.float32)
+    turn = np.zeros((512, 384), np.float32)
     for t in range(2):
         for h in range(2):
+            row, col = 256 * t + 128 * h, 192 * t + 96 * h
             for c in range(96):
-                place[256 * t + 128 * h + c, 192 * t + 96 * h + c] = 1
-    return place
-
-
-def rope_tables():
-    swap = np.zeros((128, 128), np.float32)
-    for g in range(3):
-        for c in range(16):
-            swap[32 * g + 16 + c, 32 * g + c] = -1
-            swap[32 * g + c, 32 * g + 16 + c] = 1
+                place[row + c, col + c] = 1
+            for c in range(64, 80):
+                turn[row + c + 16, col + c] = 1
+                turn[row + c, col + c + 16] = -1
+    return place, turn
+
+
+def rope_table():
     spread = np.zeros((128, 384), np.float32)
     for c in range(32):
         spread[c, c] = 1
         spread[32 + c, 128 + c] = 1
         spread[64 + c, 256 + c] = 1
-    for c in range(16):
-        spread[64 + 16 + c, 256 + 32 + c] = 1
-        spread[64 + c, 256 + 32 + 16 + c] = -1
-    return swap, spread
-
-
-def pack_kernel(query, d_out, rope, first, second, out0, out1):
+    return spread
+
+
+def turned_halves(x):
+    lane = lax.broadcasted_iota(jnp.int32, x.shape, 1)
+    return jnp.where(lane % 32 < 16, -pltpu.roll(x, 112, 1), pltpu.roll(x, 16, 1))
+
+
+def pack_kernel(query, d_out, rope, first, second, cosine, sine, out0, out1):
     both = jnp.concatenate([query[...], d_out[...], rope[...]], axis=1)
-    one = jnp.dot(both, first[...], preferred_element_type=f32).astype(bf16)
+    one = jnp.dot(both, first[...], preferred_element_type=f32)
     two = jnp.dot(both, second[...], preferred_element_type=f32).astype(bf16)
     for t in range(2):
-        out0[t] = one[:, 256 * t : 256 * t + 256]
+        out0[t, :, 0:128] = one[:, 256 * t : 256 * t + 128].astype(bf16)
+        raw = one[:, 256 * t + 128 : 256 * t + 256]
+        out0[t, :, 128:256] = (raw * cosine[...] + turned_halves(raw) * sine[...]).astype(bf16)
         out1[t] = two[:, 128 * t : 128 * t + 128]
 
 
-def pack(query, d_out, rope):
+def pack(query, d_out, rope, cosine, sine):
     first, second = pack_tables()
     whole = lambda shape: pl.BlockSpec(shape, lambda j: (0, 0))
     return pl.pallas_call(
@@ -95,6 +99,8 @@
             whole((TOKENS, 128)),
             whole((768, 512)),
             whole((768, 256)),
+            whole((TOKENS, 128)),
+            whole((TOKENS, 128)),
         ],
         out_specs=[
             pl.BlockSpec((2, TOKENS, 256), lambda j: (j, 0, 0)),
@@ -108,7 +114,7 @@
             flops=16 * 192 * 768 * 768, bytes_accessed=5_000_000, transcendentals=0
         ),
         name="pack",
-    )(query, d_out, rope, jnp.asarray(first, bf16), jnp.asarray(second, bf16))
+    )(query, d_out, rope, jnp.asarray(first, bf16), jnp.asarray(second, bf16), cosine, sine)
 
 
 def dot_t(a, b):
@@ -120,7 +126,7 @@
     return functools.reduce(combine, parts)
 
 
-def attention_kernel(a_ref, q2_ref, kv_ref, k2_ref, tab_ref, out_ref, s_ref, dp_ref, m_ref, l_ref, d_ref, dq_ref, acc_ref):
+def attention_kernel(a_ref, q2_ref, kv_ref, k2_ref, out_ref, s_ref, dp_ref, m_ref, l_ref, d_ref, dq_ref, acc_ref):
     step = pl.program_id(0)
     count = LENGTH // BLOCK
     i = count - 1 - step
@@ -191,9 +197,7 @@
         acc_ref[0:96, tile(j)] += jnp.dot(left_k, ds, preferred_element_type=f32)
         acc_ref[96:160, tile(j)] += jnp.dot(left_v, p.astype(bf16), preferred_element_type=f32)
 
-    turned = dq_ref[:, 128:256] * tab_ref[...]
-    turned = turned + pltpu.roll(turned, 96, 1)
-    dq = jnp.where(lane < 64, dq_ref[:, 0:128], pltpu.roll(turned, 64, 1)) * SCALE
+    dq = jnp.where(lane < 64, dq_ref[:, 0:128], pltpu.roll(dq_ref[:, 128:256], 64, 1)) * SCALE
     done = acc_ref[:, rows]
     k_rope = done[0:32] * SCALE
     k_nope = done[32:96] * SCALE
@@ -202,13 +206,16 @@
     out_ref[:, 128:256] = jnp.concatenate([k_nope, done[96:160]], axis=0).T.astype(bf16)
 
 
-def attention(a, q2, kv, k2, table):
+def attention(a, kv, ropes, head):
     count = LENGTH // BLOCK
-    whole = pl.BlockSpec((LENGTH, 128), lambda i: (0, 0))
+
+    def column(k):
+        return pl.BlockSpec((LENGTH, 128), lambda i: (0, k))
+
     return pl.pallas_call(
         attention_kernel,
         grid=(count,),
-        in_specs=[whole] * 4 + [pl.BlockSpec((BLOCK, 128), lambda i: (count - 1 - i, 0))],
+        in_specs=[column(0), column(head), column(head), column(2)],
         out_specs=pl.BlockSpec((BLOCK, 256), lambda i: (count - 1 - i, 0)),
         out_shape=jax.ShapeDtypeStruct((LENGTH, 256), bf16),
         scratch_shapes=[
@@ -227,10 +234,13 @@
             flops=12_000_000_000, bytes_accessed=8_000_000, transcendentals=5_000_000
         ),
         name="attention",
-    )(a, q2, kv, k2, table)
-
-
-def finish_kernel(ret0, ret1, w, place, latent, gain, query_grad, latent_grad, rope_sum, acc):
+    )(a, ropes, kv, ropes)
+
+
+def finish_kernel(
+    ret0, ret1, w, place, turn, latent, gain, wide_cos, wide_sin, cosine, sine,
+    query_grad, latent_grad, rope_sum, acc,
+):
     step = pl.program_id(0)
 
     @pl.when(step == 0)
@@ -239,9 +249,10 @@
         rope_sum[...] = jnp.zeros_like(rope_sum)
 
     left = [ret[t, :, 0:128] for t in range(2) for ret in (ret0, ret1)]
-    query_grad[...] = jnp.dot(
-        jnp.concatenate(left, axis=1), place[...], preferred_element_type=f32
-    ).astype(bf16)
+    row = jnp.concatenate(left, axis=1)
+    plain = jnp.dot(row, place[...], preferred_element_type=f32)
+    turned = jnp.dot(row, turn[...], preferred_element_type=f32)
+    query_grad[...] = (plain * wide_cos[...] + turned * wide_sin[...]).astype(bf16)
     rope_sum[...] += sum(x.astype(f32) for x in left)
     total = acc[...]
     for t in range(2):
@@ -258,10 +269,13 @@
         latent_grad[...] = inverse * (
             scaled - normed * jnp.mean(scaled * normed, axis=1, keepdims=True)
         )
-
-
-def finish(ret0, ret1, w, latent, gain):
+        total_rope = rope_sum[...]
+        rope_sum[...] = total_rope * cosine[...] - turned_halves(total_rope) * sine[...]
+
+
+def finish(ret0, ret1, w, latent, gain, wide_cos, wide_sin, cosine, sine):
     fixed = lambda shape: pl.BlockSpec(shape, lambda j: (0,) * len(shape))
+    place, turn = unpack_tables()
     return pl.pallas_call(
         finish_kernel,
         grid=(8,),
@@ -270,8 +284,13 @@
             pl.BlockSpec((2, TOKENS, 256), lambda j: (j, 0, 0)),
             pl.BlockSpec((2, 256, LATENT), lambda j: (j, 0, 0)),
             fixed((512, 384)),
+            fixed((512, 384)),
             fixed((TOKENS, LATENT)),
             fixed((1, LATENT)),
+            fixed((TOKENS, 384)),
+            fixed((TOKENS, 384)),
+            fixed((TOKENS, 128)),
+            fixed((TOKENS, 128)),
         ],
         out_specs=[
             pl.BlockSpec((TOKENS, 384), lambda j: (0, j)),
@@ -289,15 +308,9 @@
             flops=4_000_000_000, bytes_accessed=14_000_000, transcendentals=0
         ),
         name="finish",
-    )(ret0, ret1, w, jnp.asarray(unpack_table(), bf16), latent, gain)
-
-
-def rotate(values, cosine, sine):
-    half = values.shape[-1] // 2
-    first = values[..., :half]
-    second = values[..., half:]
-    return jnp.concatenate(
-        [first * cosine - second * sine, second * cosine + first * sine], axis=-1
+    )(
+        ret0, ret1, w, jnp.asarray(place, bf16), jnp.asarray(turn, bf16), latent, gain,
+        wide_cos, wide_sin, cosine, sine,
     )
 
 
@@ -315,10 +328,12 @@
 
 
 def spread_kernel(with_messages, *refs):
+    count = 2 if with_messages else 1
+    x, full = refs[0], refs[count]
+    own_sem, leg, leg_in, pass1, pass1_in, far, far_in, pass2, pass2_in = refs[2 * count : 2 * count + 9]
     if with_messages:
-        x, msgs, full, got, own_sem, leg_send, leg_recv, far_send, far_recv, msg_send, msg_recv = refs
-    else:
-        x, full, own_sem, leg_send, leg_recv, far_send, far_recv = refs
+        msgs, got = refs[1], refs[3]
+        msg_send, msg_recv = refs[2 * count + 9 :]
     z, y = lax.axis_index("sp_0"), lax.axis_index("sp_1")
     me = 4 * z + y
     size = x.shape[0] // 2
@@ -326,12 +341,26 @@
     def at(dz, dy):
         return {"sp_0": lax.rem(z + dz, 4), "sp_1": lax.rem(y + dy, 4)}
 
+    def along(h, s):
+        return at(0, s) if h == 0 else at(s, 0)
+
+    def across(h, s):
+        return at(s, 0) if h == 0 else at(0, s)
+
+    def block(h, s, c):
+        dz, dy = (c, s) if h == 0 else (s, c)
+        return 4 * lax.rem(z + dz, 4) + lax.rem(y + dy, 4)
+
+    if with_messages:
+        peers = [(k // 4, k % 4) for k in range(1, SP_SIZE)]
+    else:
+        peers = [(0, 1), (0, 3), (1, 0), (3, 0)]
     barrier = pltpu.get_barrier_semaphore()
-    for k in range(1, SP_SIZE):
+    for dz, dy in peers:
         pl.semaphore_signal(
-            barrier, inc=1, device_id=at(k // 4, k % 4), device_id_type=pl.DeviceIdType.MESH
+            barrier, inc=1, device_id=at(dz, dy), device_id_type=pl.DeviceIdType.MESH
         )
-    pl.semaphore_wait(barrier, SP_SIZE - 1)
+    pl.semaphore_wait(barrier, len(peers))
 
     def copy(src, dst, send, recv, where):
         c = pltpu.make_async_remote_copy(
@@ -345,67 +374,67 @@
         c.start()
         return c
 
-    steps = (1, 3, 2)
-    halves = (pl.ds(0, size), pl.ds(size, size))
+    half = [pl.ds(h * size, size) for h in range(2)]
+    quarter = [[pl.ds(h * size + q * size // 2, size // 2) for q in range(2)] for h in range(2)]
+    ways = (1, 3)
+    lines = (0, 3, 1, 2)
+    first, second, third, fourth, rest = {}, {}, {}, {}, []
+    for w, s in enumerate(ways):
+        for h in range(2):
+            first[h, w] = copy(
+                x.at[half[h]], full.at[me, half[h]], leg.at[h, w], leg_in.at[h, w], along(h, s)
+            )
+    for w, s in enumerate(ways):
+        for h in range(2):
+            third[h, 0, w] = copy(
+                x.at[half[h]], full.at[me, half[h]], far.at[h, 0, w], far_in.at[h, 0, w], across(h, s)
+            )
     own = [pltpu.make_async_copy(x, full.at[me], own_sem.at[0])]
     if with_messages:
         own.append(pltpu.make_async_copy(msgs.at[me], got.at[me], own_sem.at[1]))
-    near = {}
-    far = []
-    for d in steps:
-        for h in range(2):
-            where = at(0, d) if h == 0 else at(d, 0)
-            near[h, d] = copy(
-                x.at[halves[h]],
-                full.at[me, halves[h]],
-                leg_send.at[h, d - 1],
-                leg_recv.at[h, d - 1],
-                where,
-            )
     for c in own:
         c.start()
-    for e in steps:
-        for h in range(2):
-            where = at(e, 0) if h == 0 else at(0, e)
-            far.append(
+    if with_messages:
+        for k, (dz, dy) in enumerate(peers):
+            rest.append(
                 copy(
-                    x.at[halves[h]],
-                    full.at[me, halves[h]],
-                    far_send.at[h, 0, e - 1],
-                    far_recv.at[h, 0, e - 1],
-                    where,
+                    msgs.at[block(0, dy, dz)],
+                    got.at[me],
+                    msg_send.at[k],
+                    msg_recv.at[k],
+                    at(dz, dy),
                 )
             )
-    if with_messages:
-        for k in range(1, SP_SIZE):
-            there = 4 * lax.rem(z + k // 4, 4) + lax.rem(y + k % 4, 4)
-            far.append(
-                copy(
-                    msgs.at[there],
-                    got.at[me],
-                    msg_send.at[k - 1],
-                    msg_recv.at[k - 1],
-                    at(k // 4, k % 4),
+
+    def onward(h, k):
+        there = full.at[block(h, lines[k], 0), half[h]]
+        for w, s in enumerate(ways):
+            third[h, k, w] = copy(there, there, far.at[h, k, w], far_in.at[h, k, w], across(h, s))
+
+    for w, s in enumerate(ways):
+        for h in range(2):
+            first[h, w].wait_recv()
+            piece = full.at[block(h, 4 - s, 0), quarter[h][w]]
+            second[h, w] = copy(piece, piece, pass1.at[h, w], pass1_in.at[h, w], along(h, s))
+            onward(h, w + 1)
+    for h in range(2):
+        for w in range(2):
+            second[h, w].wait_recv()
+        onward(h, 3)
+    for k in range(4):
+        for w, s in enumerate(ways):
+            for h in range(2):
+                third[h, k, w].wait_recv()
+                piece = full.at[block(h, lines[k], 4 - s), quarter[h][w]]
+                fourth[h, k, w] = copy(
+                    piece, piece, pass2.at[h, k, w], pass2_in.at[h, k, w], across(h, s)
                 )
-            )
-    for d in steps:
-        for h in range(2):
-            near[h, d].wait_recv()
-            if h == 0:
-                source = 4 * z + lax.rem(y + 4 - d, 4)
-            else:
-                source = 4 * lax.rem(z + 4 - d, 4) + y
-            block = full.at[source, halves[h]]
-            for e in steps:
-                where = at(e, 0) if h == 0 else at(0, e)
-                far.append(
-                    copy(block, block, far_send.at[h, d, e - 1], far_recv.at[h, d, e - 1], where)
-                )
-    for c in near.values():
-        c.wait_send()
-    for c in far:
+    for group in (first, second, third):
+        for c in group.values():
+            c.wait_send()
+    for c in fourth.values():
         c.wait()
-    for c in own:
+    for c in rest + own:
         c.wait()
 
 
@@ -415,7 +444,7 @@
     anywhere = pl.BlockSpec(memory_space=pl.ANY)
     out_shape = [jax.ShapeDtypeStruct((SP_SIZE, *x.shape), x.dtype)]
     dma = pltpu.SemaphoreType.DMA
-    scratch = [dma((2,)), dma((2, 3)), dma((2, 3)), dma((2, 4, 3)), dma((2, 4, 3))]
+    scratch = [dma((2,))] + [dma((2, 2))] * 4 + [dma((2, 4, 2))] * 4
     if with_messages:
         out_shape.append(jax.ShapeDtypeStruct(msgs.shape, msgs.dtype))
         scratch += [dma((SP_SIZE - 1,)), dma((SP_SIZE - 1,))]
@@ -451,27 +480,24 @@
     w_own = lax.ppermute(half, SP_DP, to_heads())
     w_whole = lax.all_gather(shard, DP, axis=0, tiled=True)
 
+    position = (spot * TOKENS + jnp.arange(TOKENS)).astype(f32)[:, None]
+    angle = position * inverse_frequency(jnp.arange(128) % 16)[None]
+    cosine, sine = jnp.cos(angle), jnp.sin(angle)
+    place = jnp.arange(384) % 96
+    wide = position * jnp.where(place < 64, 0.0, inverse_frequency(place % 16))[None]
+    wide_cos, wide_sin = jnp.cos(wide), jnp.sin(wide)
+
     rope_wide = jnp.pad(rope_key[0], ((0, 0), (0, 96)))
-    sent0, sent1 = pack(query[0], out_grad[0], rope_wide)
+    sent0, sent1 = pack(query[0], out_grad[0], rope_wide, cosine, sine)
     nlat_full, got0 = spread_over_sp(nlat, sent0, 0)
     nlat_full = nlat_full.reshape(LENGTH, LATENT)
     got0 = got0.reshape(LENGTH, 256)
     sent1, got0 = lax.optimization_barrier((sent1, got0))
     got1 = exchange(sent1).reshape(LENGTH, 128)
 
-    column = jnp.arange(128)
-    turned = jnp.arange(LENGTH, dtype=f32)[:, None] * inverse_frequency(column % 16)[None, :]
-    cosine = jnp.cos(turned)
-    sine = jnp.sin(turned)
-    table = jnp.where(column < 32, cosine, jnp.where(column < 64, sine, 0.0))
-    swap, spread = rope_tables()
-
-    raw = got0[:, 128:256]
-    swapped = jnp.dot(raw, jnp.asarray(swap, bf16), preferred_element_type=f32)
-    rotated = (raw.astype(f32) * cosine + swapped * sine).astype(bf16)
-    apart = jnp.dot(rotated, jnp.asarray(spread, bf16), preferred_element_type=f32).astype(bf16)
-    q2_0, q2_1, k2 = apart[:, 0:128], apart[:, 128:256], apart[:, 256:384]
-
+    ropes = jnp.dot(
+        got0[:, 128:256], jnp.asarray(rope_table(), bf16), preferred_element_type=f32
+    ).astype(bf16)
     kv = lax.dot_general(
         nlat_full, w_own, (((1,), (1,)), ((), ())), preferred_element_type=f32
     ).astype(bf16)
@@ -490,31 +516,28 @@
         arrived = lax.psum_scatter(pieces, DP, scatter_dimension=0, tiled=True)[0]
         return arrived, gain_part
 
-    grads0 = attention(got0[:, 0:128], q2_0, kv[:, 0:128], k2, table)
+    grads0 = attention(got0, kv, ropes, 0)
     grads0, got1 = lax.optimization_barrier((grads0, got1))
     ret0 = exchange(grads0.reshape(SP_SIZE, TOKENS, 256))
     arrived0, gain0 = weight_part(grads0, 0)
-    grads1 = attention(got1, q2_1, kv[:, 128:256], k2, table)
+    grads1 = attention(got1, kv, ropes, 1)
     grads1, ret0 = lax.optimization_barrier((grads1, ret0))
     ret1 = exchange(grads1.reshape(SP_SIZE, TOKENS, 256))
     arrived1, gain1 = weight_part(grads1, 1)
     piece = jnp.concatenate([arrived0, arrived1], axis=0)
     moved = lax.ppermute(piece, SP_DP, [(b, a) for a, b in to_heads()])
-    gain_grad = lax.psum((gain0 + gain1) / latent_norm_gain, SP_DP)
+    gain_grad = functools.reduce(lax.psum, SP_DP, (gain0 + gain1) / latent_norm_gain)
     (blocks,) = spread_over_sp(moved, None, 1)
 
     query_grad, latent_grad, rope_sum = finish(
-        ret0, ret1, w_whole, latent[0], latent_norm_gain[None]
+        ret0, ret1, w_whole, latent[0], latent_norm_gain[None], wide_cos, wide_sin, cosine, sine
     )
-    position = (spot * TOKENS + jnp.arange(TOKENS)).astype(f32)
-    angle = position[:, None] * inverse_frequency(jnp.arange(16))[None, :]
-    rope_grad = rotate(rope_sum[:, 96:128], jnp.cos(angle), -jnp.sin(angle))
     blocks = blocks.reshape(2, DP_SIZE, 2, 2, 8, LATENT).transpose(3, 0, 2, 1, 4, 5)
     blocks = blocks.reshape(2, 256, LATENT)
     return (
         query_grad[None],
         latent_grad[None],
-        rope_grad[None],
+        rope_sum[None, :, 96:128],
         blocks[0],
         blocks[1],
         gain_grad,

time: 381 us -> 326 us (0.86)
  blocking collectives: 71.6 us -> 35.9 us
  Pallas kernels: 188 us -> 178 us
  other arithmetic: 12.1 us -> 6.39 us
  matrix products: 19.3 us -> 15.2 us
    psum x1 -> x4, blocking collectives: 71.6 us -> 35.9 us  [layer(): functools.reduce(lax.psum, SP_DP, (gain0 + gain1) / latent_norm_gain)]
    pallas_call x2, Pallas kernels: 109 us -> 97.8 us  [spread_over_sp(): pl.pallas_call(functools.partial(spread_kernel, with_messages), in_specs=...]
    select_n x1, other arithmetic: 6.75 us -> 0.02 us  [layer(): jnp.where(place < 64, 0.0, inverse_frequency(place % 16))[None]]
    dot_general x1, matrix products: 8.07 us -> 2.21 us  [layer(): jnp.dot(got0[:, 128:256], jnp.asarray(rope_table(), bf16), preferred_elem...]
  transfers between devices with their start and end apart: 8 -> 8, of which waited for: 1 -> 1; matrix products, arithmetic and copies ran while one was open for 10% -> 8% of each run, Pallas kernels for 47% -> 51%
where the time goes in v3:
time: 326 us; the launch traced here: 325 us
  Pallas kernels  178 us (55%)
  blocking collectives  35.9 us (11%)
  starting transfers between devices  34 us (10%)
  waiting for transfers between devices  29.6 us (9%)
  matrix products  15.2 us (5%)
  between operations  14 us (4%)
  local copies, waits for them, and re-layouts  11.9 us (4%)
  other arithmetic  6.39 us (2%)
    pallas_call x2, Pallas kernels, spread_over_sp(): pl.pallas_call(functools.partial(spread_kernel, with_messages), in_specs=...  97.8 us
    pallas_call x2, Pallas kernels, attention(): pl.pallas_call(attention_kernel, grid=(count,), in_specs=[column(0), colu...  61.4 us
    psum x4, blocking collectives, layer(): functools.reduce(lax.psum, SP_DP, (gain0 + gain1) / latent_norm_gain)  35.9 us
    reduce_scatter x2, waiting for transfers between devices, weight_part(): arrived = lax.psum_scatter(pieces, DP, scatter_dimension=0, tiled=True)[0]  28.8 us
    all_to_all x3, starting transfers between devices, exchange(): return lax.all_to_all(value, SP, split_axis=0, concat_axis=0, tiled=True)  27.8 us
    pallas_call x1, Pallas kernels, finish(): pl.pallas_call(finish_kernel, grid=(8,), in_specs=[pl.BlockSpec((2, TOKEN...  10.9 us
    dot_general x2, matrix products, weight_part(): lax.dot_general(grads[:, 128:256], nlat_full, (((0,), (0,)), ((), ())), p...  8.28 us
    pallas_call x1, Pallas kernels, pack(): pl.pallas_call(pack_kernel, grid=(8,), in_specs=[pl.BlockSpec((TOKENS, 38...  7.74 us
  transfers between devices with their start and end apart: 8, of which 1 were waited for; matrix products, arithmetic and copies ran while one was open for 8% of the time, Pallas kernels for 51%

profile of v3, /device:TPU:0, one launch (start us, length us, event | category | flops | bytes accessed | tf_op | source)
XLA Modules:
  0.0 324.7 jit_solution(3799348824926222415)
XLA Ops:
  7.2 1.3 pad_maximum_fusion
  9.5 5.3 %collective-permute-start = (bf16[256,1024]{1,0:T(8,128)(2,1)}, bf16[256,1024]{1,0:T(8,128)(2,1)}, u32[]{:S(2)}, u32[]{:S(2)}) collective-permute-start(bf16[256,1024]{1,0:T(8,128)(2,1)} %dynamic-slice_bitcast_fusion), channel_id=1, source_target_pairs={{0,0},{64,8},{8,1},{72,9},{16,2},{80,10},{24,3},{88,11},{32,4},{96... | collective-permute-start | bytes 1572872 | tf_op jit(solution)/shard_map/ppermute | solution.py:480
  17.8 7.7 %pack.1 = (bf16[16,192,256]{2,1,0:T(8,128)(2,1)}, bf16[16,192,128]{2,1,0:T(8,128)(2,1)}) custom-call(bf16[192,3072]{1,0:T(8,128)(2,1)} %bitcast.71, bf16[192,2048]{1,0:T(8,128)(2,1)} %bitcast.72, bf16[192,128]{1,0:T(8,128)(2,1)} %pad.4.rope, bf16[768,512]{1,0:T(8,128)(2,1)} %constant.101.clone.first, bf16[768,256]{1,0:T(8,128)(2,1)} %constant.102.clone.second, ...), custom_call_target="tpu_custom_call" | custom-call | flops 1811939328 | bytes 5000000 | tf_op jit(solution)/shard_map/pack/pallas_call | solution.py:93
  25.6 75.6 %spread.2 = (bf16[16,192,1024]{2,1,0:T(8,128)(2,1)}, bf16[16,192,256]{2,1,0:T(8,128)(2,1)}) custom-call(bf16[192,1024]{1,0:T(8,128)(2,1)} %fusion.2.refs_0_, bf16[16,192,256]{2,1,0:T(8,128)(2,1)} %get-tuple-element.20.refs_1_), custom_call_target="tpu_custom_call" | custom-call | flops 8000000000 | bytes 8000000 | tf_op jit(solution)/shard_map/spread/pallas_call | solution.py:451
  101.2 13.4 %all-to-all-start = ((bf16[16,192,128]{2,1,0:T(8,128)(2,1)}), bf16[16,192,128]{2,1,0:T(8,128)(2,1)S(1)}, u32[]{:S(2)}, u32[]{:S(2)}) async-start(bf16[16,192,128]{2,1,0:T(8,128)(2,1)} %get-tuple-element.24), calls=%async_computation | async-start | bytes 1572864 | tf_op jit(solution)/shard_map/all_to_all | solution.py:466
  114.6 2.2 convolution_convert_fusion.q2_ref.k2_ref
  116.8 4.7 %convolution_convert_fusion.1.kv_ref = bf16[3072,256]{1,0:T(8,128)(2,1)S(1)} fusion(bf16[3072,1024]{1,0:T(8,128)(2,1)} %bitcast.52, bf16[256,1024]{1,0:T(8,128)(2,1)} %collective-permute-done), kind=kOutput, calls=%fused_computation.1 | convolution fusion | flops 1611399168 | bytes 8388608 | tf_op jit(solution)/shard_map/dot_general | solution.py:501
  121.5 30.8 %attention.2 = bf16[3072,256]{1,0:T(8,128)(2,1)} custom-call(bf16[3072,256]{1,0:T(8,128)(2,1)S(1)} %bitcast.51, bf16[3072,384]{1,0:T(8,128)(2,1)} %convolution_convert_fusion.q2_ref.k2_ref, bf16[3072,256]{1,0:T(8,128)(2,1)S(1)} %convolution_convert_fusion.1.kv_ref, bf16[3072,384]{1,0:T(8,128)(2,1)} %convolution_convert_fusion.q2_ref.k2_ref), custom_call_target="tpu_custom_call" | custom-call | flops 12000000000 | bytes 8000000 | tf_op jit(solution)/shard_map/attention/pallas_call | solution.py:215
  152.3 1.2 copy-done.1
  153.5 7.3 %all-to-all-start.1 = ((bf16[16,192,256]{2,1,0:T(8,128)(2,1)}), bf16[16,192,256]{2,1,0:T(8,128)(2,1)}, u32[]{:S(2)}, u32[]{:S(2)}) async-start(bf16[16,192,256]{2,1,0:T(8,128)(2,1)} %bitcast.13), calls=%async_computation.1 | async-start | bytes 3145728 | tf_op jit(solution)/shard_map/all_to_all | solution.py:466
  160.8 4.1 %fusion.5 = f32[128,1024]{1,0:T(8,128)S(1)} fusion(bf16[3072,1024]{1,0:T(8,128)(2,1)} %bitcast.53, bf16[3072,256]{1,0:T(8,128)(2,1)} %attention.2), kind=kOutput, calls=%fused_computation.10 | convolution fusion | flops 805306368 | bytes 7602176 | tf_op jit(solution)/shard_map/dot_general | solution.py:506
  165.9 30.6 %attention.3 = bf16[3072,256]{1,0:T(8,128)(2,1)} custom-call(bf16[3072,128]{1,0:T(8,128)(2,1)S(1)} %bitcast.49, bf16[3072,384]{1,0:T(8,128)(2,1)} %convolution_convert_fusion.q2_ref.k2_ref, bf16[3072,256]{1,0:T(8,128)(2,1)S(1)} %copy-done.2, bf16[3072,384]{1,0:T(8,128)(2,1)} %convolution_convert_fusion.q2_ref.k2_ref), custom_call_target="tpu_custom_call" | custom-call | flops 12000000000 | bytes 8000000 | tf_op jit(solution)/shard_map/attention/pallas_call | solution.py:215
  196.5 4.1 %multiply_reduce_fusion = (f32[1024]{0:T(1024)S(1)}, f32[1024]{0:T(1024)S(1)}, f32[128,1024]{1,0:T(8,128)S(1)}) fusion(bf16[256,1024]{1,0:T(8,128)(2,1)} %collective-permute-done, f32[128,1024]{1,0:T(8,128)S(1)} %fusion.5, bf16[3072,1024]{1,0:T(8,128)(2,1)} %bitcast.54, bf16[3072,256]{1,0:T(8,128)(2,1)} %attention.3), kind=kOutput, calls=%fused_computation.15 | convolution fusion | flops 806090752 | bytes 8658944 | tf_op jit(solution)/shard_map/dot_general | solution.py:506
  202.3 7.2 %all-to-all-start.2 = ((bf16[16,192,256]{2,1,0:T(8,128)(2,1)}), bf16[16,192,256]{2,1,0:T(8,128)(2,1)S(1)}, u32[]{:S(2)}, u32[]{:S(2)}) async-start(bf16[16,192,256]{2,1,0:T(8,128)(2,1)} %bitcast.14), calls=%async_computation.2 | async-start | bytes 3145728 | tf_op jit(solution)/shard_map/all_to_all | solution.py:466
  209.5 1.9 multiply_sine_fusion
  211.4 28.8 %reduce-scatter.5.cloned.1.call-done = f32[1,16,1024]{2,1,0:T(8,128)} async-done(((f32[8,16,1024]{2,1,0:T(8,128)}), f32[1,16,1024]{2,1,0:T(8,128)}) %reduce-scatter.5.cloned.1.call-update) | async-done | bytes 65552 | tf_op jit(solution)/shard_map/reduce_scatter | solution.py:516
  241.8 11.8 %psum.28 = f32[1024]{0:T(1024)S(1)} all-reduce(f32[1024]{0:T(1024)S(1)} %add_divide_fusion), channel_id=1, replica_groups=mesh['sp_0'=4,'sp_1'=4,'dp_0'=4,'dp_1'=2] {'sp_0'}, use_global_device_ids=true, to_apply=%region_5.6 | all-reduce | flops 1024 | bytes 8192 | tf_op jit(solution)/shard_map/psum | solution.py:529
  253.6 11.2 %psum.29 = f32[1024]{0:T(1024)S(1)} all-reduce(f32[1024]{0:T(1024)S(1)} %psum.28), channel_id=1, replica_groups=mesh['sp_0'=4,'sp_1'=4,'dp_0'=4,'dp_1'=2] {'sp_1'}, use_global_device_ids=true, to_apply=%region_6.7 | all-reduce | flops 1024 | bytes 8192 | tf_op jit(solution)/shard_map/psum | solution.py:529
  264.8 9.9 %psum.30 = f32[1024]{0:T(1024)S(1)} all-reduce(f32[1024]{0:T(1024)S(1)} %psum.29), channel_id=1, replica_groups=mesh['sp_0'=4,'sp_1'=4,'dp_0'=4,'dp_1'=2] {'dp_0'}, use_global_device_ids=true, to_apply=%region_7.8 | all-reduce | flops 1024 | bytes 8192 | tf_op jit(solution)/shard_map/psum | solution.py:529
  274.6 3.0 psum.31
  278.3 22.2 %spread.3 = f32[16,32,1024]{2,1,0:T(8,128)} custom-call(f32[32,1024]{1,0:T(8,128)} %copy-done.9), custom_call_target="tpu_custom_call" | custom-call | flops 8000000000 | bytes 8000000 | tf_op jit(solution)/shard_map/spread/pallas_call | solution.py:451
  300.6 1.7 fusion.22
  304.3 1.2 copy-done.4
  305.5 10.9 %finish.1 = (bf16[192,3072]{1,0:T(8,128)(2,1)}, f32[192,1024]{1,0:T(8,128)}, f32[192,128]{1,0:T(8,128)}) custom-call(bf16[16,192,256]{2,1,0:T(8,128)(2,1)} %all-to-all-done.1.ret0, bf16[16,192,256]{2,1,0:T(8,128)(2,1)} %copy-done.4, bf16[16,256,1024]{2,1,0:T(8,128)(2,1)} %all-gather.2.cloned.1.call-done.w, bf16[512,384]{1,0:T(8,128)(2,1)} %constant.104.clone.place, ...), custom_call_target="tpu_custom_call" | custom-call | flops 4000000000 | bytes 14000000 | tf_op jit(solution)/shard_map/finish/pallas_call | solution.py:279
  (50 shorter events, 12.4 us)
Async XLA Ops:
  7.2 7.7 %copy-start.8 = (bf16[1,192,32]{1,2,0:T(8,128)(2,1)S(1)}, bf16[1,192,32]{1,2,0:T(8,128)(2,1)}, u32[]{:S(2)}) copy-start(bf16[1,192,32]{1,2,0:T(8,128)(2,1)} %param.14) | copy-start | bytes 36868
  7.2 7.8 %copy-start.5 = (bf16[1,192,1024]{2,1,0:T(8,128)(2,1)S(1)}, bf16[1,192,1024]{2,1,0:T(8,128)(2,1)}, u32[]{:S(2)}) copy-start(bf16[1,192,1024]{2,1,0:T(8,128)(2,1)} %param.13) | copy-start | bytes 1179652
  7.2 9.7 %copy-start.7 = (f32[1024]{0:T(1024)S(1)}, f32[1024]{0:T(1024)}, u32[]{:S(2)}) copy-start(f32[1024]{0:T(1024)} %param.15) | copy-start | bytes 12292
  8.6 17.0 %copy-start.3 = (bf16[2,2,2,64,1024]{4,3,2,1,0:T(8,128)(2,1)}, bf16[2,2,2,64,1024]{4,3,2,1,0:T(8,128)(2,1)S(1)}, u32[]{:S(2)}) copy-start(bf16[2,2,2,64,1024]{4,3,2,1,0:T(8,128)(2,1)S(1)} %pad_maximum_fusion) | copy-start | bytes 3145732
  9.5 107.3 %collective-permute-start = (bf16[256,1024]{1,0:T(8,128)(2,1)}, bf16[256,1024]{1,0:T(8,128)(2,1)}, u32[]{:S(2)}, u32[]{:S(2)}) collective-permute-start(bf16[256,1024]{1,0:T(8,128)(2,1)} %dynamic-slice_bitcast_fusion), channel_id=1, source_target_pairs={{0,0},{64,8},{8,1},{72,9},{16,2},{80,10},{24,3},{88,11},{32,4},{96... | collective-permute-start | bytes 1572872 | tf_op jit(solution)/shard_map/ppermute | solution.py:480
  25.5 89.0 %copy-start.6 = (bf16[128,384]{1,0:T(8,128)(2,1)S(1)}, bf16[128,384]{1,0:T(8,128)(2,1)}, u32[]{:S(2)}) copy-start(bf16[128,384]{1,0:T(8,128)(2,1)} %constant.103.clone) | copy-start | bytes 294916
  101.2 13.4 %copy-start = (bf16[16,192,256]{2,1,0:T(8,128)(2,1)S(1)}, bf16[16,192,256]{2,1,0:T(8,128)(2,1)}, u32[]{:S(2)}) copy-start(bf16[16,192,256]{2,1,0:T(8,128)(2,1)} %get-tuple-element.21) | copy-start | bytes 4718596
  101.2 52.3 %all-to-all-start = ((bf16[16,192,128]{2,1,0:T(8,128)(2,1)}), bf16[16,192,128]{2,1,0:T(8,128)(2,1)S(1)}, u32[]{:S(2)}, u32[]{:S(2)}) async-start(bf16[16,192,128]{2,1,0:T(8,128)(2,1)} %get-tuple-element.24), calls=%async_computation | async-start | bytes 1572864 | tf_op jit(solution)/shard_map/all_to_all | solution.py:466
  152.3 1.2 copy-start.1
  153.5 43.0 %all-to-all-start.1 = ((bf16[16,192,256]{2,1,0:T(8,128)(2,1)}), bf16[16,192,256]{2,1,0:T(8,128)(2,1)}, u32[]{:S(2)}, u32[]{:S(2)}) async-start(bf16[16,192,256]{2,1,0:T(8,128)(2,1)} %bitcast.13), calls=%async_computation.1 | async-start | bytes 3145728 | tf_op jit(solution)/shard_map/all_to_all | solution.py:466
  160.7 5.1 %copy-start.2 = (bf16[3072,256]{1,0:T(8,128)(2,1)S(1)}, bf16[3072,256]{1,0:T(8,128)(2,1)}, u32[]{:S(2)}) copy-start(bf16[3072,256]{1,0:T(8,128)(2,1)} %copy-done.1) | copy-start | bytes 4718596
  160.8 50.7 %reduce-scatter.3.cloned.1.call-start = ((), (), s32[]{:S(2)}) async-start(), calls=%async_computation.6 | async-start | bytes 589824 | tf_op jit(solution)/shard_map/reduce_scatter | solution.py:516
  165.8 74.4 %reduce-scatter.5.cloned.1.call-start = ((), (), s32[]{:S(2)}) async-start(), calls=%async_computation.7 | async-start | bytes 589824 | tf_op jit(solution)/shard_map/reduce_scatter | solution.py:516
  201.5 102.8 %all-gather.2.cloned.1.call-start = ((), (), s32[]{:S(2)}) async-start(), calls=%async_computation.5 | async-start | bytes 9437184 | tf_op jit(solution)/shard_map/all_gather | solution.py:481
  202.3 102.1 %all-to-all-start.2 = ((bf16[16,192,256]{2,1,0:T(8,128)(2,1)}), bf16[16,192,256]{2,1,0:T(8,128)(2,1)S(1)}, u32[]{:S(2)}, u32[]{:S(2)}) async-start(bf16[16,192,256]{2,1,0:T(8,128)(2,1)} %bitcast.14), calls=%async_computation.2 | async-start | bytes 3145728 | tf_op jit(solution)/shard_map/all_to_all | solution.py:466
  241.1 36.5 %collective-permute-start.1 = (f32[32,1024]{1,0:T(8,128)S(1)}, f32[32,1024]{1,0:T(8,128)S(1)}, u32[]{:S(2)}, u32[]{:S(2)}) collective-permute-start(f32[32,1024]{1,0:T(8,128)S(1)} %pad_maximum_fusion.1), channel_id=1, source_target_pairs={{0,0},{8,64},{1,8},{9,72},{2,16},{10,80},{3,24},{11,88},{4,32},{12... | collective-permute-start | bytes 393224 | tf_op jit(solution)/shard_map/ppermute | solution.py:528
  277.7 0.7 copy-start.9
  304.3 1.2 copy-start.4
Sparse Core Ops, SparseCore 0:
  165.9 38.2 reduce-scatter.2
  207.2 32.9 reduce-scatter.4
  242.5 48.6 all-gather.1

commit v4 on v3

--- a/solution.py
+++ b/solution.py
@@ -76,15 +76,15 @@
     return jnp.where(lane % 32 < 16, -pltpu.roll(x, 112, 1), pltpu.roll(x, 16, 1))
 
 
-def pack_kernel(query, d_out, rope, first, second, cosine, sine, out0, out1):
+def pack_kernel(query, d_out, rope, first, second, cosine, sine, out):
     both = jnp.concatenate([query[...], d_out[...], rope[...]], axis=1)
     one = jnp.dot(both, first[...], preferred_element_type=f32)
     two = jnp.dot(both, second[...], preferred_element_type=f32).astype(bf16)
     for t in range(2):
-        out0[t, :, 0:128] = one[:, 256 * t : 256 * t + 128].astype(bf16)
+        out[t, :, 0:128] = one[:, 256 * t : 256 * t + 128].astype(bf16)
         raw = one[:, 256 * t + 128 : 256 * t + 256]
-        out0[t, :, 128:256] = (raw * cosine[...] + turned_halves(raw) * sine[...]).astype(bf16)
-        out1[t] = two[:, 128 * t : 128 * t + 128]
+        out[t, :, 128:256] = (raw * cosine[...] + turned_halves(raw) * sine[...]).astype(bf16)
+        out[t, :, 256:384] = two[:, 128 * t : 128 * t + 128]
 
 
 def pack(query, d_out, rope, cosine, sine):
@@ -102,14 +102,8 @@
             whole((TOKENS, 128)),
             whole((TOKENS, 128)),
         ],
-        out_specs=[
-            pl.BlockSpec((2, TOKENS, 256), lambda j: (j, 0, 0)),
-            pl.BlockSpec((2, TOKENS, 128), lambda j: (j, 0, 0)),
-        ],
-        out_shape=[
-            jax.ShapeDtypeStruct((SP_SIZE, TOKENS, 256), bf16),
-            jax.ShapeDtypeStruct((SP_SIZE, TOKENS, 128), bf16),
-        ],
+        out_specs=pl.BlockSpec((2, TOKENS, 384), lambda j: (j, 0, 0)),
+        out_shape=jax.ShapeDtypeStruct((SP_SIZE, TOKENS, 384), bf16),
         cost_estimate=pl.CostEstimate(
             flops=16 * 192 * 768 * 768, bytes_accessed=5_000_000, transcendentals=0
         ),
@@ -215,7 +209,7 @@
     return pl.pallas_call(
         attention_kernel,
         grid=(count,),
-        in_specs=[column(0), column(head), column(head), column(2)],
+        in_specs=[column(2 * head), column(head), column(head), column(2)],
         out_specs=pl.BlockSpec((BLOCK, 256), lambda i: (count - 1 - i, 0)),
         out_shape=jax.ShapeDtypeStruct((LENGTH, 256), bf16),
         scratch_shapes=[
@@ -327,139 +321,239 @@
     return pairs
 
 
-def spread_kernel(with_messages, *refs):
-    count = 2 if with_messages else 1
-    x, full = refs[0], refs[count]
-    own_sem, leg, leg_in, pass1, pass1_in, far, far_in, pass2, pass2_in = refs[2 * count : 2 * count + 9]
-    if with_messages:
-        msgs, got = refs[1], refs[3]
-        msg_send, msg_recv = refs[2 * count + 9 :]
+def place():
     z, y = lax.axis_index("sp_0"), lax.axis_index("sp_1")
+    x, core = lax.axis_index("dp_0"), lax.axis_index("dp_1")
+    return z, y, x, core
+
+
+def on_sp(dz, dy):
+    z, y, _, _ = place()
+    return {"sp_0": lax.rem(z + dz, 4), "sp_1": lax.rem(y + dy, 4)}
+
+
+def on_dp(dx, dcore):
+    _, _, x, core = place()
+    return {"dp_0": lax.rem(x + dx, 4), "dp_1": lax.rem(core + dcore, 2)}
+
+
+SP_PEERS = [(k // 4, k % 4) for k in range(1, SP_SIZE)]
+DP_PEERS = [(k // 2, k % 2) for k in range(1, DP_SIZE)]
+NEAR = [(0, 1), (0, 3), (1, 0), (3, 0)]
+X_PEERS = [(1, 0), (3, 0), (0, 1)]
+
+
+def meet(sp_peers, dp_peers):
+    barrier = pltpu.get_barrier_semaphore()
+    for where in [on_sp(*p) for p in sp_peers] + [on_dp(*p) for p in dp_peers]:
+        pl.semaphore_signal(
+            barrier, inc=1, device_id=where, device_id_type=pl.DeviceIdType.MESH
+        )
+    pl.semaphore_wait(barrier, len(sp_peers) + len(dp_peers))
+
+
+def copy_to(src, dst, send, recv, where):
+    c = pltpu.make_async_remote_copy(
+        src_ref=src,
+        dst_ref=dst,
+        send_sem=send,
+        recv_sem=recv,
+        device_id=where,
+        device_id_type=pl.DeviceIdType.MESH,
+    )
+    c.start()
+    return c
+
+
+def keep(src, dst, sem):
+    c = pltpu.make_async_copy(src, dst, sem)
+    c.start()
+    return c
+
+
+def send_over_sp(block_for, got, send, recv):
+    z, y, _, _ = place()
+    sent = []
+    for k, (dz, dy) in enumerate(SP_PEERS):
+        there = 4 * lax.rem(z + dz, 4) + lax.rem(y + dy, 4)
+        sent.append(
+            copy_to(block_for(there), got.at[4 * z + y], send.at[k], recv.at[k], on_sp(dz, dy))
+        )
+    return sent
+
+
+def send_over_dp(block_for, got, send, recv):
+    _, _, x, core = place()
+    sent = []
+    for k, (dx, dcore) in enumerate(DP_PEERS):
+        there = 2 * lax.rem(x + dx, 4) + lax.rem(core + dcore, 2)
+        sent.append(
+            copy_to(block_for(there), got.at[2 * x + core], send.at[k], recv.at[k], on_dp(dx, dcore))
+        )
+    return sent
+
+
+def gather_over_sp(x, full, sems, between, midway=lambda: None):
+    leg, leg_in, pass1, pass1_in, far, far_in, pass2, pass2_in = sems
+    z, y, _, _ = place()
     me = 4 * z + y
     size = x.shape[0] // 2
 
-    def at(dz, dy):
-        return {"sp_0": lax.rem(z + dz, 4), "sp_1": lax.rem(y + dy, 4)}
-
     def along(h, s):
-        return at(0, s) if h == 0 else at(s, 0)
+        return on_sp(0, s) if h == 0 else on_sp(s, 0)
 
     def across(h, s):
-        return at(s, 0) if h == 0 else at(0, s)
+        return on_sp(s, 0) if h == 0 else on_sp(0, s)
 
     def block(h, s, c):
         dz, dy = (c, s) if h == 0 else (s, c)
         return 4 * lax.rem(z + dz, 4) + lax.rem(y + dy, 4)
-
-    if with_messages:
-        peers = [(k // 4, k % 4) for k in range(1, SP_SIZE)]
-    else:
-        peers = [(0, 1), (0, 3), (1, 0), (3, 0)]
-    barrier = pltpu.get_barrier_semaphore()
-    for dz, dy in peers:
-        pl.semaphore_signal(
-            barrier, inc=1, device_id=at(dz, dy), device_id_type=pl.DeviceIdType.MESH
-        )
-    pl.semaphore_wait(barrier, len(peers))
-
-    def copy(src, dst, send, recv, where):
-        c = pltpu.make_async_remote_copy(
-            src_ref=src,
-            dst_ref=dst,
-            send_sem=send,
-            recv_sem=recv,
-            device_id=where,
-            device_id_type=pl.DeviceIdType.MESH,
-        )
-        c.start()
-        return c
 
     half = [pl.ds(h * size, size) for h in range(2)]
     quarter = [[pl.ds(h * size + q * size // 2, size // 2) for q in range(2)] for h in range(2)]
     ways = (1, 3)
     lines = (0, 3, 1, 2)
-    first, second, third, fourth, rest = {}, {}, {}, {}, []
+    first, second, third, fourth = {}, {}, {}, {}
     for w, s in enumerate(ways):
         for h in range(2):
-            first[h, w] = copy(
+            first[h, w] = copy_to(
                 x.at[half[h]], full.at[me, half[h]], leg.at[h, w], leg_in.at[h, w], along(h, s)
             )
     for w, s in enumerate(ways):
         for h in range(2):
-            third[h, 0, w] = copy(
+            third[h, 0, w] = copy_to(
                 x.at[half[h]], full.at[me, half[h]], far.at[h, 0, w], far_in.at[h, 0, w], across(h, s)
             )
-    own = [pltpu.make_async_copy(x, full.at[me], own_sem.at[0])]
-    if with_messages:
-        own.append(pltpu.make_async_copy(msgs.at[me], got.at[me], own_sem.at[1]))
-    for c in own:
-        c.start()
-    if with_messages:
-        for k, (dz, dy) in enumerate(peers):
-            rest.append(
-                copy(
-                    msgs.at[block(0, dy, dz)],
-                    got.at[me],
-                    msg_send.at[k],
-                    msg_recv.at[k],
-                    at(dz, dy),
-                )
-            )
+    rest = between()
 
     def onward(h, k):
         there = full.at[block(h, lines[k], 0), half[h]]
         for w, s in enumerate(ways):
-            third[h, k, w] = copy(there, there, far.at[h, k, w], far_in.at[h, k, w], across(h, s))
+            third[h, k, w] = copy_to(
+                there, there, far.at[h, k, w], far_in.at[h, k, w], across(h, s)
+            )
 
     for w, s in enumerate(ways):
         for h in range(2):
             first[h, w].wait_recv()
             piece = full.at[block(h, 4 - s, 0), quarter[h][w]]
-            second[h, w] = copy(piece, piece, pass1.at[h, w], pass1_in.at[h, w], along(h, s))
+            second[h, w] = copy_to(piece, piece, pass1.at[h, w], pass1_in.at[h, w], along(h, s))
             onward(h, w + 1)
     for h in range(2):
         for w in range(2):
             second[h, w].wait_recv()
         onward(h, 3)
     for k in range(4):
+        if k == 2:
+            midway()
         for w, s in enumerate(ways):
             for h in range(2):
                 third[h, k, w].wait_recv()
                 piece = full.at[block(h, lines[k], 4 - s), quarter[h][w]]
-                fourth[h, k, w] = copy(
+                fourth[h, k, w] = copy_to(
                     piece, piece, pass2.at[h, k, w], pass2_in.at[h, k, w], across(h, s)
                 )
     for group in (first, second, third):
         for c in group.values():
             c.wait_send()
-    for c in fourth.values():
+    for c in list(fourth.values()) + rest:
         c.wait()
-    for c in rest + own:
+
+
+def front_kernel(x, msgs, w, full, got, w_full, own_sem, *sems):
+    msg_send, msg_recv, ring, ring_in, pair, pair_in = sems[8:]
+    z, y, chip, core = place()
+    me = 4 * z + y
+    mine = 2 * chip + core
+    size = w.shape[0] // 2
+    meet(SP_PEERS, X_PEERS)
+    ways = (1, 3)
+    beside = {}
+
+    def to_partner(k, source, where):
+        beside[k] = copy_to(source, w_full.at[where], pair.at[k], pair_in.at[k], on_dp(0, 1))
+
+    out = [
+        copy_to(w, w_full.at[mine], ring.at[0, k], ring_in.at[0, k], on_dp(s, 0))
+        for k, s in enumerate(ways)
+    ]
+    to_partner(0, w, mine)
+
+    def between():
+        own = [
+            keep(x, full.at[me], own_sem.at[0]),
+            keep(msgs.at[me], got.at[me], own_sem.at[1]),
+            keep(w, w_full.at[mine], own_sem.at[2]),
+        ]
+        return own + send_over_sp(lambda there: msgs.at[there], got, msg_send, msg_recv)
+
+    def row(s):
+        return 2 * lax.rem(chip + s, 4) + core
+
+    passed = []
+
+    def midway():
+        for k, s in enumerate(ways):
+            out[k].wait_recv()
+            piece = w_full.at[row(4 - s), pl.ds(k * size, size)]
+            passed.append(copy_to(piece, piece, ring.at[1, k], ring_in.at[1, k], on_dp(s, 0)))
+            to_partner(1 + k, w_full.at[row(4 - s)], row(4 - s))
+
+    gather_over_sp(x, full, sems[:8], between, midway)
+    for c in passed:
+        c.wait_recv()
+    to_partner(3, w_full.at[row(2)], row(2))
+    for c in out + passed:
+        c.wait_send()
+    for c in beside.values():
         c.wait()
 
 
-def spread_over_sp(x, msgs, collective_id):
-    with_messages = msgs is not None
-    vmem = pl.BlockSpec(memory_space=pltpu.VMEM)
-    anywhere = pl.BlockSpec(memory_space=pl.ANY)
-    out_shape = [jax.ShapeDtypeStruct((SP_SIZE, *x.shape), x.dtype)]
+def tail_kernel(msgs, pieces, gain, got, arrived, gains, own_sem, *sems):
+    z, y, chip, core = place()
+    me = 4 * z + y
+    mine = 2 * chip + core
+    meet(SP_PEERS, DP_PEERS)
+    going = send_over_dp(lambda there: pieces.at[there], arrived, sems[0], sems[1])
+    going += send_over_sp(lambda there: gain, gains, sems[2], sems[3])
+    going += send_over_sp(lambda there: msgs.at[there], got, sems[4], sems[5])
+    going.append(keep(pieces.at[mine], arrived.at[mine], own_sem.at[0]))
+    going.append(keep(gain, gains.at[me], own_sem.at[1]))
+    going.append(keep(msgs.at[me], got.at[me], own_sem.at[2]))
+    for c in going:
+        c.wait()
+
+
+def last_kernel(x, gain, full, gains, own_sem, *sems):
+    z, y, chip, core = place()
+    meet(NEAR, DP_PEERS)
+
+    def between():
+        own = [
+            keep(x, full.at[4 * z + y], own_sem.at[0]),
+            keep(gain, gains.at[2 * chip + core], own_sem.at[1]),
+        ]
+        return own + send_over_dp(lambda there: gain, gains, sems[8], sems[9])
+
+    gather_over_sp(x, full, sems[:8], between)
+
+
+def moving(kernel, collective_id, operands, results, sem_shapes):
     dma = pltpu.SemaphoreType.DMA
-    scratch = [dma((2,))] + [dma((2, 2))] * 4 + [dma((2, 4, 2))] * 4
-    if with_messages:
-        out_shape.append(jax.ShapeDtypeStruct(msgs.shape, msgs.dtype))
-        scratch += [dma((SP_SIZE - 1,)), dma((SP_SIZE - 1,))]
     return pl.pallas_call(
-        functools.partial(spread_kernel, with_messages),
-        in_specs=[vmem] * (1 + with_messages),
-        out_specs=[anywhere] * (1 + with_messages),
-        out_shape=out_shape,
-        scratch_shapes=scratch,
+        kernel,
+        in_specs=[pl.BlockSpec(memory_space=pltpu.VMEM)] * len(operands),
+        out_specs=[pl.BlockSpec(memory_space=pl.ANY)] * len(results),
+        out_shape=[jax.ShapeDtypeStruct(shape, dtype) for shape, dtype in results],
+        scratch_shapes=[dma((3,))] + [dma(shape) for shape in sem_shapes for _ in range(2)],
         compiler_params=pltpu.CompilerParams(collective_id=collective_id, has_side_effects=True),
         cost_estimate=pl.CostEstimate(
             flops=8_000_000_000, bytes_accessed=8_000_000, transcendentals=0
         ),
-        name="spread",
-    )(*((x, msgs) if with_messages else (x,)))
+    )(*operands)
+
+
+GATHER_SEMS = [(2, 2), (2, 2), (2, 4, 2), (2, 4, 2)]
 
 
 def exchange(value):
@@ -478,7 +572,6 @@
     spot = lax.axis_index(SP)
     half = lax.dynamic_index_in_dim(shard, spot // 8, 0, keepdims=False)
     w_own = lax.ppermute(half, SP_DP, to_heads())
-    w_whole = lax.all_gather(shard, DP, axis=0, tiled=True)
 
     position = (spot * TOKENS + jnp.arange(TOKENS)).astype(f32)[:, None]
     angle = position * inverse_frequency(jnp.arange(128) % 16)[None]
@@ -488,15 +581,24 @@
     wide_cos, wide_sin = jnp.cos(wide), jnp.sin(wide)
 
     rope_wide = jnp.pad(rope_key[0], ((0, 0), (0, 96)))
-    sent0, sent1 = pack(query[0], out_grad[0], rope_wide, cosine, sine)
-    nlat_full, got0 = spread_over_sp(nlat, sent0, 0)
+    sent = pack(query[0], out_grad[0], rope_wide, cosine, sine)
+    nlat_full, got, w_whole = moving(
+        front_kernel,
+        0,
+        [nlat, sent, shard.reshape(512, LATENT)],
+        [
+            ((SP_SIZE, TOKENS, LATENT), bf16),
+            ((SP_SIZE, TOKENS, 384), bf16),
+            ((DP_SIZE, 512, LATENT), bf16),
+        ],
+        GATHER_SEMS + [(SP_SIZE - 1,), (2, 2), (4,)],
+    )
     nlat_full = nlat_full.reshape(LENGTH, LATENT)
-    got0 = got0.reshape(LENGTH, 256)
-    sent1, got0 = lax.optimization_barrier((sent1, got0))
-    got1 = exchange(sent1).reshape(LENGTH, 128)
+    got = got.reshape(LENGTH, 384)
+    w_whole = w_whole.reshape(SP_SIZE, 256, LATENT)
 
     ropes = jnp.dot(
-        got0[:, 128:256], jnp.asarray(rope_table(), bf16), preferred_element_type=f32
+        got[:, 128:256], jnp.asarray(rope_table(), bf16), preferred_element_type=f32
     ).astype(bf16)
     kv = lax.dot_general(
         nlat_full, w_own, (((1,), (1,)), ((), ())), preferred_element_type=f32
@@ -507,27 +609,39 @@
             grads[:, 128:256], nlat_full, (((0,), (0,)), ((), ())), preferred_element_type=f32
         )
         own = w_own[128 * h : 128 * h + 128].astype(f32)
-        gain_part = jnp.sum(d_w * own, axis=0)
         pieces = (
             d_w.reshape(2, DP_SIZE, 8, LATENT)
             .transpose(1, 0, 2, 3)
             .reshape(DP_SIZE, 16, LATENT)
         )
-        arrived = lax.psum_scatter(pieces, DP, scatter_dimension=0, tiled=True)[0]
-        return arrived, gain_part
-
-    grads0 = attention(got0, kv, ropes, 0)
-    grads0, got1 = lax.optimization_barrier((grads0, got1))
+        return pieces, jnp.sum(d_w * own, axis=0)
+
+    grads0 = attention(got, kv, ropes, 0)
     ret0 = exchange(grads0.reshape(SP_SIZE, TOKENS, 256))
-    arrived0, gain0 = weight_part(grads0, 0)
-    grads1 = attention(got1, kv, ropes, 1)
-    grads1, ret0 = lax.optimization_barrier((grads1, ret0))
-    ret1 = exchange(grads1.reshape(SP_SIZE, TOKENS, 256))
-    arrived1, gain1 = weight_part(grads1, 1)
-    piece = jnp.concatenate([arrived0, arrived1], axis=0)
-    moved = lax.ppermute(piece, SP_DP, [(b, a) for a, b in to_heads()])
-    gain_grad = functools.reduce(lax.psum, SP_DP, (gain0 + gain1) / latent_norm_gain)
-    (blocks,) = spread_over_sp(moved, None, 1)
+    pieces0, gain0 = weight_part(grads0, 0)
+    grads1 = attention(got, kv, ropes, 1)
+    pieces1, gain1 = weight_part(grads1, 1)
+    gain_part = ((gain0 + gain1) / latent_norm_gain).reshape(8, 128)
+    ret1, arrived, gains = moving(
+        tail_kernel,
+        1,
+        [
+            grads1.reshape(SP_SIZE, TOKENS, 256),
+            jnp.concatenate([pieces0, pieces1], axis=1),
+            gain_part,
+        ],
+        [((SP_SIZE, TOKENS, 256), bf16), ((DP_SIZE, 32, LATENT), f32), ((SP_SIZE, 8, 128), f32)],
+        [(DP_SIZE - 1,), (SP_SIZE - 1,), (SP_SIZE - 1,)],
+    )
+    moved = lax.ppermute(arrived.sum(axis=0), SP_DP, [(b, a) for a, b in to_heads()])
+    blocks, gains = moving(
+        last_kernel,
+        2,
+        [moved, gains.sum(axis=0)],
+        [((SP_SIZE, 32, LATENT), f32), ((DP_SIZE, 8, 128), f32)],
+        GATHER_SEMS + [(DP_SIZE - 1,)],
+    )
+    gain_grad = gains.sum(axis=0).reshape(LATENT)
 
     query_grad, latent_grad, rope_sum = finish(
         ret0, ret1, w_whole, latent[0], latent_norm_gain[None], wide_cos, wide_sin, cosine, sine

time: 326 us -> 296 us (0.908)
  Pallas kernels: 178 us -> 256 us
  blocking collectives: 35.9 us -> 0 us
  waiting for transfers between devices: 29.6 us -> 0.01 us
  starting transfers between devices: 34 us -> 5.97 us
  between operations: 14 us -> 0.92 us
  local copies, waits for them, and re-layouts: 11.9 us -> 7 us
  other arithmetic: 6.39 us -> 10.5 us
    pallas_call x4 -> x5, Pallas kernels: 159 us -> 237 us  [the longest x3 176 us: moving(): pl.pallas_call(kernel, in_specs=[pl.BlockSpec(memory_space=pltpu.VMEM)] *...]
    psum x4 -> x0, blocking collectives: 35.9 us -> none  [layer(): functools.reduce(lax.psum, SP_DP, (gain0 + gain1) / latent_norm_gain)]
    reduce_scatter x2 -> x0, waiting for transfers between devices: 28.8 us -> none  [weight_part(): arrived = lax.psum_scatter(pieces, DP, scatter_dimension=0, tiled=True)[0]]
    all_to_all x3 -> x1, starting transfers between devices: 27.8 us -> 4.6 us  [exchange(): return lax.all_to_all(value, SP, split_axis=0, concat_axis=0, tiled=True)]
    ppermute x1, starting transfers between devices: 5.35 us -> 0.69 us  [layer(): w_own = lax.ppermute(half, SP_DP, to_heads())]
    reduce_sum x0 -> x3, other arithmetic: none -> 3.34 us  [the longest x1 1.45 us: layer(): gains.sum(axis=0)]
  transfers between devices with their start and end apart: 8 -> 3, of which waited for: 1 -> 0; matrix products, arithmetic and copies ran while one was open for 8% -> 7% of each run, Pallas kernels for 51% -> 62%
where the time goes in v4:
time: 296 us; the launch traced here: 295 us
  Pallas kernels  256 us (86%)
  matrix products  14.6 us (5%)
  other arithmetic  10.5 us (4%)
  local copies, waits for them, and re-layouts  7 us (2%)
  starting transfers between devices  5.97 us (2%)
    pallas_call x3, Pallas kernels, moving(): pl.pallas_call(kernel, in_specs=[pl.BlockSpec(memory_space=pltpu.VMEM)] *...  176 us
    pallas_call x2, Pallas kernels, attention(): pl.pallas_call(attention_kernel, grid=(count,), in_specs=[column(2 * head...  61 us
    pallas_call x1, Pallas kernels, finish(): pl.pallas_call(finish_kernel, grid=(8,), in_specs=[pl.BlockSpec((2, TOKEN...  10.9 us
    pallas_call x1, Pallas kernels, pack(): pl.pallas_call(pack_kernel, grid=(8,), in_specs=[pl.BlockSpec((TOKENS, 38...  7.9 us
    dot_general x2, matrix products, weight_part(): lax.dot_general(grads[:, 128:256], nlat_full, (((0,), (0,)), ((), ())), p...  6.55 us
  transfers between devices with their start and end apart: 3, of which 0 were waited for; matrix products, arithmetic and copies ran while one was open for 7% of the time, Pallas kernels for 62%

profile of v4, /device:TPU:0, one launch (start us, length us, event | category | flops | bytes accessed | tf_op | source)
XLA Modules:
  0.0 295.0 jit_solution(13845181233466019406)
XLA Ops:
  0.7 1.3 pad_maximum_fusion
  3.1 1.1 multiply_sine_fusion.1
  4.9 0.9 fusion.2.x
  5.8 7.9 %pack.1.msgs = bf16[16,192,384]{2,1,0:T(8,128)(2,1)} custom-call(bf16[192,3072]{1,0:T(8,128)(2,1)} %bitcast.71, bf16[192,2048]{1,0:T(8,128)(2,1)} %bitcast.72, bf16[192,128]{1,0:T(8,128)(2,1)} %pad.4.rope, bf16[768,512]{1,0:T(8,128)(2,1)} %constant.101.clone.first, bf16[768,256]{1,0:T(8,128)(2,1)} %constant.102.clone.second, ...), custom_call_target="tpu_custom_call" | custom-call | flops 1811939328 | bytes 5000000 | tf_op jit(solution)/shard_map/pack/pallas_call | solution.py:93
  13.7 104.5 %shard_map.163 = (bf16[16,192,1024]{2,1,0:T(8,128)(2,1)}, bf16[16,192,384]{2,1,0:T(8,128)(2,1)}, bf16[8,512,1024]{2,1,0:T(8,128)(2,1)}) custom-call(bf16[192,1024]{1,0:T(8,128)(2,1)} %fusion.2.x, bf16[16,192,384]{2,1,0:T(8,128)(2,1)} %pack.1.msgs, bf16[512,1024]{1,0:T(8,128)(2,1)} %bitcast.60), custom_call_target="tpu_custom_call" | custom-call | flops 8000000000 | bytes 8000000 | tf_op jit(solution)/shard_map/pallas_call | solution.py:543
  118.2 3.3 %convolution_convert_fusion.q2_ref.k2_ref = bf16[3072,384]{1,0:T(8,128)(2,1)} fusion(bf16[128,384]{1,0:T(8,128)(2,1)S(1)} %copy-done.4, bf16[3072,384]{1,0:T(8,128)(2,1)} %bitcast.50), kind=kOutput, calls=%fused_computation | convolution fusion | flops 303169536 | bytes 3244032 | tf_op jit(solution)/shard_map/dot_general | solution.py:600
  121.5 4.8 %convolution_convert_fusion.1.kv_ref = bf16[3072,256]{1,0:T(8,128)(2,1)S(1)} fusion(bf16[3072,1024]{1,0:T(8,128)(2,1)} %bitcast.53, bf16[256,1024]{1,0:T(8,128)(2,1)S(1)} %collective-permute-done), kind=kOutput, calls=%fused_computation.1 | convolution fusion | flops 1611399168 | bytes 8388608 | tf_op jit(solution)/shard_map/dot_general | solution.py:603
  126.3 30.9 %attention.2 = bf16[3072,256]{1,0:T(8,128)(2,1)} custom-call(bf16[3072,384]{1,0:T(8,128)(2,1)S(1)} %bitcast.51, bf16[3072,384]{1,0:T(8,128)(2,1)} %convolution_convert_fusion.q2_ref.k2_ref, bf16[3072,256]{1,0:T(8,128)(2,1)S(1)} %convolution_convert_fusion.1.kv_ref, bf16[3072,384]{1,0:T(8,128)(2,1)} %convolution_convert_fusion.q2_ref.k2_ref), custom_call_target="tpu_custom_call" | custom-call | flops 12000000000 | bytes 8000000 | tf_op jit(solution)/shard_map/attention/pallas_call | solution.py:209
  157.2 30.2 %attention.3 = bf16[3072,256]{1,0:T(8,128)(2,1)S(1)} custom-call(bf16[3072,384]{1,0:T(8,128)(2,1)S(1)} %bitcast.52, bf16[3072,384]{1,0:T(8,128)(2,1)} %convolution_convert_fusion.q2_ref.k2_ref, bf16[3072,256]{1,0:T(8,128)(2,1)S(1)} %convolution_convert_fusion.1.kv_ref, bf16[3072,384]{1,0:T(8,128)(2,1)} %convolution_convert_fusion.q2_ref.k2_ref), custom_call_target="tpu_custom_call" | custom-call | flops 12000000000 | bytes 8000000 | tf_op jit(solution)/shard_map/attention/pallas_call | solution.py:209
  187.4 2.7 fusion.5
  190.1 4.6 %all-to-all-start = ((bf16[16,192,256]{2,1,0:T(8,128)(2,1)}), bf16[16,192,256]{2,1,0:T(8,128)(2,1)}, u32[]{:S(2)}, u32[]{:S(2)}) async-start(bf16[16,192,256]{2,1,0:T(8,128)(2,1)} %bitcast.13), calls=%async_computation | async-start | bytes 3145728 | tf_op jit(solution)/shard_map/all_to_all | solution.py:560
  194.7 3.8 %multiply_reduce_fusion = (f32[1024]{0:T(1024)S(1)}, f32[1024]{0:T(1024)S(1)}, f32[128,1024]{1,0:T(8,128)S(1)}) fusion(bf16[256,1024]{1,0:T(8,128)(2,1)S(1)} %collective-permute-done, f32[128,1024]{1,0:T(8,128)S(1)} %fusion.5, bf16[3072,1024]{1,0:T(8,128)(2,1)} %bitcast.54, bf16[3072,256]{1,0:T(8,128)(2,1)S(1)} %attention.3), kind=kOutput, calls=%fused_computation.16 | convolution fusion | flops 806090752 | bytes 8658944 | tf_op jit(solution)/shard_map/dot_general | solution.py:608
  199.3 1.0 pad_maximum_fusion.1.pieces
  200.3 40.4 %shard_map.164 = (bf16[16,192,256]{2,1,0:T(8,128)(2,1)}, f32[8,32,1024]{2,1,0:T(8,128)}, f32[16,8,128]{2,1,0:T(8,128)}) custom-call(bf16[16,192,256]{2,1,0:T(8,128)(2,1)} %bitcast.49, f32[8,32,1024]{2,1,0:T(8,128)} %pad_maximum_fusion.1.pieces, f32[8,128]{1,0:T(8,128)} %divide_bitcast_fusion.gain), custom_call_target="tpu_custom_call" | custom-call | flops 8000000000 | bytes 8000000 | tf_op jit(solution)/shard_map/pallas_call | solution.py:543
  240.8 1.3 reduce_sum.57
  242.7 1.9 multiply_sine_fusion
  244.7 1.4 reduce_sum.58.gain
  246.8 31.3 %shard_map.165 = (f32[16,32,1024]{2,1,0:T(8,128)}, f32[8,8,128]{2,1,0:T(8,128)}) custom-call(f32[32,1024]{1,0:T(8,128)} %copy-done.8, f32[8,128]{1,0:T(8,128)} %reduce_sum.58.gain), custom_call_target="tpu_custom_call" | custom-call | flops 8000000000 | bytes 8000000 | tf_op jit(solution)/shard_map/pallas_call | solution.py:543
  278.0 1.7 fusion.22
  279.7 1.0 copy.23
  280.8 1.0 copy.24
  282.4 10.9 %finish.1 = (bf16[192,3072]{1,0:T(8,128)(2,1)}, f32[192,1024]{1,0:T(8,128)}, f32[192,128]{1,0:T(8,128)}) custom-call(bf16[16,192,256]{2,1,0:T(8,128)(2,1)} %all-to-all-done.ret0, bf16[16,192,256]{2,1,0:T(8,128)(2,1)} %get-tuple-element.19.ret1, bf16[16,256,1024]{2,1,0:T(8,128)(2,1)} %bitcast.73, bf16[512,384]{1,0:T(8,128)(2,1)} %constant.104.clone.place, ...), custom_call_target="tpu_custom_call" | custom-call | flops 4000000000 | bytes 14000000 | tf_op jit(solution)/shard_map/finish/pallas_call | solution.py:273
  293.4 1.0 slice_bitcast_fusion
  294.3 0.7 copy.25
  (39 shorter events, 4.3 us)
Async XLA Ops:
  0.6 2.2 copy-start.7
  0.6 2.3 copy-start.3
  0.7 4.2 %copy-start.6 = (f32[1024]{0:T(1024)S(1)}, f32[1024]{0:T(1024)}, u32[]{:S(2)}) copy-start(f32[1024]{0:T(1024)} %param.15) | copy-start | bytes 12292
  2.0 11.6 %copy-start.2 = (bf16[2,2,2,64,1024]{4,3,2,1,0:T(8,128)(2,1)}, bf16[2,2,2,64,1024]{4,3,2,1,0:T(8,128)(2,1)S(1)}, u32[]{:S(2)}) copy-start(bf16[2,2,2,64,1024]{4,3,2,1,0:T(8,128)(2,1)S(1)} %pad_maximum_fusion) | copy-start | bytes 3145732
  2.1 119.4 %collective-permute-start = (bf16[256,1024]{1,0:T(8,128)(2,1)S(1)}, bf16[256,1024]{1,0:T(8,128)(2,1)S(1)}, u32[]{:S(2)}, u32[]{:S(2)}) collective-permute-start(bf16[256,1024]{1,0:T(8,128)(2,1)S(1)} %dynamic-slice_bitcast_fusion), channel_id=1, source_target_pairs={{0,0},{64,8},{8,1},{72,9},{16,2},{80,10},{24,3},{88,11},{32,4},{96... | collective-permute-start | bytes 1572872 | tf_op jit(solution)/shard_map/ppermute | solution.py:574
  13.7 104.5 %copy-start.4 = (bf16[128,384]{1,0:T(8,128)(2,1)S(1)}, bf16[128,384]{1,0:T(8,128)(2,1)}, u32[]{:S(2)}) copy-start(bf16[128,384]{1,0:T(8,128)(2,1)} %constant.103.clone) | copy-start | bytes 294916
  121.5 4.8 %copy-start.1 = (bf16[16,192,384]{2,1,0:T(8,128)(2,1)S(1)}, bf16[16,192,384]{2,1,0:T(8,128)(2,1)}, u32[]{:S(2)}) copy-start(bf16[16,192,384]{2,1,0:T(8,128)(2,1)} %get-tuple-element.17) | copy-start | bytes 7077892
  126.3 61.0 %slice-start = ((s8[6291456]{0:T(1024)(128)(4,1)}), s8[2097152]{0:T(1024)(128)(4,1)S(1)}, s32[]{:S(2)}) async-start(s8[6291456]{0:T(1024)(128)(4,1)} %bitcast.55), calls=%async_computation.1 | async-start | bytes 4194304
  157.2 30.2 %slice-start.1 = ((s8[6291456]{0:T(1024)(128)(4,1)}), s8[4194304]{0:T(1024)(128)(4,1)S(1)}, s32[]{:S(2)}) async-start(s8[6291456]{0:T(1024)(128)(4,1)} %bitcast.55), calls=%async_computation.2 | async-start | bytes 8388608
  187.4 7.3 %copy-start = (bf16[3072,256]{1,0:T(8,128)(2,1)}, bf16[3072,256]{1,0:T(8,128)(2,1)S(1)}, u32[]{:S(2)}) copy-start(bf16[3072,256]{1,0:T(8,128)(2,1)S(1)} %attention.3) | copy-start | bytes 4718596
  190.1 92.3 %all-to-all-start = ((bf16[16,192,256]{2,1,0:T(8,128)(2,1)}), bf16[16,192,256]{2,1,0:T(8,128)(2,1)}, u32[]{:S(2)}, u32[]{:S(2)}) async-start(bf16[16,192,256]{2,1,0:T(8,128)(2,1)} %bitcast.13), calls=%async_computation | async-start | bytes 3145728 | tf_op jit(solution)/shard_map/all_to_all | solution.py:560
  242.0 4.1 %collective-permute-start.1 = (f32[32,1024]{1,0:T(8,128)S(1)}, f32[32,1024]{1,0:T(8,128)S(1)}, u32[]{:S(2)}, u32[]{:S(2)}) collective-permute-start(f32[32,1024]{1,0:T(8,128)S(1)} %reduce_sum.57), channel_id=1, source_target_pairs={{0,0},{8,64},{1,8},{9,72},{2,16},{10,80},{3,24},{11,88},{4,32},{12... | collective-permute-start | bytes 393224 | tf_op jit(solution)/shard_map/ppermute | solution.py:636
  246.1 0.7 copy-start.8
  279.7 2.1 copy-start.5

commit v5 on v4

--- a/solution.py
+++ b/solution.py
@@ -382,6 +382,50 @@
     return sent
 
 
+RELAYED = {
+    (2, 0): ((3, 0), (3, 0)),
+    (2, 1): ((3, 1), (3, 0)),
+    (0, 2): ((0, 3), (0, 3)),
+    (1, 2): ((1, 3), (0, 3)),
+}
+
+
+def send_balanced(msgs, got, held, send, recv, leg_send, leg_recv):
+    z, y, _, _ = place()
+
+    def number(dz, dy):
+        return 4 * lax.rem(z + dz, 4) + lax.rem(y + dy, 4)
+
+    legs = []
+    for r, (goal, (leg, _)) in enumerate(RELAYED.items()):
+        legs.append(
+            copy_to(msgs.at[number(*goal)], held.at[r], leg_send.at[r], leg_recv.at[r], on_sp(*leg))
+        )
+    sent = []
+    for k, peer in enumerate(SP_PEERS):
+        if peer not in RELAYED:
+            sent.append(
+                copy_to(
+                    msgs.at[number(*peer)], got.at[number(0, 0)], send.at[k], recv.at[k], on_sp(*peer)
+                )
+            )
+
+    def pass_on():
+        passed = []
+        for r, (goal, (leg, step)) in enumerate(RELAYED.items()):
+            legs[r].wait_recv()
+            source = number((4 - leg[0]) % 4, (4 - leg[1]) % 4)
+            k = SP_PEERS.index(goal)
+            passed.append(
+                copy_to(held.at[r], got.at[source], send.at[k], recv.at[k], on_sp(*step))
+            )
+        for c in legs:
+            c.wait_send()
+        return passed
+
+    return sent, pass_on
+
+
 def send_over_dp(block_for, got, send, recv):
     _, _, x, core = place()
     sent = []
@@ -460,8 +504,9 @@
         c.wait()
 
 
-def front_kernel(x, msgs, w, full, got, w_full, own_sem, *sems):
-    msg_send, msg_recv, ring, ring_in, pair, pair_in = sems[8:]
+def front_kernel(x, msgs, w, full, got, w_full, held, own_sem, *sems):
+    msg_send, msg_recv, ring, ring_in, pair, pair_in, leg_send, leg_recv = sems[8:]
+    later = []
     z, y, chip, core = place()
     me = 4 * z + y
     mine = 2 * chip + core
@@ -485,7 +530,9 @@
             keep(msgs.at[me], got.at[me], own_sem.at[1]),
             keep(w, w_full.at[mine], own_sem.at[2]),
         ]
-        return own + send_over_sp(lambda there: msgs.at[there], got, msg_send, msg_recv)
+        sent, pass_on = send_balanced(msgs, got, held, msg_send, msg_recv, leg_send, leg_recv)
+        later.append(pass_on)
+        return own + sent
 
     def row(s):
         return 2 * lax.rem(chip + s, 4) + core
@@ -493,6 +540,7 @@
     passed = []
 
     def midway():
+        out.extend(later[0]())
         for k, s in enumerate(ways):
             out[k].wait_recv()
             piece = w_full.at[row(4 - s), pl.ds(k * size, size)]
@@ -503,23 +551,26 @@
     for c in passed:
         c.wait_recv()
     to_partner(3, w_full.at[row(2)], row(2))
-    for c in out + passed:
+    for c in out[:2] + passed:
         c.wait_send()
+    for c in out[2:]:
+        c.wait()
     for c in beside.values():
         c.wait()
 
 
-def tail_kernel(msgs, pieces, gain, got, arrived, gains, own_sem, *sems):
+def tail_kernel(msgs, pieces, gain, got, arrived, gains, held, own_sem, *sems):
     z, y, chip, core = place()
     me = 4 * z + y
     mine = 2 * chip + core
     meet(SP_PEERS, DP_PEERS)
-    going = send_over_dp(lambda there: pieces.at[there], arrived, sems[0], sems[1])
+    going, pass_on = send_balanced(msgs, got, held, *sems[4:8])
+    going += send_over_dp(lambda there: pieces.at[there], arrived, sems[0], sems[1])
     going += send_over_sp(lambda there: gain, gains, sems[2], sems[3])
-    going += send_over_sp(lambda there: msgs.at[there], got, sems[4], sems[5])
     going.append(keep(pieces.at[mine], arrived.at[mine], own_sem.at[0]))
     going.append(keep(gain, gains.at[me], own_sem.at[1]))
     going.append(keep(msgs.at[me], got.at[me], own_sem.at[2]))
+    going += pass_on()
     for c in going:
         c.wait()
 
@@ -582,7 +633,7 @@
 
     rope_wide = jnp.pad(rope_key[0], ((0, 0), (0, 96)))
     sent = pack(query[0], out_grad[0], rope_wide, cosine, sine)
-    nlat_full, got, w_whole = moving(
+    nlat_full, got, w_whole, _ = moving(
         front_kernel,
         0,
         [nlat, sent, shard.reshape(512, LATENT)],
@@ -590,8 +641,9 @@
             ((SP_SIZE, TOKENS, LATENT), bf16),
             ((SP_SIZE, TOKENS, 384), bf16),
             ((DP_SIZE, 512, LATENT), bf16),
+            ((len(RELAYED), TOKENS, 384), bf16),
         ],
-        GATHER_SEMS + [(SP_SIZE - 1,), (2, 2), (4,)],
+        GATHER_SEMS + [(SP_SIZE - 1,), (2, 2), (4,), (len(RELAYED),)],
     )
     nlat_full = nlat_full.reshape(LENGTH, LATENT)
     got = got.reshape(LENGTH, 384)
@@ -622,7 +674,7 @@
     grads1 = attention(got, kv, ropes, 1)
     pieces1, gain1 = weight_part(grads1, 1)
     gain_part = ((gain0 + gain1) / latent_norm_gain).reshape(8, 128)
-    ret1, arrived, gains = moving(
+    ret1, arrived, gains, _ = moving(
         tail_kernel,
         1,
         [
@@ -630,8 +682,13 @@
             jnp.concatenate([pieces0, pieces1], axis=1),
             gain_part,
         ],
-        [((SP_SIZE, TOKENS, 256), bf16), ((DP_SIZE, 32, LATENT), f32), ((SP_SIZE, 8, 128), f32)],
-        [(DP_SIZE - 1,), (SP_SIZE - 1,), (SP_SIZE - 1,)],
+        [
+            ((SP_SIZE, TOKENS, 256), bf16),
+            ((DP_SIZE, 32, LATENT), f32),
+            ((SP_SIZE, 8, 128), f32),
+            ((len(RELAYED), TOKENS, 256), bf16),
+        ],
+        [(DP_SIZE - 1,), (SP_SIZE - 1,), (SP_SIZE - 1,), (len(RELAYED),)],
     )
     moved = lax.ppermute(arrived.sum(axis=0), SP_DP, [(b, a) for a, b in to_heads()])
     blocks, gains = moving(

time: 296 us -> 302 us (1.020)
  starting transfers between devices: 5.97 us -> 22.5 us
  Pallas kernels: 256 us -> 246 us
    all_to_all x1, starting transfers between devices: 4.6 us -> 21.1 us  [exchange(): return lax.all_to_all(value, SP, split_axis=0, concat_axis=0, tiled=True)]
    pallas_call x3, Pallas kernels: 176 us -> 166 us  [moving(): pl.pallas_call(kernel, in_specs=[pl.BlockSpec(memory_space=pltpu.VMEM)] *...]
  transfers between devices with their start and end apart: 3 -> 3, of which waited for: 0 -> 0; matrix products, arithmetic and copies ran while one was open for 7% -> 7% of each run, Pallas kernels for 62% -> 58%
where the time goes in v5:
time: 302 us; the launch traced here: 301 us
  Pallas kernels  246 us (81%)
  starting transfers between devices  22.5 us (7%)
  matrix products  14.6 us (5%)
  other arithmetic  10.5 us (3%)
  local copies, waits for them, and re-layouts  7 us (2%)
    pallas_call x3, Pallas kernels, moving(): pl.pallas_call(kernel, in_specs=[pl.BlockSpec(memory_space=pltpu.VMEM)] *...  166 us
    pallas_call x2, Pallas kernels, attention(): pl.pallas_call(attention_kernel, grid=(count,), in_specs=[column(2 * head...  61 us
    all_to_all x1, starting transfers between devices, exchange(): return lax.all_to_all(value, SP, split_axis=0, concat_axis=0, tiled=True)  21.1 us
    pallas_call x1, Pallas kernels, finish(): pl.pallas_call(finish_kernel, grid=(8,), in_specs=[pl.BlockSpec((2, TOKEN...  10.9 us
    pallas_call x1, Pallas kernels, pack(): pl.pallas_call(pack_kernel, grid=(8,), in_specs=[pl.BlockSpec((TOKENS, 38...  7.9 us
    dot_general x2, matrix products, weight_part(): lax.dot_general(grads[:, 128:256], nlat_full, (((0,), (0,)), ((), ())), p...  6.55 us
  transfers between devices with their start and end apart: 3, of which 0 were waited for; matrix products, arithmetic and copies ran while one was open for 7% of the time, Pallas kernels for 58%

profile of v5, /device:TPU:0, one launch (start us, length us, event | category | flops | bytes accessed | tf_op | source)
XLA Modules:
  0.0 301.2 jit_solution(7098883952741953852)
XLA Ops:
  0.7 1.3 pad_maximum_fusion
  3.1 1.1 multiply_sine_fusion.1
  4.9 0.9 fusion.2.x
  5.8 7.9 %pack.1.msgs = bf16[16,192,384]{2,1,0:T(8,128)(2,1)} custom-call(bf16[192,3072]{1,0:T(8,128)(2,1)} %bitcast.71, bf16[192,2048]{1,0:T(8,128)(2,1)} %bitcast.72, bf16[192,128]{1,0:T(8,128)(2,1)} %pad.4.rope, bf16[768,512]{1,0:T(8,128)(2,1)} %constant.101.clone.first, bf16[768,256]{1,0:T(8,128)(2,1)} %constant.102.clone.second, ...), custom_call_target="tpu_custom_call" | custom-call | flops 1811939328 | bytes 5000000 | tf_op jit(solution)/shard_map/pack/pallas_call | solution.py:93
  13.7 94.1 %shard_map.163 = (bf16[16,192,1024]{2,1,0:T(8,128)(2,1)}, bf16[16,192,384]{2,1,0:T(8,128)(2,1)}, bf16[8,512,1024]{2,1,0:T(8,128)(2,1)}, bf16[4,192,384]{2,1,0:T(8,128)(2,1)}) custom-call(bf16[192,1024]{1,0:T(8,128)(2,1)} %fusion.2.x, bf16[16,192,384]{2,1,0:T(8,128)(2,1)} %pack.1.msgs, bf16[512,1024]{1,0:T(8,128)(2,1)} %bitcast.60), custom_call_target="tpu_custom_call" | custom-call | flops 8000000000 | bytes 8000000 | tf_op jit(solution)/shard_map/pallas_call | solution.py:594
  107.8 3.3 %convolution_convert_fusion.q2_ref.k2_ref = bf16[3072,384]{1,0:T(8,128)(2,1)} fusion(bf16[128,384]{1,0:T(8,128)(2,1)S(1)} %copy-done.4, bf16[3072,384]{1,0:T(8,128)(2,1)} %bitcast.50), kind=kOutput, calls=%fused_computation | convolution fusion | flops 303169536 | bytes 3244032 | tf_op jit(solution)/shard_map/dot_general | solution.py:652
  111.1 4.8 %convolution_convert_fusion.1.kv_ref = bf16[3072,256]{1,0:T(8,128)(2,1)S(1)} fusion(bf16[3072,1024]{1,0:T(8,128)(2,1)} %bitcast.53, bf16[256,1024]{1,0:T(8,128)(2,1)S(1)} %collective-permute-done), kind=kOutput, calls=%fused_computation.1 | convolution fusion | flops 1611399168 | bytes 8388608 | tf_op jit(solution)/shard_map/dot_general | solution.py:655
  115.9 30.9 %attention.2 = bf16[3072,256]{1,0:T(8,128)(2,1)} custom-call(bf16[3072,384]{1,0:T(8,128)(2,1)S(1)} %bitcast.51, bf16[3072,384]{1,0:T(8,128)(2,1)} %convolution_convert_fusion.q2_ref.k2_ref, bf16[3072,256]{1,0:T(8,128)(2,1)S(1)} %convolution_convert_fusion.1.kv_ref, bf16[3072,384]{1,0:T(8,128)(2,1)} %convolution_convert_fusion.q2_ref.k2_ref), custom_call_target="tpu_custom_call" | custom-call | flops 12000000000 | bytes 8000000 | tf_op jit(solution)/shard_map/attention/pallas_call | solution.py:209
  146.7 30.2 %attention.3 = bf16[3072,256]{1,0:T(8,128)(2,1)S(1)} custom-call(bf16[3072,384]{1,0:T(8,128)(2,1)S(1)} %bitcast.52, bf16[3072,384]{1,0:T(8,128)(2,1)} %convolution_convert_fusion.q2_ref.k2_ref, bf16[3072,256]{1,0:T(8,128)(2,1)S(1)} %convolution_convert_fusion.1.kv_ref, bf16[3072,384]{1,0:T(8,128)(2,1)} %convolution_convert_fusion.q2_ref.k2_ref), custom_call_target="tpu_custom_call" | custom-call | flops 12000000000 | bytes 8000000 | tf_op jit(solution)/shard_map/attention/pallas_call | solution.py:209
  177.0 2.7 fusion.5
  179.7 21.1 %all-to-all-start = ((bf16[16,192,256]{2,1,0:T(8,128)(2,1)}), bf16[16,192,256]{2,1,0:T(8,128)(2,1)}, u32[]{:S(2)}, u32[]{:S(2)}) async-start(bf16[16,192,256]{2,1,0:T(8,128)(2,1)} %bitcast.13), calls=%async_computation | async-start | bytes 3145728 | tf_op jit(solution)/shard_map/all_to_all | solution.py:611
  200.8 3.8 %multiply_reduce_fusion = (f32[1024]{0:T(1024)S(1)}, f32[1024]{0:T(1024)S(1)}, f32[128,1024]{1,0:T(8,128)S(1)}) fusion(bf16[256,1024]{1,0:T(8,128)(2,1)S(1)} %collective-permute-done, f32[128,1024]{1,0:T(8,128)S(1)} %fusion.5, bf16[3072,1024]{1,0:T(8,128)(2,1)} %bitcast.54, bf16[3072,256]{1,0:T(8,128)(2,1)S(1)} %attention.3), kind=kOutput, calls=%fused_computation.16 | convolution fusion | flops 806090752 | bytes 8658944 | tf_op jit(solution)/shard_map/dot_general | solution.py:660
  205.3 1.0 pad_maximum_fusion.1.pieces
  206.4 38.6 %shard_map.164 = (bf16[16,192,256]{2,1,0:T(8,128)(2,1)}, f32[8,32,1024]{2,1,0:T(8,128)}, f32[16,8,128]{2,1,0:T(8,128)}, bf16[4,192,256]{2,1,0:T(8,128)(2,1)}) custom-call(bf16[16,192,256]{2,1,0:T(8,128)(2,1)} %bitcast.49, f32[8,32,1024]{2,1,0:T(8,128)} %pad_maximum_fusion.1.pieces, f32[8,128]{1,0:T(8,128)} %divide_bitcast_fusion.gain), custom_call_target="tpu_custom_call" | custom-call | flops 8000000000 | bytes 8000000 | tf_op jit(solution)/shard_map/pallas_call | solution.py:594
  245.0 1.3 reduce_sum.57
  247.0 1.9 multiply_sine_fusion
  248.9 1.4 reduce_sum.58.gain
  251.0 33.2 %shard_map.165 = (f32[16,32,1024]{2,1,0:T(8,128)}, f32[8,8,128]{2,1,0:T(8,128)}) custom-call(f32[32,1024]{1,0:T(8,128)} %copy-done.8, f32[8,128]{1,0:T(8,128)} %reduce_sum.58.gain), custom_call_target="tpu_custom_call" | custom-call | flops 8000000000 | bytes 8000000 | tf_op jit(solution)/shard_map/pallas_call | solution.py:594
  284.2 1.7 fusion.22
  285.9 1.0 copy.23
  287.0 1.0 copy.24
  288.6 10.9 %finish.1 = (bf16[192,3072]{1,0:T(8,128)(2,1)}, f32[192,1024]{1,0:T(8,128)}, f32[192,128]{1,0:T(8,128)}) custom-call(bf16[16,192,256]{2,1,0:T(8,128)(2,1)} %all-to-all-done.ret0, bf16[16,192,256]{2,1,0:T(8,128)(2,1)} %get-tuple-element.19.ret1, bf16[16,256,1024]{2,1,0:T(8,128)(2,1)} %bitcast.73, bf16[512,384]{1,0:T(8,128)(2,1)} %constant.104.clone.place, ...), custom_call_target="tpu_custom_call" | custom-call | flops 4000000000 | bytes 14000000 | tf_op jit(solution)/shard_map/finish/pallas_call | solution.py:273
  299.6 1.0 slice_bitcast_fusion
  300.5 0.7 copy.25
  (39 shorter events, 4.3 us)
Async XLA Ops:
  0.6 2.2 copy-start.7
  0.6 2.3 copy-start.3
  0.7 4.2 %copy-start.6 = (f32[1024]{0:T(1024)S(1)}, f32[1024]{0:T(1024)}, u32[]{:S(2)}) copy-start(f32[1024]{0:T(1024)} %param.15) | copy-start | bytes 12292
  2.0 11.6 %copy-start.2 = (bf16[2,2,2,64,1024]{4,3,2,1,0:T(8,128)(2,1)}, bf16[2,2,2,64,1024]{4,3,2,1,0:T(8,128)(2,1)S(1)}, u32[]{:S(2)}) copy-start(bf16[2,2,2,64,1024]{4,3,2,1,0:T(8,128)(2,1)S(1)} %pad_maximum_fusion) | copy-start | bytes 3145732
  2.1 109.0 %collective-permute-start = (bf16[256,1024]{1,0:T(8,128)(2,1)S(1)}, bf16[256,1024]{1,0:T(8,128)(2,1)S(1)}, u32[]{:S(2)}, u32[]{:S(2)}) collective-permute-start(bf16[256,1024]{1,0:T(8,128)(2,1)S(1)} %dynamic-slice_bitcast_fusion), channel_id=1, source_target_pairs={{0,0},{64,8},{8,1},{72,9},{16,2},{80,10},{24,3},{88,11},{32,4},{96... | collective-permute-start | bytes 1572872 | tf_op jit(solution)/shard_map/ppermute | solution.py:625
  13.7 94.1 %copy-start.4 = (bf16[128,384]{1,0:T(8,128)(2,1)S(1)}, bf16[128,384]{1,0:T(8,128)(2,1)}, u32[]{:S(2)}) copy-start(bf16[128,384]{1,0:T(8,128)(2,1)} %constant.103.clone) | copy-start | bytes 294916
  111.1 4.8 %copy-start.1 = (bf16[16,192,384]{2,1,0:T(8,128)(2,1)S(1)}, bf16[16,192,384]{2,1,0:T(8,128)(2,1)}, u32[]{:S(2)}) copy-start(bf16[16,192,384]{2,1,0:T(8,128)(2,1)} %get-tuple-element.17) | copy-start | bytes 7077892
  115.9 61.0 %slice-start = ((s8[6291456]{0:T(1024)(128)(4,1)}), s8[2097152]{0:T(1024)(128)(4,1)S(1)}, s32[]{:S(2)}) async-start(s8[6291456]{0:T(1024)(128)(4,1)} %bitcast.55), calls=%async_computation.1 | async-start | bytes 4194304
  146.7 30.2 %slice-start.1 = ((s8[6291456]{0:T(1024)(128)(4,1)}), s8[4194304]{0:T(1024)(128)(4,1)S(1)}, s32[]{:S(2)}) async-start(s8[6291456]{0:T(1024)(128)(4,1)} %bitcast.55), calls=%async_computation.2 | async-start | bytes 8388608
  177.0 23.8 %copy-start = (bf16[3072,256]{1,0:T(8,128)(2,1)}, bf16[3072,256]{1,0:T(8,128)(2,1)S(1)}, u32[]{:S(2)}) copy-start(bf16[3072,256]{1,0:T(8,128)(2,1)S(1)} %attention.3) | copy-start | bytes 4718596
  179.7 108.9 %all-to-all-start = ((bf16[16,192,256]{2,1,0:T(8,128)(2,1)}), bf16[16,192,256]{2,1,0:T(8,128)(2,1)}, u32[]{:S(2)}, u32[]{:S(2)}) async-start(bf16[16,192,256]{2,1,0:T(8,128)(2,1)} %bitcast.13), calls=%async_computation | async-start | bytes 3145728 | tf_op jit(solution)/shard_map/all_to_all | solution.py:611
  246.3 4.1 %collective-permute-start.1 = (f32[32,1024]{1,0:T(8,128)S(1)}, f32[32,1024]{1,0:T(8,128)S(1)}, u32[]{:S(2)}, u32[]{:S(2)}) collective-permute-start(f32[32,1024]{1,0:T(8,128)S(1)} %reduce_sum.57), channel_id=1, source_target_pairs={{0,0},{8,64},{1,8},{9,72},{2,16},{10,80},{3,24},{11,88},{4,32},{12... | collective-permute-start | bytes 393224 | tf_op jit(solution)/shard_map/ppermute | solution.py:693
  250.4 0.7 copy-start.8
  285.9 2.1 copy-start.5

commit v6 on v4

--- a/solution.py
+++ b/solution.py
@@ -232,7 +232,7 @@
 
 
 def finish_kernel(
-    ret0, ret1, w, place, turn, latent, gain, wide_cos, wide_sin, cosine, sine,
+    ret0, ret1, w, place, turn, latent, gain, cosine, sine,
     query_grad, latent_grad, rope_sum, acc,
 ):
     step = pl.program_id(0)
@@ -246,7 +246,10 @@
     row = jnp.concatenate(left, axis=1)
     plain = jnp.dot(row, place[...], preferred_element_type=f32)
     turned = jnp.dot(row, turn[...], preferred_element_type=f32)
-    query_grad[...] = (plain * wide_cos[...] + turned * wide_sin[...]).astype(bf16)
+    roped = lax.broadcasted_iota(jnp.int32, plain.shape, 1) % 96 >= 64
+    wide_cos = jnp.where(roped, jnp.concatenate([cosine[...]] * 3, axis=1), 1.0)
+    wide_sin = jnp.concatenate([sine[...]] * 3, axis=1)
+    query_grad[...] = (plain * wide_cos + turned * wide_sin).astype(bf16)
     rope_sum[...] += sum(x.astype(f32) for x in left)
     total = acc[...]
     for t in range(2):
@@ -267,7 +270,7 @@
         rope_sum[...] = total_rope * cosine[...] - turned_halves(total_rope) * sine[...]
 
 
-def finish(ret0, ret1, w, latent, gain, wide_cos, wide_sin, cosine, sine):
+def finish(ret0, ret1, w, latent, gain, cosine, sine):
     fixed = lambda shape: pl.BlockSpec(shape, lambda j: (0,) * len(shape))
     place, turn = unpack_tables()
     return pl.pallas_call(
@@ -281,8 +284,6 @@
             fixed((512, 384)),
             fixed((TOKENS, LATENT)),
             fixed((1, LATENT)),
-            fixed((TOKENS, 384)),
-            fixed((TOKENS, 384)),
             fixed((TOKENS, 128)),
             fixed((TOKENS, 128)),
         ],
@@ -304,7 +305,7 @@
         name="finish",
     )(
         ret0, ret1, w, jnp.asarray(place, bf16), jnp.asarray(turn, bf16), latent, gain,
-        wide_cos, wide_sin, cosine, sine,
+        cosine, sine,
     )
 
 
@@ -339,6 +340,7 @@
 
 SP_PEERS = [(k // 4, k % 4) for k in range(1, SP_SIZE)]
 DP_PEERS = [(k // 2, k % 2) for k in range(1, DP_SIZE)]
+MESSAGE_TURNS = [(4, 10, 9), (5, 13, 1), (6, 14), (3, 11), (2, 12), (7, 8), (0,), ()]
 NEAR = [(0, 1), (0, 3), (1, 0), (3, 0)]
 X_PEERS = [(1, 0), (3, 0), (0, 1)]
 
@@ -371,10 +373,11 @@
     return c
 
 
-def send_over_sp(block_for, got, send, recv):
+def send_over_sp(block_for, got, send, recv, chosen=range(SP_SIZE - 1)):
     z, y, _, _ = place()
     sent = []
-    for k, (dz, dy) in enumerate(SP_PEERS):
+    for k in chosen:
+        dz, dy = SP_PEERS[k]
         there = 4 * lax.rem(z + dz, 4) + lax.rem(y + dy, 4)
         sent.append(
             copy_to(block_for(there), got.at[4 * z + y], send.at[k], recv.at[k], on_sp(dz, dy))
@@ -424,7 +427,7 @@
             third[h, 0, w] = copy_to(
                 x.at[half[h]], full.at[me, half[h]], far.at[h, 0, w], far_in.at[h, 0, w], across(h, s)
             )
-    rest = between()
+    rest = list(between(0))
 
     def onward(h, k):
         there = full.at[block(h, lines[k], 0), half[h]]
@@ -439,10 +442,12 @@
             piece = full.at[block(h, 4 - s, 0), quarter[h][w]]
             second[h, w] = copy_to(piece, piece, pass1.at[h, w], pass1_in.at[h, w], along(h, s))
             onward(h, w + 1)
+        rest += between(w + 1)
     for h in range(2):
         for w in range(2):
             second[h, w].wait_recv()
         onward(h, 3)
+    rest += between(3)
     for k in range(4):
         if k == 2:
             midway()
@@ -453,6 +458,7 @@
                 fourth[h, k, w] = copy_to(
                     piece, piece, pass2.at[h, k, w], pass2_in.at[h, k, w], across(h, s)
                 )
+        rest += between(k + 4)
     for group in (first, second, third):
         for c in group.values():
             c.wait_send()
@@ -479,13 +485,17 @@
     ]
     to_partner(0, w, mine)
 
-    def between():
-        own = [
-            keep(x, full.at[me], own_sem.at[0]),
-            keep(msgs.at[me], got.at[me], own_sem.at[1]),
-            keep(w, w_full.at[mine], own_sem.at[2]),
-        ]
-        return own + send_over_sp(lambda there: msgs.at[there], got, msg_send, msg_recv)
+    def between(step):
+        own = []
+        if step == 0:
+            own = [
+                keep(x, full.at[me], own_sem.at[0]),
+                keep(msgs.at[me], got.at[me], own_sem.at[1]),
+                keep(w, w_full.at[mine], own_sem.at[2]),
+            ]
+        return own + send_over_sp(
+            lambda there: msgs.at[there], got, msg_send, msg_recv, MESSAGE_TURNS[step]
+        )
 
     def row(s):
         return 2 * lax.rem(chip + s, 4) + core
@@ -528,7 +538,9 @@
     z, y, chip, core = place()
     meet(NEAR, DP_PEERS)
 
-    def between():
+    def between(step):
+        if step > 0:
+            return []
         own = [
             keep(x, full.at[4 * z + y], own_sem.at[0]),
             keep(gain, gains.at[2 * chip + core], own_sem.at[1]),
@@ -576,10 +588,6 @@
     position = (spot * TOKENS + jnp.arange(TOKENS)).astype(f32)[:, None]
     angle = position * inverse_frequency(jnp.arange(128) % 16)[None]
     cosine, sine = jnp.cos(angle), jnp.sin(angle)
-    place = jnp.arange(384) % 96
-    wide = position * jnp.where(place < 64, 0.0, inverse_frequency(place % 16))[None]
-    wide_cos, wide_sin = jnp.cos(wide), jnp.sin(wide)
-
     rope_wide = jnp.pad(rope_key[0], ((0, 0), (0, 96)))
     sent = pack(query[0], out_grad[0], rope_wide, cosine, sine)
     nlat_full, got, w_whole = moving(
@@ -644,7 +652,7 @@
     gain_grad = gains.sum(axis=0).reshape(LATENT)
 
     query_grad, latent_grad, rope_sum = finish(
-        ret0, ret1, w_whole, latent[0], latent_norm_gain[None], wide_cos, wide_sin, cosine, sine
+        ret0, ret1, w_whole, latent[0], latent_norm_gain[None], cosine, sine
     )
     blocks = blocks.reshape(2, DP_SIZE, 2, 2, 8, LATENT).transpose(3, 0, 2, 1, 4, 5)
     blocks = blocks.reshape(2, 256, LATENT)

time: 296 us -> 296 us (level)
  starting transfers between devices: 5.97 us -> 14.9 us
  Pallas kernels: 256 us -> 249 us
    all_to_all x1, starting transfers between devices: 4.6 us -> 13.6 us  [exchange(): return lax.all_to_all(value, SP, split_axis=0, concat_axis=0, tiled=True)]
    pallas_call x3, Pallas kernels: 176 us -> 169 us  [moving(): pl.pallas_call(kernel, in_specs=[pl.BlockSpec(memory_space=pltpu.VMEM)] *...]
  transfers between devices with their start and end apart: 3 -> 3, of which waited for: 0 -> 0; matrix products, arithmetic and copies ran while one was open for 7% -> 6% of each run, Pallas kernels for 62% -> 60%
where the time goes in v6:
time: 296 us; the launch traced here: 295 us
  Pallas kernels  249 us (84%)
  starting transfers between devices  14.9 us (5%)
  matrix products  14.1 us (5%)
  other arithmetic  8.51 us (3%)
  local copies, waits for them, and re-layouts  7.02 us (2%)
    pallas_call x3, Pallas kernels, moving(): pl.pallas_call(kernel, in_specs=[pl.BlockSpec(memory_space=pltpu.VMEM)] *...  169 us
    pallas_call x2, Pallas kernels, attention(): pl.pallas_call(attention_kernel, grid=(count,), in_specs=[column(2 * head...  61.3 us
    all_to_all x1, starting transfers between devices, exchange(): return lax.all_to_all(value, SP, split_axis=0, concat_axis=0, tiled=True)  13.6 us
    pallas_call x1, Pallas kernels, finish(): pl.pallas_call(finish_kernel, grid=(8,), in_specs=[pl.BlockSpec((2, TOKEN...  10.7 us
    pallas_call x1, Pallas kernels, pack(): pl.pallas_call(pack_kernel, grid=(8,), in_specs=[pl.BlockSpec((TOKENS, 38...  7.92 us
    dot_general x2, matrix products, weight_part(): lax.dot_general(grads[:, 128:256], nlat_full, (((0,), (0,)), ((), ())), p...  5.98 us
  transfers between devices with their start and end apart: 3, of which 0 were waited for; matrix products, arithmetic and copies ran while one was open for 6% of the time, Pallas kernels for 60%

profile of v6, /device:TPU:0, one launch (start us, length us, event | category | flops | bytes accessed | tf_op | source)
XLA Modules:
  0.0 294.6 jit_solution(16311911190317275465)
XLA Ops:
  0.7 1.3 pad_maximum_fusion
  2.1 0.7 collective-permute-start
  3.8 1.1 multiply_sine_fusion
  4.9 0.9 fusion.2.x
  5.8 7.9 %pack.1.msgs = bf16[16,192,384]{2,1,0:T(8,128)(2,1)} custom-call(bf16[192,3072]{1,0:T(8,128)(2,1)} %bitcast.71, bf16[192,2048]{1,0:T(8,128)(2,1)} %bitcast.72, bf16[192,128]{1,0:T(8,128)(2,1)} %pad.4.rope, bf16[768,512]{1,0:T(8,128)(2,1)} %constant.77.clone.first, bf16[768,256]{1,0:T(8,128)(2,1)} %constant.78.clone.second, ...), custom_call_target="tpu_custom_call" | custom-call | flops 1811939328 | bytes 5000000 | tf_op jit(solution)/shard_map/pack/pallas_call | solution.py:93
  13.7 96.5 %shard_map.163 = (bf16[16,192,1024]{2,1,0:T(8,128)(2,1)}, bf16[16,192,384]{2,1,0:T(8,128)(2,1)}, bf16[8,512,1024]{2,1,0:T(8,128)(2,1)}) custom-call(bf16[192,1024]{1,0:T(8,128)(2,1)} %fusion.2.x, bf16[16,192,384]{2,1,0:T(8,128)(2,1)} %pack.1.msgs, bf16[512,1024]{1,0:T(8,128)(2,1)} %bitcast.60), custom_call_target="tpu_custom_call" | custom-call | flops 8000000000 | bytes 8000000 | tf_op jit(solution)/shard_map/pallas_call | solution.py:555
  110.2 3.3 %convolution_convert_fusion.q2_ref.k2_ref = bf16[3072,384]{1,0:T(8,128)(2,1)} fusion(bf16[128,384]{1,0:T(8,128)(2,1)S(1)} %copy-done.4, bf16[3072,384]{1,0:T(8,128)(2,1)} %bitcast.50), kind=kOutput, calls=%fused_computation | convolution fusion | flops 303169536 | bytes 3244032 | tf_op jit(solution)/shard_map/dot_general | solution.py:608
  113.5 4.8 %convolution_convert_fusion.1.kv_ref = bf16[3072,256]{1,0:T(8,128)(2,1)S(1)} fusion(bf16[3072,1024]{1,0:T(8,128)(2,1)} %bitcast.53, bf16[256,1024]{1,0:T(8,128)(2,1)S(1)} %collective-permute-done), kind=kOutput, calls=%fused_computation.1 | convolution fusion | flops 1611399168 | bytes 8388608 | tf_op jit(solution)/shard_map/dot_general | solution.py:611
  118.3 30.2 %attention.3 = bf16[3072,256]{1,0:T(8,128)(2,1)S(1)} custom-call(bf16[3072,384]{1,0:T(8,128)(2,1)S(1)} %bitcast.51, bf16[3072,384]{1,0:T(8,128)(2,1)} %convolution_convert_fusion.q2_ref.k2_ref, bf16[3072,256]{1,0:T(8,128)(2,1)S(1)} %convolution_convert_fusion.1.kv_ref, bf16[3072,384]{1,0:T(8,128)(2,1)} %convolution_convert_fusion.q2_ref.k2_ref), custom_call_target="tpu_custom_call" | custom-call | flops 12000000000 | bytes 8000000 | tf_op jit(solution)/shard_map/attention/pallas_call | solution.py:209
  148.5 31.1 %attention.2 = bf16[3072,256]{1,0:T(8,128)(2,1)} custom-call(bf16[3072,384]{1,0:T(8,128)(2,1)S(1)} %bitcast.52, bf16[3072,384]{1,0:T(8,128)(2,1)} %convolution_convert_fusion.q2_ref.k2_ref, bf16[3072,256]{1,0:T(8,128)(2,1)S(1)} %convolution_convert_fusion.1.kv_ref, bf16[3072,384]{1,0:T(8,128)(2,1)} %convolution_convert_fusion.q2_ref.k2_ref), custom_call_target="tpu_custom_call" | custom-call | flops 12000000000 | bytes 8000000 | tf_op jit(solution)/shard_map/attention/pallas_call | solution.py:209
  179.7 2.1 fusion.5
  181.8 13.6 %all-to-all-start = ((bf16[16,192,256]{2,1,0:T(8,128)(2,1)}), bf16[16,192,256]{2,1,0:T(8,128)(2,1)}, u32[]{:S(2)}, u32[]{:S(2)}) async-start(bf16[16,192,256]{2,1,0:T(8,128)(2,1)} %bitcast.13), calls=%async_computation | async-start | bytes 3145728 | tf_op jit(solution)/shard_map/all_to_all | solution.py:572
  195.4 3.9 %multiply_reduce_fusion = (f32[1024]{0:T(1024)S(1)}, f32[1024]{0:T(1024)S(1)}, f32[128,1024]{1,0:T(8,128)S(1)}) fusion(bf16[256,1024]{1,0:T(8,128)(2,1)S(1)} %collective-permute-done, f32[128,1024]{1,0:T(8,128)S(1)} %fusion.5, bf16[3072,1024]{1,0:T(8,128)(2,1)} %bitcast.54, bf16[3072,256]{1,0:T(8,128)(2,1)S(1)} %attention.3), kind=kOutput, calls=%fused_computation.16 | convolution fusion | flops 806090752 | bytes 8658944 | tf_op jit(solution)/shard_map/dot_general | solution.py:616
  199.9 1.0 pad_maximum_fusion.1.pieces
  201.0 40.1 %shard_map.164 = (bf16[16,192,256]{2,1,0:T(8,128)(2,1)}, f32[8,32,1024]{2,1,0:T(8,128)}, f32[16,8,128]{2,1,0:T(8,128)}) custom-call(bf16[16,192,256]{2,1,0:T(8,128)(2,1)} %bitcast.49, f32[8,32,1024]{2,1,0:T(8,128)} %pad_maximum_fusion.1.pieces, f32[8,128]{1,0:T(8,128)} %divide_bitcast_fusion.gain), custom_call_target="tpu_custom_call" | custom-call | flops 8000000000 | bytes 8000000 | tf_op jit(solution)/shard_map/pallas_call | solution.py:555
  241.1 1.3 reduce_sum.57
  243.0 1.5 reduce_sum.58.gain
  245.1 32.6 %shard_map.165 = (f32[16,32,1024]{2,1,0:T(8,128)}, f32[8,8,128]{2,1,0:T(8,128)}) custom-call(f32[32,1024]{1,0:T(8,128)} %copy-done.8, f32[8,128]{1,0:T(8,128)} %reduce_sum.58.gain), custom_call_target="tpu_custom_call" | custom-call | flops 8000000000 | bytes 8000000 | tf_op jit(solution)/shard_map/pallas_call | solution.py:555
  277.8 1.7 fusion.12
  279.5 1.0 copy.24
  281.1 1.0 copy.23
  282.2 10.7 %finish.1 = (bf16[192,3072]{1,0:T(8,128)(2,1)}, f32[192,1024]{1,0:T(8,128)}, f32[192,128]{1,0:T(8,128)}) custom-call(bf16[16,192,256]{2,1,0:T(8,128)(2,1)} %all-to-all-done.ret0, bf16[16,192,256]{2,1,0:T(8,128)(2,1)} %get-tuple-element.19.ret1, bf16[16,256,1024]{2,1,0:T(8,128)(2,1)} %bitcast.73, bf16[512,384]{1,0:T(8,128)(2,1)} %constant.80.clone.place, ...), custom_call_target="tpu_custom_call" | custom-call | flops 4000000000 | bytes 14000000 | tf_op jit(solution)/shard_map/finish/pallas_call | solution.py:276
  292.9 1.0 slice_bitcast_fusion
  293.9 0.7 copy.25
  (37 shorter events, 3.6 us)
Async XLA Ops:
  0.6 2.2 copy-start.3
  0.6 2.4 copy-start.7
  0.7 4.2 %copy-start.6 = (f32[1024]{0:T(1024)S(1)}, f32[1024]{0:T(1024)}, u32[]{:S(2)}) copy-start(f32[1024]{0:T(1024)} %param.15) | copy-start | bytes 12292
  2.0 11.7 %copy-start.2 = (bf16[2,2,2,64,1024]{4,3,2,1,0:T(8,128)(2,1)}, bf16[2,2,2,64,1024]{4,3,2,1,0:T(8,128)(2,1)S(1)}, u32[]{:S(2)}) copy-start(bf16[2,2,2,64,1024]{4,3,2,1,0:T(8,128)(2,1)S(1)} %pad_maximum_fusion) | copy-start | bytes 3145732
  2.1 111.4 %collective-permute-start = (bf16[256,1024]{1,0:T(8,128)(2,1)S(1)}, bf16[256,1024]{1,0:T(8,128)(2,1)S(1)}, u32[]{:S(2)}, u32[]{:S(2)}) collective-permute-start(bf16[256,1024]{1,0:T(8,128)(2,1)S(1)} %dynamic-slice_bitcast_fusion), channel_id=1, source_target_pairs={{0,0},{64,8},{8,1},{72,9},{16,2},{80,10},{24,3},{88,11},{32,4},{96... | collective-permute-start | bytes 1572872 | tf_op jit(solution)/shard_map/ppermute | solution.py:586
  13.7 96.5 %copy-start.4 = (bf16[128,384]{1,0:T(8,128)(2,1)S(1)}, bf16[128,384]{1,0:T(8,128)(2,1)}, u32[]{:S(2)}) copy-start(bf16[128,384]{1,0:T(8,128)(2,1)} %constant.79.clone) | copy-start | bytes 294916
  113.5 4.8 %copy-start.1 = (bf16[16,192,384]{2,1,0:T(8,128)(2,1)S(1)}, bf16[16,192,384]{2,1,0:T(8,128)(2,1)}, u32[]{:S(2)}) copy-start(bf16[16,192,384]{2,1,0:T(8,128)(2,1)} %get-tuple-element.17) | copy-start | bytes 7077892
  113.5 66.1 %slice-start = ((s8[6291456]{0:T(1024)(128)(4,1)}), s8[4194304]{0:T(1024)(128)(4,1)S(1)}, s32[]{:S(2)}) async-start(s8[6291456]{0:T(1024)(128)(4,1)} %bitcast.55), calls=%async_computation.1 | async-start | bytes 8388608
  118.3 61.3 %slice-start.1 = ((s8[6291456]{0:T(1024)(128)(4,1)}), s8[2097152]{0:T(1024)(128)(4,1)S(1)}, s32[]{:S(2)}) async-start(s8[6291456]{0:T(1024)(128)(4,1)} %bitcast.55), calls=%async_computation.2 | async-start | bytes 4194304
  148.5 46.9 %copy-start = (bf16[3072,256]{1,0:T(8,128)(2,1)}, bf16[3072,256]{1,0:T(8,128)(2,1)S(1)}, u32[]{:S(2)}) copy-start(bf16[3072,256]{1,0:T(8,128)(2,1)S(1)} %attention.3) | copy-start | bytes 4718596
  181.8 100.3 %all-to-all-start = ((bf16[16,192,256]{2,1,0:T(8,128)(2,1)}), bf16[16,192,256]{2,1,0:T(8,128)(2,1)}, u32[]{:S(2)}, u32[]{:S(2)}) async-start(bf16[16,192,256]{2,1,0:T(8,128)(2,1)} %bitcast.13), calls=%async_computation | async-start | bytes 3145728 | tf_op jit(solution)/shard_map/all_to_all | solution.py:572
  242.4 2.1 collective-permute-start.1
  244.5 0.7 copy-start.8
  277.8 2.7 copy-start.5

commit v7 on v6

--- a/solution.py
+++ b/solution.py
@@ -396,7 +396,7 @@
     return sent
 
 
-def gather_over_sp(x, full, sems, between, midway=lambda: None):
+def gather_over_sp(x, full, sems, between, midway=lambda k: None):
     leg, leg_in, pass1, pass1_in, far, far_in, pass2, pass2_in = sems
     z, y, _, _ = place()
     me = 4 * z + y
@@ -449,8 +449,7 @@
         onward(h, 3)
     rest += between(3)
     for k in range(4):
-        if k == 2:
-            midway()
+        midway(k)
         for w, s in enumerate(ways):
             for h in range(2):
                 third[h, k, w].wait_recv()
@@ -502,17 +501,19 @@
 
     passed = []
 
-    def midway():
-        for k, s in enumerate(ways):
-            out[k].wait_recv()
-            piece = w_full.at[row(4 - s), pl.ds(k * size, size)]
-            passed.append(copy_to(piece, piece, ring.at[1, k], ring_in.at[1, k], on_dp(s, 0)))
-            to_partner(1 + k, w_full.at[row(4 - s)], row(4 - s))
+    def midway(step):
+        if step == 0:
+            for k, s in enumerate(ways):
+                out[k].wait_recv()
+                piece = w_full.at[row(4 - s), pl.ds(k * size, size)]
+                passed.append(copy_to(piece, piece, ring.at[1, k], ring_in.at[1, k], on_dp(s, 0)))
+                to_partner(1 + k, w_full.at[row(4 - s)], row(4 - s))
+        if step == 3:
+            for c in passed:
+                c.wait_recv()
+            to_partner(3, w_full.at[row(2)], row(2))
 
     gather_over_sp(x, full, sems[:8], between, midway)
-    for c in passed:
-        c.wait_recv()
-    to_partner(3, w_full.at[row(2)], row(2))
     for c in out + passed:
         c.wait_send()
     for c in beside.values():
@@ -641,12 +642,12 @@
         [((SP_SIZE, TOKENS, 256), bf16), ((DP_SIZE, 32, LATENT), f32), ((SP_SIZE, 8, 128), f32)],
         [(DP_SIZE - 1,), (SP_SIZE - 1,), (SP_SIZE - 1,)],
     )
-    moved = lax.ppermute(arrived.sum(axis=0), SP_DP, [(b, a) for a, b in to_heads()])
+    moved = lax.ppermute(arrived.sum(axis=0).astype(bf16), SP_DP, [(b, a) for a, b in to_heads()])
     blocks, gains = moving(
         last_kernel,
         2,
         [moved, gains.sum(axis=0)],
-        [((SP_SIZE, 32, LATENT), f32), ((DP_SIZE, 8, 128), f32)],
+        [((SP_SIZE, 32, LATENT), bf16), ((DP_SIZE, 8, 128), f32)],
         GATHER_SEMS + [(DP_SIZE - 1,)],
     )
     gain_grad = gains.sum(axis=0).reshape(LATENT)
@@ -655,7 +656,7 @@
         ret0, ret1, w_whole, latent[0], latent_norm_gain[None], cosine, sine
     )
     blocks = blocks.reshape(2, DP_SIZE, 2, 2, 8, LATENT).transpose(3, 0, 2, 1, 4, 5)
-    blocks = blocks.reshape(2, 256, LATENT)
+    blocks = blocks.reshape(2, 256, LATENT).astype(f32)
     return (
         query_grad[None],
         latent_grad[None],

time: 296 us -> 282 us (0.953)
  Pallas kernels: 249 us -> 236 us
    pallas_call x3, Pallas kernels: 169 us -> 156 us  [moving(): pl.pallas_call(kernel, in_specs=[pl.BlockSpec(memory_space=pltpu.VMEM)] *...]
  transfers between devices with their start and end apart: 3 -> 3, of which waited for: 0 -> 0; matrix products, arithmetic and copies ran while one was open for 6% -> 7% of each run, Pallas kernels for 60% -> 58%
where the time goes in v7:
time: 282 us; the launch traced here: 281 us
  Pallas kernels  236 us (84%)
  matrix products  14.1 us (5%)
  starting transfers between devices  13.5 us (5%)
  other arithmetic  10.7 us (4%)
  local copies, waits for them, and re-layouts  5.55 us (2%)
    pallas_call x3, Pallas kernels, moving(): pl.pallas_call(kernel, in_specs=[pl.BlockSpec(memory_space=pltpu.VMEM)] *...  156 us
    pallas_call x2, Pallas kernels, attention(): pl.pallas_call(attention_kernel, grid=(count,), in_specs=[column(2 * head...  61.3 us
    all_to_all x1, starting transfers between devices, exchange(): return lax.all_to_all(value, SP, split_axis=0, concat_axis=0, tiled=True)  12.1 us
    pallas_call x1, Pallas kernels, finish(): pl.pallas_call(finish_kernel, grid=(8,), in_specs=[pl.BlockSpec((2, TOKEN...  10.8 us
    pallas_call x1, Pallas kernels, pack(): pl.pallas_call(pack_kernel, grid=(8,), in_specs=[pl.BlockSpec((TOKENS, 38...  7.93 us
    dot_general x2, matrix products, weight_part(): lax.dot_general(grads[:, 128:256], nlat_full, (((0,), (0,)), ((), ())), p...  5.98 us
  transfers between devices with their start and end apart: 3, of which 0 were waited for; matrix products, arithmetic and copies ran while one was open for 7% of the time, Pallas kernels for 58%

profile of v7, /device:TPU:0, one launch (start us, length us, event | category | flops | bytes accessed | tf_op | source)
XLA Modules:
  0.0 281.2 jit_solution(7447219000717838686)
XLA Ops:
  0.7 1.3 pad_maximum_fusion
  3.8 1.1 multiply_sine_fusion
  4.9 0.9 fusion.2.x
  5.8 7.9 %pack.1.msgs = bf16[16,192,384]{2,1,0:T(8,128)(2,1)} custom-call(bf16[192,3072]{1,0:T(8,128)(2,1)} %bitcast.72, bf16[192,2048]{1,0:T(8,128)(2,1)} %bitcast.73, bf16[192,128]{1,0:T(8,128)(2,1)} %pad.4.rope, bf16[768,512]{1,0:T(8,128)(2,1)} %constant.77.clone.first, bf16[768,256]{1,0:T(8,128)(2,1)} %constant.78.clone.second, ...), custom_call_target="tpu_custom_call" | custom-call | flops 1811939328 | bytes 5000000 | tf_op jit(solution)/shard_map/pack/pallas_call | solution.py:93
  13.7 92.3 %shard_map.163 = (bf16[16,192,1024]{2,1,0:T(8,128)(2,1)}, bf16[16,192,384]{2,1,0:T(8,128)(2,1)}, bf16[8,512,1024]{2,1,0:T(8,128)(2,1)}) custom-call(bf16[192,1024]{1,0:T(8,128)(2,1)} %fusion.2.x, bf16[16,192,384]{2,1,0:T(8,128)(2,1)} %pack.1.msgs, bf16[512,1024]{1,0:T(8,128)(2,1)} %bitcast.61), custom_call_target="tpu_custom_call" | custom-call | flops 8000000000 | bytes 8000000 | tf_op jit(solution)/shard_map/pallas_call | solution.py:556
  106.0 3.3 %convolution_convert_fusion.q2_ref.k2_ref = bf16[3072,384]{1,0:T(8,128)(2,1)} fusion(bf16[128,384]{1,0:T(8,128)(2,1)S(1)} %copy-done.4, bf16[3072,384]{1,0:T(8,128)(2,1)} %bitcast.51), kind=kOutput, calls=%fused_computation | convolution fusion | flops 303169536 | bytes 3244032 | tf_op jit(solution)/shard_map/dot_general | solution.py:609
  109.3 4.8 %convolution_convert_fusion.1.kv_ref = bf16[3072,256]{1,0:T(8,128)(2,1)S(1)} fusion(bf16[3072,1024]{1,0:T(8,128)(2,1)} %bitcast.54, bf16[256,1024]{1,0:T(8,128)(2,1)S(1)} %collective-permute-done), kind=kOutput, calls=%fused_computation.1 | convolution fusion | flops 1611399168 | bytes 8388608 | tf_op jit(solution)/shard_map/dot_general | solution.py:612
  114.1 30.2 %attention.3 = bf16[3072,256]{1,0:T(8,128)(2,1)S(1)} custom-call(bf16[3072,384]{1,0:T(8,128)(2,1)S(1)} %bitcast.52, bf16[3072,384]{1,0:T(8,128)(2,1)} %convolution_convert_fusion.q2_ref.k2_ref, bf16[3072,256]{1,0:T(8,128)(2,1)S(1)} %convolution_convert_fusion.1.kv_ref, bf16[3072,384]{1,0:T(8,128)(2,1)} %convolution_convert_fusion.q2_ref.k2_ref), custom_call_target="tpu_custom_call" | custom-call | flops 12000000000 | bytes 8000000 | tf_op jit(solution)/shard_map/attention/pallas_call | solution.py:209
  144.3 31.1 %attention.2 = bf16[3072,256]{1,0:T(8,128)(2,1)} custom-call(bf16[3072,384]{1,0:T(8,128)(2,1)S(1)} %bitcast.53, bf16[3072,384]{1,0:T(8,128)(2,1)} %convolution_convert_fusion.q2_ref.k2_ref, bf16[3072,256]{1,0:T(8,128)(2,1)S(1)} %convolution_convert_fusion.1.kv_ref, bf16[3072,384]{1,0:T(8,128)(2,1)} %convolution_convert_fusion.q2_ref.k2_ref), custom_call_target="tpu_custom_call" | custom-call | flops 12000000000 | bytes 8000000 | tf_op jit(solution)/shard_map/attention/pallas_call | solution.py:209
  175.4 2.1 fusion.5
  177.6 12.1 %all-to-all-start = ((bf16[16,192,256]{2,1,0:T(8,128)(2,1)}), bf16[16,192,256]{2,1,0:T(8,128)(2,1)}, u32[]{:S(2)}, u32[]{:S(2)}) async-start(bf16[16,192,256]{2,1,0:T(8,128)(2,1)} %bitcast.13), calls=%async_computation | async-start | bytes 3145728 | tf_op jit(solution)/shard_map/all_to_all | solution.py:573
  189.7 3.8 %multiply_reduce_fusion = (f32[1024]{0:T(1024)S(1)}, f32[1024]{0:T(1024)S(1)}, f32[128,1024]{1,0:T(8,128)S(1)}) fusion(bf16[256,1024]{1,0:T(8,128)(2,1)S(1)} %collective-permute-done, f32[128,1024]{1,0:T(8,128)S(1)} %fusion.5, bf16[3072,1024]{1,0:T(8,128)(2,1)} %bitcast.55, bf16[3072,256]{1,0:T(8,128)(2,1)S(1)} %attention.3), kind=kOutput, calls=%fused_computation.17 | convolution fusion | flops 806090752 | bytes 8658944 | tf_op jit(solution)/shard_map/dot_general | solution.py:617
  194.3 1.0 pad_maximum_fusion.1.pieces
  195.3 33.3 %shard_map.164 = (bf16[16,192,256]{2,1,0:T(8,128)(2,1)}, f32[8,32,1024]{2,1,0:T(8,128)}, f32[16,8,128]{2,1,0:T(8,128)}) custom-call(bf16[16,192,256]{2,1,0:T(8,128)(2,1)} %bitcast.50, f32[8,32,1024]{2,1,0:T(8,128)} %pad_maximum_fusion.1.pieces, f32[8,128]{1,0:T(8,128)} %divide_bitcast_fusion.gain), custom_call_target="tpu_custom_call" | custom-call | flops 8000000000 | bytes 8000000 | tf_op jit(solution)/shard_map/pallas_call | solution.py:556
  228.6 1.3 reduce_sum.57
  230.6 1.5 reduce_sum.58.gain
  232.7 30.9 %shard_map.165 = (bf16[16,32,1024]{2,1,0:T(8,128)(2,1)}, f32[8,8,128]{2,1,0:T(8,128)}) custom-call(bf16[32,1024]{1,0:T(8,128)(2,1)} %copy-done.7, f32[8,128]{1,0:T(8,128)} %reduce_sum.58.gain), custom_call_target="tpu_custom_call" | custom-call | flops 8000000000 | bytes 8000000 | tf_op jit(solution)/shard_map/pallas_call | solution.py:556
  263.6 1.4 reduce_sum.59
  264.9 1.5 convert_bitcast_fusion
  266.7 1.0 copy.24
  267.7 1.0 copy.23
  268.8 10.8 %finish.1 = (bf16[192,3072]{1,0:T(8,128)(2,1)}, f32[192,1024]{1,0:T(8,128)}, f32[192,128]{1,0:T(8,128)}) custom-call(bf16[16,192,256]{2,1,0:T(8,128)(2,1)} %all-to-all-done.ret0, bf16[16,192,256]{2,1,0:T(8,128)(2,1)} %get-tuple-element.19.ret1, bf16[16,256,1024]{2,1,0:T(8,128)(2,1)} %bitcast.74, bf16[512,384]{1,0:T(8,128)(2,1)} %constant.80.clone.place, ...), custom_call_target="tpu_custom_call" | custom-call | flops 4000000000 | bytes 14000000 | tf_op jit(solution)/shard_map/finish/pallas_call | solution.py:276
  279.5 1.0 slice_bitcast_fusion
  280.5 0.7 copy.25
  (36 shorter events, 3.9 us)
Async XLA Ops:
  0.6 2.2 copy-start.3
  0.6 2.4 copy-start.6
  0.7 4.2 %copy-start.5 = (f32[1024]{0:T(1024)S(1)}, f32[1024]{0:T(1024)}, u32[]{:S(2)}) copy-start(f32[1024]{0:T(1024)} %param.15) | copy-start | bytes 12292
  2.0 11.7 %copy-start.2 = (bf16[2,2,2,64,1024]{4,3,2,1,0:T(8,128)(2,1)}, bf16[2,2,2,64,1024]{4,3,2,1,0:T(8,128)(2,1)S(1)}, u32[]{:S(2)}) copy-start(bf16[2,2,2,64,1024]{4,3,2,1,0:T(8,128)(2,1)S(1)} %pad_maximum_fusion) | copy-start | bytes 3145732
  2.1 107.2 %collective-permute-start = (bf16[256,1024]{1,0:T(8,128)(2,1)S(1)}, bf16[256,1024]{1,0:T(8,128)(2,1)S(1)}, u32[]{:S(2)}, u32[]{:S(2)}) collective-permute-start(bf16[256,1024]{1,0:T(8,128)(2,1)S(1)} %dynamic-slice_bitcast_fusion), channel_id=1, source_target_pairs={{0,0},{64,8},{8,1},{72,9},{16,2},{80,10},{24,3},{88,11},{32,4},{96... | collective-permute-start | bytes 1572872 | tf_op jit(solution)/shard_map/ppermute | solution.py:587
  13.7 92.3 %copy-start.4 = (bf16[128,384]{1,0:T(8,128)(2,1)S(1)}, bf16[128,384]{1,0:T(8,128)(2,1)}, u32[]{:S(2)}) copy-start(bf16[128,384]{1,0:T(8,128)(2,1)} %constant.79.clone) | copy-start | bytes 294916
  109.3 4.8 %copy-start.1 = (bf16[16,192,384]{2,1,0:T(8,128)(2,1)S(1)}, bf16[16,192,384]{2,1,0:T(8,128)(2,1)}, u32[]{:S(2)}) copy-start(bf16[16,192,384]{2,1,0:T(8,128)(2,1)} %get-tuple-element.17) | copy-start | bytes 7077892
  109.3 66.1 %slice-start = ((s8[6291456]{0:T(1024)(128)(4,1)}), s8[4194304]{0:T(1024)(128)(4,1)S(1)}, s32[]{:S(2)}) async-start(s8[6291456]{0:T(1024)(128)(4,1)} %bitcast.56), calls=%async_computation.1 | async-start | bytes 8388608
  114.1 61.3 %slice-start.1 = ((s8[6291456]{0:T(1024)(128)(4,1)}), s8[2097152]{0:T(1024)(128)(4,1)S(1)}, s32[]{:S(2)}) async-start(s8[6291456]{0:T(1024)(128)(4,1)} %bitcast.56), calls=%async_computation.2 | async-start | bytes 4194304
  144.3 45.4 %copy-start = (bf16[3072,256]{1,0:T(8,128)(2,1)}, bf16[3072,256]{1,0:T(8,128)(2,1)S(1)}, u32[]{:S(2)}) copy-start(bf16[3072,256]{1,0:T(8,128)(2,1)S(1)} %attention.3) | copy-start | bytes 4718596
  177.6 91.2 %all-to-all-start = ((bf16[16,192,256]{2,1,0:T(8,128)(2,1)}), bf16[16,192,256]{2,1,0:T(8,128)(2,1)}, u32[]{:S(2)}, u32[]{:S(2)}) async-start(bf16[16,192,256]{2,1,0:T(8,128)(2,1)} %bitcast.13), calls=%async_computation | async-start | bytes 3145728 | tf_op jit(solution)/shard_map/all_to_all | solution.py:573
  229.9 2.1 collective-permute-start.1
  232.0 0.6 copy-start.7
